TPU v7x, 256 devices: a whole 4x4x8 slice. The times are simulated.
256 devices in a mesh: sp: 64 (over z, y, core), tp: 4 (over x).
Axes of the slice: x: 4, y: 4, z: 8, core: 2. Of those that a mesh axis runs over, the one named last changes fastest.
Arguments:
- queries: bfloat16 [8192, 1280], P('sp', 'tp'), may hold values from -4000 to 4000
- latents: bfloat16 [8192, 512], P('sp'), may hold values from -6 to 6
- shared_key: bfloat16 [8192, 64], P('sp'), may hold values from -4 to 4
- expand_weight: bfloat16 [512, 1536], P(None, 'tp'), may hold values from -0.25 to 0.25
- residual: bfloat16 [8192, 2048], P('sp'), may hold values from -3 to 3
- out_weight: bfloat16 [768, 2048], replicated, may hold values from -0.21875 to 0.21875
- norm_gain: bfloat16 [2048], replicated, may hold values from 0.099609375 to 1.8984375
- gate_weight: bfloat16 [2048, 3072], P('sp', 'tp'), may hold values from -0.125 to 0.125
- value_weight: bfloat16 [2048, 3072], P('sp', 'tp'), may hold values from -0.125 to 0.125
- conv_weight: bfloat16 [3, 3072], P(None, 'tp'), may hold values from -3.5 to 3.5
- down_weight: bfloat16 [3072, 2048], P('tp', 'sp'), may hold values from -0.109375 to 0.109375
Outputs:
- output: bfloat16 [8192, 2048], P(('sp', 'tp'))
All inputs are finite; a program needn't handle non-finite values.
Results may differ from a plain program's by a relative error of at most 0.018.
Values may be sent and summed in bfloat16 or wider, within the bound.
No kernel may reach another device: no remote copies, remote signals or barrier semaphores. Data moves between devices by JAX's collectives and lax.ppermute only.
A program may use at most 128 MiB of HBM per device.

v0:
```python
import functools

import jax
import jax.numpy as jnp
from jax import lax
from jax.experimental import pallas as pl
from jax.experimental.pallas import tpu as pltpu
from jax.sharding import Mesh
from jax.sharding import PartitionSpec as P

NOPE_A = 128
NOPE_B = 64
ROPE = 64
Z, Y, C, X = 8, 4, 2, 4
SP = ("z", "y", "c")
SP_TP = ("z", "y", "c", "x")
LOG2E = 1.4426950408889634
ROWS = 144
BF = jnp.bfloat16
F32 = jnp.float32


def limit(mib):
    return pltpu.CompilerParams(vmem_limit_bytes=mib * 1024 * 1024)


def shift(x, axis, k):
    n = lax.axis_size(axis)
    return lax.ppermute(x, axis, [(i, (i + k) % n) for i in range(n)])


def swap(x):
    return lax.ppermute(x, "c", [(0, 1), (1, 0)])


def tables(positions, width):
    half_width = width // 2
    frequency = 10000.0 ** (-jnp.arange(half_width, dtype=F32) / half_width)
    angles = positions.astype(F32)[:, None] * frequency[None, :]
    return (jnp.cos(angles), jnp.sin(angles))


def rotate(vectors, cos_table, sine_table):
    half_width = vectors.shape[-1] // 2
    a = vectors[:, :half_width].astype(F32)
    b = vectors[:, half_width:].astype(F32)
    turned = jnp.concatenate(
        [a * cos_table - b * sine_table, b * cos_table + a * sine_table], axis=1
    )
    return turned.astype(BF)


def split3(v):
    hi = v.astype(BF)
    r = v - hi.astype(F32)
    mid = r.astype(BF)
    lo = (r - mid.astype(F32)).astype(BF)
    return [hi.astype(F32), mid.astype(F32), lo.astype(F32)]


def attend_kernel(nq, nk, *refs):
    qs, ks, outs = refs[:nq], refs[nq : nq + nk], refs[nq + nk :]
    keys = jnp.concatenate([k[:, 0:256] for k in ks], axis=0)
    values = jnp.concatenate([k[:, 256:512] for k in ks], axis=0)
    cw = float((NOPE_A + ROPE) ** -0.5 * LOG2E)
    cn = float((NOPE_B + ROPE) ** -0.5 * LOG2E)
    nt = (((1,), (1,)), ((), ()))
    lane = lax.broadcasted_iota(jnp.int32, (ROWS, 128), 1)
    for q, o in zip(qs, outs):
        sw = lax.dot_general(q[:, 0:256], keys, nt, preferred_element_type=F32)
        mw = jnp.max(sw, axis=1, keepdims=True)
        pw = jnp.exp2((sw - mw) * cw).astype(BF)
        ow = jnp.dot(pw, values, preferred_element_type=F32)
        sn = lax.dot_general(q[:, 256:384], keys[:, 128:256], nt, preferred_element_type=F32)
        mn = jnp.max(sn, axis=1, keepdims=True)
        pn = jnp.exp2((sn - mn) * cn).astype(BF)
        on = jnp.dot(pn, values[:, 128:256], preferred_element_type=F32)
        lw = ow[:, 192:193]
        ln = on[:, 64:65]
        second = on / ln
        pieces = split3(mw * cw) + split3(lw) + split3(mn * cn) + split3(ln)
        for at, piece in enumerate(pieces):
            second = jnp.where(lane == 64 + at, piece, second)
        o[:, 0:128] = (ow[:, 0:128] / lw).astype(BF)
        o[:, 128:256] = second.astype(BF)


def attend(q_blocks, k_blocks):
    nq, nk = len(q_blocks), len(k_blocks)
    return pl.pallas_call(
        functools.partial(attend_kernel, nq, nk),
        out_shape=[jax.ShapeDtypeStruct((ROWS, 256), BF)] * nq,
        name="attend", compiler_params=limit(24),
    )(*q_blocks, *k_blocks)


def join_kernel(*refs):
    parts, out = refs[:-1], refs[-1]
    seconds = [p[:, 128:256].astype(F32) for p in parts]

    def stat(at):
        return [s[:, at : at + 1] + s[:, at + 1 : at + 2] + s[:, at + 2 : at + 3] for s in seconds]

    def weights(ms, ls):
        top = functools.reduce(jnp.maximum, ms)
        ws = [jnp.exp2(m - top) * l for m, l in zip(ms, ls)]
        total = functools.reduce(jnp.add, ws)
        return [w / total for w in ws]

    ww = weights(stat(64), stat(67))
    wn = weights(stat(70), stat(73))
    wide = functools.reduce(jnp.add, [w * p[:, 0:128].astype(F32) for w, p in zip(ww, parts)])
    narrow = functools.reduce(jnp.add, [w * s for w, s in zip(wn, seconds)])
    lane = lax.broadcasted_iota(jnp.int32, (ROWS, 128), 1)
    out[:, 0:128] = wide.astype(BF)
    out[:, 128:256] = jnp.where(lane < 64, narrow, 0.0).astype(BF)


def join(parts):
    return pl.pallas_call(
        join_kernel, out_shape=jax.ShapeDtypeStruct((ROWS, 256), BF), name="join", compiler_params=limit(4)
    )(*parts)


def project_kernel(meta, *refs):
    parts = refs[:X]
    out_weight, residual, halo, gain, stream_own, normed, stream = refs[X:]
    x = meta[0]
    total = None
    for k, part in enumerate(parts):
        first = pl.multiple_of(lax.rem(x + k, X) * 192, 64)
        d = jnp.dot(part[:, 0:192], out_weight[pl.ds(first, 192), :], preferred_element_type=F32)
        total = d if total is None else total + d
    res = jnp.concatenate([residual[...], halo[...]], axis=0).astype(F32)
    s = (res + total).astype(BF)
    stream[...] = s
    s = s.astype(F32)
    n = s * lax.rsqrt(jnp.mean(s * s, axis=1, keepdims=True) + 1e-06) * gain[...].astype(F32)
    row = lax.broadcasted_iota(jnp.int32, (ROWS, 1), 0)
    n = jnp.where(row < 128 + meta[1], n, 0.0)
    normed[...] = n.astype(BF)
    stream_own[...] = stream[pl.ds(pl.multiple_of(x * 32, 32), 32), :]


def project(meta, parts, out_weight, residual, halo, gain):
    vmem = pl.BlockSpec(memory_space=pltpu.VMEM)
    return pl.pallas_call(
        project_kernel,
        in_specs=[pl.BlockSpec(memory_space=pltpu.SMEM)] + [vmem] * 8,
        out_shape=[
            jax.ShapeDtypeStruct((32, 2048), BF),
            jax.ShapeDtypeStruct((ROWS, 2048), BF),
        ],
        scratch_shapes=[pltpu.VMEM((ROWS, 2048), BF)],
        name="project", compiler_params=limit(16),
    )(meta, *parts, out_weight, residual, halo, gain)


def mixer_kernel(meta, own, other, taps, *refs):
    parts, (keep, send, gates, values, downs) = refs[:-5], refs[-5:]
    z, c, y = meta[2], meta[3], meta[4]
    for part, off in zip(parts, OFFSETS):
        for k in range(Y):
            at = (lax.rem(z + off, Z) * Y + lax.rem(y + k, Y)) * 64
            rows = pl.ds(pl.multiple_of(at, 64), 64)
            for m, to in enumerate((gates, values, downs)):
                first = k * 192 + m * 64
                to[rows, :] = part[first : first + 64, :]
    both = jnp.concatenate([own[...], other[...]], axis=0)
    gate = jnp.dot(both, gates[...], preferred_element_type=F32).astype(BF).astype(F32)
    value = jnp.dot(both, values[...], preferred_element_type=F32).astype(BF).astype(F32)
    ga, gb = gate[0:128], gate[ROWS : ROWS + 128]
    ha, hb = gate[128:129], gate[ROWS + 128 : ROWS + 129]
    va, vb = value[0:128], value[ROWS : ROWS + 128]
    t0 = taps[0:1, :].astype(F32)
    t1 = taps[1:2, :].astype(F32)
    t2 = taps[2:3, :].astype(F32)
    row = lax.broadcasted_iota(jnp.int32, (128, 1), 0)
    low = c == 0

    def mixed(g, before, behind, v):
        prev = jnp.where(row == 0, before, pltpu.roll(g, 1, 0))
        nxt = jnp.where(row == 127, behind, pltpu.roll(g, 127, 0))
        m = prev * t0 + g * t1 + nxt * t2
        return (m / (1.0 + jnp.exp(-m)) * v).astype(BF)

    aa = mixed(ga, jnp.where(low, ha, gb[127:128]), jnp.where(low, gb[0:1], ha), va)
    ab = mixed(gb, jnp.where(low, ga[127:128], hb), jnp.where(low, hb, ga[0:1]), vb)
    act = jnp.concatenate([aa, ab], axis=0)
    d = lax.dot_general(act, downs[...], (((1,), (1,)), ((), ())), preferred_element_type=F32)
    keep[...] = d[0:128]
    send[...] = d[128:256].astype(BF)


OFFSETS = (0, 7, 1, 6, 2, 5, 3, 4)


def mixer(meta, own, other, taps, parts):
    vmem = pl.BlockSpec(memory_space=pltpu.VMEM)
    return pl.pallas_call(
        mixer_kernel,
        in_specs=[pl.BlockSpec(memory_space=pltpu.SMEM)] + [vmem] * (3 + len(parts)),
        out_shape=[
            jax.ShapeDtypeStruct((128, 2048), F32),
            jax.ShapeDtypeStruct((128, 2048), BF),
        ],
        scratch_shapes=[pltpu.VMEM((2048, 384), BF)] * 3,
        name="mixer",
        compiler_params=limit(20),
    )(meta, own, other, taps, *parts)


def body(
    queries,
    latents,
    shared_key,
    expand_weight,
    residual,
    out_weight,
    norm_gain,
    gate_weight,
    value_weight,
    conv_weight,
    down_weight,
):
    z, y, c, x = (lax.axis_index(a) for a in ("z", "y", "c", "x"))
    s = lax.axis_index(SP)
    tok = queries.shape[0]
    lat2 = jnp.concatenate([latents, swap(latents)], axis=0)
    sk2 = jnp.concatenate([shared_key, swap(shared_key)], axis=0)
    own_pos = s * tok + jnp.arange(tok, dtype=jnp.int32)
    other_pos = (s + 1 - 2 * c) * tok + jnp.arange(tok, dtype=jnp.int32)
    cos2, sin2 = tables(jnp.concatenate([own_pos, other_pos]), ROPE)
    cos, sin = cos2[:tok], sin2[:tok]
    ew = expand_weight
    expanded = jnp.dot(lat2, ew, preferred_element_type=F32).astype(BF)
    turned = rotate(sk2, cos2, sin2)
    ones = jnp.broadcast_to(
        (jnp.arange(64) == 0).astype(BF)[None, :], (2 * tok, 64)
    )
    kv = jnp.concatenate(
        [
            expanded[:, 0:128],
            turned,
            expanded[:, 256:320],
            expanded[:, 128:256],
            expanded[:, 320:384],
            ones,
        ],
        axis=1,
    )
    rot0 = NOPE_A + NOPE_B
    q = jnp.concatenate(
        [
            queries[:, 0:128],
            rotate(queries[:, rot0 : rot0 + 64], cos, sin),
            jnp.zeros((tok, 64), BF),
            rotate(queries[:, rot0 + 64 : rot0 + 128], cos, sin),
            queries[:, 128:192],
        ],
        axis=1,
    )
    nsp = Z * Y * C
    pairs = [(i, i + 1) for i in range(1, nsp - 1, 2)] + [(i, i - 1) for i in range(2, nsp, 2)]
    edge = jnp.concatenate([q, residual], axis=1)
    edge = jnp.where(c == 1, edge[tok - 1 : tok], edge[0:1])
    edge = lax.ppermute(edge, SP, pairs)
    edge = jnp.pad(edge, ((0, 15), (0, 0)))
    q = jnp.concatenate([q, edge[:, :384]], axis=0)
    halo_res = edge[:, 384:]
    ring = [(2 * i, 2 * ((i + 1) % Z)) for i in range(Z)]
    ring += [(2 * i + 1, 2 * ((i - 1) % Z) + 1) for i in range(Z)]

    def step(v):
        return lax.ppermute(v, ("z", "c"), ring)

    r1 = step(kv)
    mats = (gate_weight, value_weight, down_weight.T)
    lo = jnp.concatenate([m[:, :384] for m in mats], axis=0)
    hi = jnp.concatenate([m[:, 384:] for m in mats], axis=0)
    wk = jnp.where(c == 0, lo, hi)
    wr = swap(jnp.where(c == 0, hi, lo))
    wa, wb = jnp.where(c == 0, wk, wr), jnp.where(c == 0, wr, wk)
    w = jnp.concatenate([v[32 * m : 32 * m + 32] for m in range(3) for v in (wa, wb)], axis=0)
    qw = jnp.concatenate([q, w], axis=0)
    got = [qw] + [shift(qw, "y", k) for k in (1, 2, 3)]
    q_blocks = [v[:ROWS] for v in got]
    w = jnp.concatenate([got[-k % Y][ROWS:] for k in range(Y)], axis=0)
    r2 = step(r1)
    r3 = step(r2)
    r4 = step(r3[:tok])
    k_blocks = [kv, r1, swap(r1), r2, swap(r2), r3, swap(r3)]
    k_blocks += [r4, swap(r4)]
    f1, b1 = shift(w, "z", 1), shift(w, "z", -1)
    f2, b2 = shift(f1, "z", 1), shift(b1, "z", -1)
    f3, b3 = shift(f2, "z", 1), shift(b2, "z", -1)
    o4 = jnp.concatenate([shift(f3[:384], "z", 1), shift(b3[384:], "z", -1)], axis=0)
    ws = [w, f1, b1, f2, b2, f3, b3, o4]
    o = attend(q_blocks, k_blocks)
    parts = [o[0]] + [shift(o[k], "y", -k) for k in (1, 2, 3)]
    attended = join(parts)
    heads = [attended] + [shift(attended, "x", -k) for k in (1, 2, 3)]
    valid = jnp.where(c == 0, s > 0, s < nsp - 1).astype(jnp.int32)
    meta = jnp.stack([x, valid, z, c, y]).astype(jnp.int32)
    stream_own, normed = project(
        meta, heads, out_weight, residual, halo_res, norm_gain.reshape(1, -1)
    )
    other = swap(normed)
    taps = jnp.where(c == 0, conv_weight[:, :384], conv_weight[:, 384:])
    keep, send = mixer(meta, normed, other, taps, ws)
    total = keep + swap(send).astype(F32)
    tb = total.astype(BF)
    got = []
    for k in (1, 2, 3):
        piece = lax.dynamic_slice_in_dim(tb, lax.rem(x + k, X) * 32, 32, 0)
        got.append(shift(piece, "x", k))
    mine = lax.dynamic_slice_in_dim(total, x * 32, 32, 0)
    summed = mine + got[0].astype(F32) + got[1].astype(F32) + got[2].astype(F32)
    return (stream_own.astype(F32) + summed).astype(BF)


def solution(mesh):
    split = Mesh(mesh.devices.reshape(Z, Y, C, X), SP_TP)
    placed = (
        P(SP, "x"),
        P(SP, None),
        P(SP, None),
        P(None, "x"),
        P(SP, None),
        P(),
        P(),
        P(SP, "x"),
        P(SP, "x"),
        P(None, "x"),
        P("x", SP),
    )

    return jax.shard_map(
        body, mesh=split, in_specs=placed, out_specs=P(SP_TP, None), check_vma=False
    )
```

profile of v0, /device:TPU:32, one launch (start us, length us, event | category | flops | bytes accessed | tf_op | source)
XLA Modules:
  0.0 145.7 jit_solution(2905505509582467542)
XLA Ops:
  7.5 4.5 %collective-permute-start = (bf16[1,2432]{1,0:T(2,128)(2,1)S(1)}, bf16[1,2432]{1,0:T(2,128)(2,1)S(1)}, u32[]{:S(2)}, u32[]{:S(2)}) collective-permute-start(bf16[1,2432]{1,0:T(2,128)(2,1)S(1)} %broadcast_select_fusion.4), channel_id=1, source_target_pairs={{4,8},{12,16},{20,24},{28,32},{36,40},{44,48},{52,56},{60,64},{68,... | collective-permute-start | bytes 14600 | tf_op jit(solution)/shard_map/ppermute | solution.py:267
  12.0 2.6 %collective-permute-done = bf16[1,2432]{1,0:T(2,128)(2,1)S(1)} collective-permute-done((bf16[1,2432]{1,0:T(2,128)(2,1)S(1)}, bf16[1,2432]{1,0:T(2,128)(2,1)S(1)}, u32[]{:S(2)}, u32[]{:S(2)}) %collective-permute-start) | collective-permute-done | bytes 4896 | tf_op jit(solution)/shard_map/ppermute | solution.py:267
  17.7 8.5 %collective-permute-done.4 = bf16[336,384]{1,0:T(8,128)(2,1)S(1)} collective-permute-done((bf16[336,384]{1,0:T(8,128)(2,1)S(1)}, bf16[336,384]{1,0:T(8,128)(2,1)S(1)}, u32[]{:S(2)}, u32[]{:S(2)}) %collective-permute-start.4) | collective-permute-done | bytes 258080 | tf_op jit(solution)/shard_map/ppermute | solution.py:29
  26.3 5.6 %collective-permute-done.2 = bf16[336,384]{1,0:T(8,128)(2,1)S(1)} collective-permute-done((bf16[336,384]{1,0:T(8,128)(2,1)S(1)}, bf16[336,384]{1,0:T(8,128)(2,1)S(1)}, u32[]{:S(2)}, u32[]{:S(2)}) %collective-permute-start.2) | collective-permute-done | bytes 258080 | tf_op jit(solution)/shard_map/ppermute | solution.py:29
  31.9 2.0 %collective-permute-start.22 = (bf16[768,384]{1,0:T(8,128)(2,1)S(1)}, bf16[768,384]{1,0:T(8,128)(2,1)S(1)}, u32[]{:S(2)}, u32[]{:S(2)}) collective-permute-start(bf16[768,384]{1,0:T(8,128)(2,1)S(1)} %slice_dynamic-update-slice_fusion.refs_0_), channel_id=1, source_target_pairs={{0,32},{32,64},{64,96},{96,128},{128,160},{160,192},{192,224},{224... | collective-permute-start | bytes 1769480 | tf_op jit(solution)/shard_map/ppermute | solution.py:29
  34.3 2.0 %collective-permute-start.7 = (bf16[256,512]{1,0:T(8,128)(2,1)S(1)}, bf16[256,512]{1,0:T(8,128)(2,1)S(1)}, u32[]{:S(2)}, u32[]{:S(2)}) collective-permute-start(bf16[256,512]{1,0:T(8,128)(2,1)S(1)} %concatenate.62.refs_4_), channel_id=1, source_target_pairs={{0,32},{32,64},{64,96},{96,128},{128,160},{160,192},{192,224},{224... | collective-permute-start | bytes 786440 | tf_op jit(solution)/shard_map/ppermute | solution.py:275
  36.3 13.8 %collective-permute-done.7.refs_5_ = bf16[256,512]{1,0:T(8,128)(2,1)S(1)} collective-permute-done((bf16[256,512]{1,0:T(8,128)(2,1)S(1)}, bf16[256,512]{1,0:T(8,128)(2,1)S(1)}, u32[]{:S(2)}, u32[]{:S(2)}) %collective-permute-start.7) | collective-permute-done | bytes 262176 | tf_op jit(solution)/shard_map/ppermute | solution.py:275
  50.1 1.9 %collective-permute-start.9 = (bf16[256,512]{1,0:T(8,128)(2,1)S(1)}, bf16[256,512]{1,0:T(8,128)(2,1)S(1)}, u32[]{:S(2)}, u32[]{:S(2)}) collective-permute-start(bf16[256,512]{1,0:T(8,128)(2,1)S(1)} %collective-permute-done.7.refs_5_), channel_id=1, source_target_pairs={{0,32},{32,64},{64,96},{96,128},{128,160},{160,192},{192,224},{224... | collective-permute-start | bytes 786440 | tf_op jit(solution)/shard_map/ppermute | solution.py:275
  52.0 3.0 %collective-permute-start.24 = (bf16[768,384]{1,0:T(8,128)(2,1)S(1)}, bf16[768,384]{1,0:T(8,128)(2,1)}, u32[]{:S(2)}, u32[]{:S(2)}) collective-permute-start(bf16[768,384]{1,0:T(8,128)(2,1)S(1)} %collective-permute-done.22.refs_1_), channel_id=1, source_target_pairs={{0,32},{32,64},{64,96},{96,128},{128,160},{160,192},{192,224},{224... | collective-permute-start | bytes 1769480 | tf_op jit(solution)/shard_map/ppermute | solution.py:29
  57.6 2.8 %collective-permute-start.11 = (bf16[256,512]{1,0:T(8,128)(2,1)S(1)}, bf16[256,512]{1,0:T(8,128)(2,1)S(1)}, u32[]{:S(2)}, u32[]{:S(2)}) collective-permute-start(bf16[256,512]{1,0:T(8,128)(2,1)S(1)} %collective-permute-done.9.refs_7_), channel_id=1, source_target_pairs={{0,32},{32,64},{64,96},{96,128},{128,160},{160,192},{192,224},{224... | collective-permute-start | bytes 786440 | tf_op jit(solution)/shard_map/ppermute | solution.py:275
  60.4 11.6 %collective-permute-done.11.refs_9_ = bf16[256,512]{1,0:T(8,128)(2,1)S(1)} collective-permute-done((bf16[256,512]{1,0:T(8,128)(2,1)S(1)}, bf16[256,512]{1,0:T(8,128)(2,1)S(1)}, u32[]{:S(2)}, u32[]{:S(2)}) %collective-permute-start.11) | collective-permute-done | bytes 262176 | tf_op jit(solution)/shard_map/ppermute | solution.py:275
  71.9 2.7 %collective-permute-start.13 = (bf16[128,512]{1,0:T(8,128)(2,1)S(1)}, bf16[128,512]{1,0:T(8,128)(2,1)S(1)}, u32[]{:S(2)}, u32[]{:S(2)}) collective-permute-start(bf16[128,512]{1,0:T(8,128)(2,1)S(1)} %slice.191), channel_id=1, source_target_pairs={{0,32},{32,64},{64,96},{96,128},{128,160},{160,192},{192,224},{224... | collective-permute-start | bytes 393224 | tf_op jit(solution)/shard_map/ppermute | solution.py:275
  75.4 3.0 %collective-permute-done.13.refs_11_ = bf16[128,512]{1,0:T(8,128)(2,1)S(1)} collective-permute-done((bf16[128,512]{1,0:T(8,128)(2,1)S(1)}, bf16[128,512]{1,0:T(8,128)(2,1)S(1)}, u32[]{:S(2)}, u32[]{:S(2)}) %collective-permute-start.13) | collective-permute-done | bytes 131104 | tf_op jit(solution)/shard_map/ppermute | solution.py:275
  78.3 1.9 %collective-permute-start.14 = (bf16[128,512]{1,0:T(8,128)(2,1)S(1)}, bf16[128,512]{1,0:T(8,128)(2,1)S(1)}, u32[]{:S(2)}, u32[]{:S(2)}) collective-permute-start(bf16[128,512]{1,0:T(8,128)(2,1)S(1)} %collective-permute-done.13.refs_11_), channel_id=1, source_target_pairs={{0,4},{4,0},{1,5},{5,1},{2,6},{6,2},{3,7},{7,3},{8,12},{12,8},{9,1... | collective-permute-start | bytes 393224 | tf_op jit(solution)/shard_map/ppermute | solution.py:33
  80.2 2.3 %collective-permute-start.26 = (bf16[768,384]{1,0:T(8,128)(2,1)}, bf16[768,384]{1,0:T(8,128)(2,1)}, u32[]{:S(2)}, u32[]{:S(2)}) collective-permute-start(bf16[768,384]{1,0:T(8,128)(2,1)} %collective-permute-done.24.refs_3_), channel_id=1, source_target_pairs={{0,32},{32,64},{64,96},{96,128},{128,160},{160,192},{192,224},{224... | collective-permute-start | bytes 1769480 | tf_op jit(solution)/shard_map/ppermute | solution.py:29
  82.6 1.1 slice.184.refs_3_
  84.6 5.2 %attend.1 = (bf16[144,256]{1,0:T(8,128)(2,1)S(1)}, bf16[144,256]{1,0:T(8,128)(2,1)}, bf16[144,256]{1,0:T(8,128)(2,1)}, bf16[144,256]{1,0:T(8,128)(2,1)}) custom-call(bf16[144,384]{1,0:T(8,128)(2,1)S(1)} %pad_maximum_fusion.1.refs_0_, bf16[144,384]{1,0:T(8,128)(2,1)S(1)} %slice.182.refs_1_, bf16[144,384]{1,0:T(8,128)(2,1)S(1)} %slice.183.refs_2_, ...), custom_call_target="tpu_custom_call" | custom-call | tf_op jit(solution)/shard_map/attend/pallas_call | solution.py:90
  92.7 2.9 %collective-permute-done.15.refs_1_ = bf16[144,256]{1,0:T(8,128)(2,1)} collective-permute-done((bf16[144,256]{1,0:T(8,128)(2,1)}, bf16[144,256]{1,0:T(8,128)(2,1)}, u32[]{:S(2)}, u32[]{:S(2)}) %collective-permute-start.15) | collective-permute-done | bytes 73760 | tf_op jit(solution)/shard_map/ppermute | solution.py:29
  95.5 1.9 %collective-permute-done.16.refs_2_ = bf16[144,256]{1,0:T(8,128)(2,1)} collective-permute-done((bf16[144,256]{1,0:T(8,128)(2,1)}, bf16[144,256]{1,0:T(8,128)(2,1)}, u32[]{:S(2)}, u32[]{:S(2)}) %collective-permute-start.16) | collective-permute-done | bytes 73760 | tf_op jit(solution)/shard_map/ppermute | solution.py:29
  98.9 1.4 join.1.refs_0_
  100.3 2.8 %collective-permute-start.18 = (bf16[144,256]{1,0:T(8,128)(2,1)S(1)}, bf16[144,256]{1,0:T(8,128)(2,1)S(1)}, u32[]{:S(2)}, u32[]{:S(2)}) collective-permute-start(bf16[144,256]{1,0:T(8,128)(2,1)S(1)} %join.1.refs_0_), channel_id=1, source_target_pairs={{0,3},{1,0},{2,1},{3,2},{4,7},{5,4},{6,5},{7,6},{8,11},{9,8},{10,9... | collective-permute-start | bytes 221192 | tf_op jit(solution)/shard_map/ppermute | solution.py:29
  105.6 3.5 %collective-permute-done.19.refs_2_ = bf16[144,256]{1,0:T(8,128)(2,1)S(1)} collective-permute-done((bf16[144,256]{1,0:T(8,128)(2,1)S(1)}, bf16[144,256]{1,0:T(8,128)(2,1)S(1)}, u32[]{:S(2)}, u32[]{:S(2)}) %collective-permute-start.19) | collective-permute-done | bytes 73760 | tf_op jit(solution)/shard_map/ppermute | solution.py:29
  110.8 1.6 %project.1 = (bf16[32,2048]{1,0:T(8,128)(2,1)S(1)}, bf16[144,2048]{1,0:T(8,128)(2,1)S(1)}) custom-call(s32[5]{0:T(128)S(1)} %stack.27.meta, bf16[144,256]{1,0:T(8,128)(2,1)S(1)} %join.1.refs_0_, bf16[144,256]{1,0:T(8,128)(2,1)S(1)} %collective-permute-done.18.refs_1_, bf16[144,256]{1,0:T(8,128)(2,1)S(1)} %collective-permute-done.19.refs_2_, ...), custom_call_target="tpu_custom_call" | custom-call | tf_op jit(solution)/shard_map/project/pallas_call | solution.py:147
  112.6 1.1 slice.195
  113.7 3.0 %collective-permute-start.28 = (bf16[384,384]{1,0:T(8,128)(2,1)S(1)}, bf16[384,384]{1,0:T(8,128)(2,1)S(1)}, u32[]{:S(2)}, u32[]{:S(2)}) collective-permute-start(bf16[384,384]{1,0:T(8,128)(2,1)S(1)} %slice.195), channel_id=1, source_target_pairs={{0,32},{32,64},{64,96},{96,128},{128,160},{160,192},{192,224},{224... | collective-permute-start | bytes 884744 | tf_op jit(solution)/shard_map/ppermute | solution.py:29
  117.9 6.0 %collective-permute-done.28 = bf16[384,384]{1,0:T(8,128)(2,1)S(1)} collective-permute-done((bf16[384,384]{1,0:T(8,128)(2,1)S(1)}, bf16[384,384]{1,0:T(8,128)(2,1)S(1)}, u32[]{:S(2)}, u32[]{:S(2)}) %collective-permute-start.28) | collective-permute-done | bytes 294944 | tf_op jit(solution)/shard_map/ppermute | solution.py:29
  123.9 4.5 %collective-permute-done.29 = bf16[384,384]{1,0:T(8,128)(2,1)S(1)} collective-permute-done((bf16[384,384]{1,0:T(8,128)(2,1)S(1)}, bf16[384,384]{1,0:T(8,128)(2,1)S(1)}, u32[]{:S(2)}, u32[]{:S(2)}) %collective-permute-start.29) | collective-permute-done | bytes 294944 | tf_op jit(solution)/shard_map/ppermute | solution.py:29
  128.5 4.0 %mixer.1 = (f32[128,2048]{1,0:T(8,128)S(1)}, bf16[128,2048]{1,0:T(8,128)(2,1)S(1)}) custom-call(s32[5]{0:T(128)S(1)} %stack.27.meta, bf16[144,2048]{1,0:T(8,128)(2,1)S(1)} %get-tuple-element.18.own, bf16[144,2048]{1,0:T(8,128)(2,1)S(1)} %collective-permute-done.21.other, bf16[3,384]{1,0:T(4,128)(2,1)S(1)} %slice_select_fusion.taps, ...), custom_call_target="tpu_custom_call" | custom-call | tf_op jit(solution)/shard_map/mixer/pallas_call | solution.py:200
  132.6 1.9 %collective-permute-done.30 = bf16[128,2048]{1,0:T(8,128)(2,1)S(1)} collective-permute-done((bf16[128,2048]{1,0:T(8,128)(2,1)S(1)}, bf16[128,2048]{1,0:T(8,128)(2,1)S(1)}, u32[]{:S(2)}, u32[]{:S(2)}) %collective-permute-start.30) | collective-permute-done | bytes 524320 | tf_op jit(solution)/shard_map/ppermute | solution.py:33
  134.8 2.0 %collective-permute-start.32 = (bf16[32,2048]{1,0:T(8,128)(2,1)S(1)}, bf16[32,2048]{1,0:T(8,128)(2,1)S(1)}, u32[]{:S(2)}, u32[]{:S(2)}) collective-permute-start(bf16[32,2048]{1,0:T(8,128)(2,1)S(1)} %get-tuple-element.25), channel_id=1, source_target_pairs={{0,2},{1,3},{2,0},{3,1},{4,6},{5,7},{6,4},{7,5},{8,10},{9,11},{10,... | collective-permute-start | bytes 393224 | tf_op jit(solution)/shard_map/ppermute | solution.py:29
  136.8 1.7 %collective-permute-start.33 = (bf16[32,2048]{1,0:T(8,128)(2,1)S(1)}, bf16[32,2048]{1,0:T(8,128)(2,1)S(1)}, u32[]{:S(2)}, u32[]{:S(2)}) collective-permute-start(bf16[32,2048]{1,0:T(8,128)(2,1)S(1)} %get-tuple-element.24), channel_id=1, source_target_pairs={{0,3},{1,0},{2,1},{3,2},{4,7},{5,4},{6,5},{7,6},{8,11},{9,8},{10,9... | collective-permute-start | bytes 393224 | tf_op jit(solution)/shard_map/ppermute | solution.py:29
  138.5 5.8 %collective-permute-done.31 = bf16[32,2048]{1,0:T(8,128)(2,1)S(1)} collective-permute-done((bf16[32,2048]{1,0:T(8,128)(2,1)S(1)}, bf16[32,2048]{1,0:T(8,128)(2,1)S(1)}, u32[]{:S(2)}, u32[]{:S(2)}) %collective-permute-start.31) | collective-permute-done | bytes 131104 | tf_op jit(solution)/shard_map/ppermute | solution.py:29
  (137 shorter events, 26.7 us)
Async XLA Ops:
  0.9 5.4 %collective-permute-start.6 = (bf16[128,64]{1,0:T(8,128)(2,1)S(1)}, bf16[128,64]{1,0:T(8,128)(2,1)S(1)}, u32[]{:S(2)}, u32[]{:S(2)}) collective-permute-start(bf16[128,64]{1,0:T(8,128)(2,1)S(1)} %copy.28), channel_id=1, source_target_pairs={{0,4},{4,0},{1,5},{5,1},{2,6},{6,2},{3,7},{7,3},{8,12},{12,8},{9,1... | collective-permute-start | bytes 49160 | tf_op jit(solution)/shard_map/ppermute | solution.py:33
  2.6 12.0 %collective-permute-start.1 = (bf16[96,384]{1,0:T(8,128)(2,1)S(1)}, bf16[96,384]{1,0:T(8,128)(2,1)S(1)}, u32[]{:S(2)}, u32[]{:S(2)}) collective-permute-start(bf16[96,384]{1,0:T(8,128)(2,1)S(1)} %broadcast_select_fusion.2), channel_id=1, source_target_pairs={{0,4},{4,0},{1,5},{5,1},{2,6},{6,2},{3,7},{7,3},{8,12},{12,8},{9,1... | collective-permute-start | bytes 221192 | tf_op jit(solution)/shard_map/ppermute | solution.py:33
  3.2 14.2 %collective-permute-start.5 = (bf16[128,512]{1,0:T(8,128)(2,1)}, bf16[128,512]{1,0:T(8,128)(2,1)S(1)}, u32[]{:S(2)}, u32[]{:S(2)}) collective-permute-start(bf16[128,512]{1,0:T(8,128)(2,1)} %param.12), channel_id=1, source_target_pairs={{0,4},{4,0},{1,5},{5,1},{2,6},{6,2},{3,7},{7,3},{8,12},{12,8},{9,1... | collective-permute-start | bytes 393224 | tf_op jit(solution)/shard_map/ppermute | solution.py:33
  7.5 7.1 %collective-permute-start = (bf16[1,2432]{1,0:T(2,128)(2,1)S(1)}, bf16[1,2432]{1,0:T(2,128)(2,1)S(1)}, u32[]{:S(2)}, u32[]{:S(2)}) collective-permute-start(bf16[1,2432]{1,0:T(2,128)(2,1)S(1)} %broadcast_select_fusion.4), channel_id=1, source_target_pairs={{4,8},{12,16},{20,24},{28,32},{36,40},{44,48},{52,56},{60,64},{68,... | collective-permute-start | bytes 14600 | tf_op jit(solution)/shard_map/ppermute | solution.py:267
  14.8 11.4 %collective-permute-start.4 = (bf16[336,384]{1,0:T(8,128)(2,1)S(1)}, bf16[336,384]{1,0:T(8,128)(2,1)S(1)}, u32[]{:S(2)}, u32[]{:S(2)}) collective-permute-start(bf16[336,384]{1,0:T(8,128)(2,1)S(1)} %get-tuple-element.43), channel_id=1, source_target_pairs={{0,24},{8,0},{16,8},{24,16},{1,25},{9,1},{17,9},{25,17},{2,26},{10... | collective-permute-start | bytes 774152 | tf_op jit(solution)/shard_map/ppermute | solution.py:29
  15.8 10.5 %collective-permute-start.3 = (bf16[336,384]{1,0:T(8,128)(2,1)S(1)}, bf16[336,384]{1,0:T(8,128)(2,1)S(1)}, u32[]{:S(2)}, u32[]{:S(2)}) collective-permute-start(bf16[336,384]{1,0:T(8,128)(2,1)S(1)} %get-tuple-element.43), channel_id=1, source_target_pairs={{0,16},{8,24},{16,0},{24,8},{1,17},{9,25},{17,1},{25,9},{2,18},{10... | collective-permute-start | bytes 774152 | tf_op jit(solution)/shard_map/ppermute | solution.py:29
  16.4 15.4 %collective-permute-start.2 = (bf16[336,384]{1,0:T(8,128)(2,1)S(1)}, bf16[336,384]{1,0:T(8,128)(2,1)S(1)}, u32[]{:S(2)}, u32[]{:S(2)}) collective-permute-start(bf16[336,384]{1,0:T(8,128)(2,1)S(1)} %get-tuple-element.43), channel_id=1, source_target_pairs={{0,8},{8,16},{16,24},{24,0},{1,9},{9,17},{17,25},{25,1},{2,10},{10... | collective-permute-start | bytes 774152 | tf_op jit(solution)/shard_map/ppermute | solution.py:29
  31.9 20.2 %collective-permute-start.22 = (bf16[768,384]{1,0:T(8,128)(2,1)S(1)}, bf16[768,384]{1,0:T(8,128)(2,1)S(1)}, u32[]{:S(2)}, u32[]{:S(2)}) collective-permute-start(bf16[768,384]{1,0:T(8,128)(2,1)S(1)} %slice_dynamic-update-slice_fusion.refs_0_), channel_id=1, source_target_pairs={{0,32},{32,64},{64,96},{96,128},{128,160},{160,192},{192,224},{224... | collective-permute-start | bytes 1769480 | tf_op jit(solution)/shard_map/ppermute | solution.py:29
  33.9 22.0 %collective-permute-start.23 = (bf16[768,384]{1,0:T(8,128)(2,1)S(1)}, bf16[768,384]{1,0:T(8,128)(2,1)S(1)}, u32[]{:S(2)}, u32[]{:S(2)}) collective-permute-start(bf16[768,384]{1,0:T(8,128)(2,1)S(1)} %slice_dynamic-update-slice_fusion.refs_0_), channel_id=1, source_target_pairs={{0,224},{32,0},{64,32},{96,64},{128,96},{160,128},{192,160},{224,1... | collective-permute-start | bytes 1769480 | tf_op jit(solution)/shard_map/ppermute | solution.py:29
  34.3 15.8 %collective-permute-start.7 = (bf16[256,512]{1,0:T(8,128)(2,1)S(1)}, bf16[256,512]{1,0:T(8,128)(2,1)S(1)}, u32[]{:S(2)}, u32[]{:S(2)}) collective-permute-start(bf16[256,512]{1,0:T(8,128)(2,1)S(1)} %concatenate.62.refs_4_), channel_id=1, source_target_pairs={{0,32},{32,64},{64,96},{96,128},{128,160},{160,192},{192,224},{224... | collective-permute-start | bytes 786440 | tf_op jit(solution)/shard_map/ppermute | solution.py:275
  50.1 7.5 %collective-permute-start.9 = (bf16[256,512]{1,0:T(8,128)(2,1)S(1)}, bf16[256,512]{1,0:T(8,128)(2,1)S(1)}, u32[]{:S(2)}, u32[]{:S(2)}) collective-permute-start(bf16[256,512]{1,0:T(8,128)(2,1)S(1)} %collective-permute-done.7.refs_5_), channel_id=1, source_target_pairs={{0,32},{32,64},{64,96},{96,128},{128,160},{160,192},{192,224},{224... | collective-permute-start | bytes 786440 | tf_op jit(solution)/shard_map/ppermute | solution.py:275
  52.0 28.2 %collective-permute-start.24 = (bf16[768,384]{1,0:T(8,128)(2,1)S(1)}, bf16[768,384]{1,0:T(8,128)(2,1)}, u32[]{:S(2)}, u32[]{:S(2)}) collective-permute-start(bf16[768,384]{1,0:T(8,128)(2,1)S(1)} %collective-permute-done.22.refs_1_), channel_id=1, source_target_pairs={{0,32},{32,64},{64,96},{96,128},{128,160},{160,192},{192,224},{224... | collective-permute-start | bytes 1769480 | tf_op jit(solution)/shard_map/ppermute | solution.py:29
  55.8 26.6 %collective-permute-start.25 = (bf16[768,384]{1,0:T(8,128)(2,1)S(1)}, bf16[768,384]{1,0:T(8,128)(2,1)}, u32[]{:S(2)}, u32[]{:S(2)}) collective-permute-start(bf16[768,384]{1,0:T(8,128)(2,1)S(1)} %collective-permute-done.23.refs_2_), channel_id=1, source_target_pairs={{0,224},{32,0},{64,32},{96,64},{128,96},{160,128},{192,160},{224,1... | collective-permute-start | bytes 1769480 | tf_op jit(solution)/shard_map/ppermute | solution.py:29
  57.6 14.4 %collective-permute-start.11 = (bf16[256,512]{1,0:T(8,128)(2,1)S(1)}, bf16[256,512]{1,0:T(8,128)(2,1)S(1)}, u32[]{:S(2)}, u32[]{:S(2)}) collective-permute-start(bf16[256,512]{1,0:T(8,128)(2,1)S(1)} %collective-permute-done.9.refs_7_), channel_id=1, source_target_pairs={{0,32},{32,64},{64,96},{96,128},{128,160},{160,192},{192,224},{224... | collective-permute-start | bytes 786440 | tf_op jit(solution)/shard_map/ppermute | solution.py:275
  60.4 14.9 %collective-permute-start.8 = (bf16[256,512]{1,0:T(8,128)(2,1)S(1)}, bf16[256,512]{1,0:T(8,128)(2,1)S(1)}, u32[]{:S(2)}, u32[]{:S(2)}) collective-permute-start(bf16[256,512]{1,0:T(8,128)(2,1)S(1)} %collective-permute-done.7.refs_5_), channel_id=1, source_target_pairs={{0,4},{4,0},{1,5},{5,1},{2,6},{6,2},{3,7},{7,3},{8,12},{12,8},{9,1... | collective-permute-start | bytes 786440 | tf_op jit(solution)/shard_map/ppermute | solution.py:33
  71.9 6.4 %collective-permute-start.13 = (bf16[128,512]{1,0:T(8,128)(2,1)S(1)}, bf16[128,512]{1,0:T(8,128)(2,1)S(1)}, u32[]{:S(2)}, u32[]{:S(2)}) collective-permute-start(bf16[128,512]{1,0:T(8,128)(2,1)S(1)} %slice.191), channel_id=1, source_target_pairs={{0,32},{32,64},{64,96},{96,128},{128,160},{160,192},{192,224},{224... | collective-permute-start | bytes 393224 | tf_op jit(solution)/shard_map/ppermute | solution.py:275
  74.6 9.0 %collective-permute-start.10 = (bf16[256,512]{1,0:T(8,128)(2,1)S(1)}, bf16[256,512]{1,0:T(8,128)(2,1)S(1)}, u32[]{:S(2)}, u32[]{:S(2)}) collective-permute-start(bf16[256,512]{1,0:T(8,128)(2,1)S(1)} %collective-permute-done.9.refs_7_), channel_id=1, source_target_pairs={{0,4},{4,0},{1,5},{5,1},{2,6},{6,2},{3,7},{7,3},{8,12},{12,8},{9,1... | collective-permute-start | bytes 786440 | tf_op jit(solution)/shard_map/ppermute | solution.py:33
  75.3 8.4 %collective-permute-start.12 = (bf16[256,512]{1,0:T(8,128)(2,1)S(1)}, bf16[256,512]{1,0:T(8,128)(2,1)S(1)}, u32[]{:S(2)}, u32[]{:S(2)}) collective-permute-start(bf16[256,512]{1,0:T(8,128)(2,1)S(1)} %collective-permute-done.11.refs_9_), channel_id=1, source_target_pairs={{0,4},{4,0},{1,5},{5,1},{2,6},{6,2},{3,7},{7,3},{8,12},{12,8},{9,1... | collective-permute-start | bytes 786440 | tf_op jit(solution)/shard_map/ppermute | solution.py:33
  78.3 5.3 %collective-permute-start.14 = (bf16[128,512]{1,0:T(8,128)(2,1)S(1)}, bf16[128,512]{1,0:T(8,128)(2,1)S(1)}, u32[]{:S(2)}, u32[]{:S(2)}) collective-permute-start(bf16[128,512]{1,0:T(8,128)(2,1)S(1)} %collective-permute-done.13.refs_11_), channel_id=1, source_target_pairs={{0,4},{4,0},{1,5},{5,1},{2,6},{6,2},{3,7},{7,3},{8,12},{12,8},{9,1... | collective-permute-start | bytes 393224 | tf_op jit(solution)/shard_map/ppermute | solution.py:33
  80.2 32.4 %collective-permute-start.26 = (bf16[768,384]{1,0:T(8,128)(2,1)}, bf16[768,384]{1,0:T(8,128)(2,1)}, u32[]{:S(2)}, u32[]{:S(2)}) collective-permute-start(bf16[768,384]{1,0:T(8,128)(2,1)} %collective-permute-done.24.refs_3_), channel_id=1, source_target_pairs={{0,32},{32,64},{64,96},{96,128},{128,160},{160,192},{192,224},{224... | collective-permute-start | bytes 1769480 | tf_op jit(solution)/shard_map/ppermute | solution.py:29
  82.5 34.3 %collective-permute-start.27 = (bf16[768,384]{1,0:T(8,128)(2,1)}, bf16[768,384]{1,0:T(8,128)(2,1)}, u32[]{:S(2)}, u32[]{:S(2)}) collective-permute-start(bf16[768,384]{1,0:T(8,128)(2,1)} %collective-permute-done.25.refs_4_), channel_id=1, source_target_pairs={{0,224},{32,0},{64,32},{96,64},{128,96},{160,128},{192,160},{224,1... | collective-permute-start | bytes 1769480 | tf_op jit(solution)/shard_map/ppermute | solution.py:29
  90.9 6.5 %collective-permute-start.16 = (bf16[144,256]{1,0:T(8,128)(2,1)}, bf16[144,256]{1,0:T(8,128)(2,1)}, u32[]{:S(2)}, u32[]{:S(2)}) collective-permute-start(bf16[144,256]{1,0:T(8,128)(2,1)} %get-tuple-element.15), channel_id=1, source_target_pairs={{0,16},{8,24},{16,0},{24,8},{1,17},{9,25},{17,1},{25,9},{2,18},{10... | collective-permute-start | bytes 221192 | tf_op jit(solution)/shard_map/ppermute | solution.py:29
  91.6 6.5 %collective-permute-start.17 = (bf16[144,256]{1,0:T(8,128)(2,1)}, bf16[144,256]{1,0:T(8,128)(2,1)}, u32[]{:S(2)}, u32[]{:S(2)}) collective-permute-start(bf16[144,256]{1,0:T(8,128)(2,1)} %get-tuple-element.16), channel_id=1, source_target_pairs={{0,8},{8,16},{16,24},{24,0},{1,9},{9,17},{17,25},{25,1},{2,10},{10... | collective-permute-start | bytes 221192 | tf_op jit(solution)/shard_map/ppermute | solution.py:29
  100.3 5.2 %collective-permute-start.18 = (bf16[144,256]{1,0:T(8,128)(2,1)S(1)}, bf16[144,256]{1,0:T(8,128)(2,1)S(1)}, u32[]{:S(2)}, u32[]{:S(2)}) collective-permute-start(bf16[144,256]{1,0:T(8,128)(2,1)S(1)} %join.1.refs_0_), channel_id=1, source_target_pairs={{0,3},{1,0},{2,1},{3,2},{4,7},{5,4},{6,5},{7,6},{8,11},{9,8},{10,9... | collective-permute-start | bytes 221192 | tf_op jit(solution)/shard_map/ppermute | solution.py:29
  103.2 5.9 %collective-permute-start.19 = (bf16[144,256]{1,0:T(8,128)(2,1)S(1)}, bf16[144,256]{1,0:T(8,128)(2,1)S(1)}, u32[]{:S(2)}, u32[]{:S(2)}) collective-permute-start(bf16[144,256]{1,0:T(8,128)(2,1)S(1)} %join.1.refs_0_), channel_id=1, source_target_pairs={{0,2},{1,3},{2,0},{3,1},{4,6},{5,7},{6,4},{7,5},{8,10},{9,11},{10,... | collective-permute-start | bytes 221192 | tf_op jit(solution)/shard_map/ppermute | solution.py:29
  104.0 5.8 %collective-permute-start.20 = (bf16[144,256]{1,0:T(8,128)(2,1)S(1)}, bf16[144,256]{1,0:T(8,128)(2,1)S(1)}, u32[]{:S(2)}, u32[]{:S(2)}) collective-permute-start(bf16[144,256]{1,0:T(8,128)(2,1)S(1)} %join.1.refs_0_), channel_id=1, source_target_pairs={{0,1},{1,2},{2,3},{3,0},{4,5},{5,6},{6,7},{7,4},{8,9},{9,10},{10,1... | collective-permute-start | bytes 221192 | tf_op jit(solution)/shard_map/ppermute | solution.py:29
  112.5 16.0 %collective-permute-start.21 = (bf16[144,2048]{1,0:T(8,128)(2,1)S(1)}, bf16[144,2048]{1,0:T(8,128)(2,1)S(1)}, u32[]{:S(2)}, u32[]{:S(2)}) collective-permute-start(bf16[144,2048]{1,0:T(8,128)(2,1)S(1)} %get-tuple-element.18.own), channel_id=1, source_target_pairs={{0,4},{4,0},{1,5},{5,1},{2,6},{6,2},{3,7},{7,3},{8,12},{12,8},{9,1... | collective-permute-start | bytes 1769480 | tf_op jit(solution)/shard_map/ppermute | solution.py:33
  113.7 10.2 %collective-permute-start.28 = (bf16[384,384]{1,0:T(8,128)(2,1)S(1)}, bf16[384,384]{1,0:T(8,128)(2,1)S(1)}, u32[]{:S(2)}, u32[]{:S(2)}) collective-permute-start(bf16[384,384]{1,0:T(8,128)(2,1)S(1)} %slice.195), channel_id=1, source_target_pairs={{0,32},{32,64},{64,96},{96,128},{128,160},{160,192},{192,224},{224... | collective-permute-start | bytes 884744 | tf_op jit(solution)/shard_map/ppermute | solution.py:29
  117.7 10.6 %collective-permute-start.29 = (bf16[384,384]{1,0:T(8,128)(2,1)S(1)}, bf16[384,384]{1,0:T(8,128)(2,1)S(1)}, u32[]{:S(2)}, u32[]{:S(2)}) collective-permute-start(bf16[384,384]{1,0:T(8,128)(2,1)S(1)} %slice.196), channel_id=1, source_target_pairs={{0,224},{32,0},{64,32},{96,64},{128,96},{160,128},{192,160},{224,1... | collective-permute-start | bytes 884744 | tf_op jit(solution)/shard_map/ppermute | solution.py:29
  134.7 9.6 %collective-permute-start.31 = (bf16[32,2048]{1,0:T(8,128)(2,1)S(1)}, bf16[32,2048]{1,0:T(8,128)(2,1)S(1)}, u32[]{:S(2)}, u32[]{:S(2)}) collective-permute-start(bf16[32,2048]{1,0:T(8,128)(2,1)S(1)} %get-tuple-element.23), channel_id=1, source_target_pairs={{0,1},{1,2},{2,3},{3,0},{4,5},{5,6},{6,7},{7,4},{8,9},{9,10},{10,1... | collective-permute-start | bytes 393224 | tf_op jit(solution)/shard_map/ppermute | solution.py:29
  134.8 9.5 %collective-permute-start.32 = (bf16[32,2048]{1,0:T(8,128)(2,1)S(1)}, bf16[32,2048]{1,0:T(8,128)(2,1)S(1)}, u32[]{:S(2)}, u32[]{:S(2)}) collective-permute-start(bf16[32,2048]{1,0:T(8,128)(2,1)S(1)} %get-tuple-element.25), channel_id=1, source_target_pairs={{0,2},{1,3},{2,0},{3,1},{4,6},{5,7},{6,4},{7,5},{8,10},{9,11},{10,... | collective-permute-start | bytes 393224 | tf_op jit(solution)/shard_map/ppermute | solution.py:29
  136.8 8.2 %collective-permute-start.33 = (bf16[32,2048]{1,0:T(8,128)(2,1)S(1)}, bf16[32,2048]{1,0:T(8,128)(2,1)S(1)}, u32[]{:S(2)}, u32[]{:S(2)}) collective-permute-start(bf16[32,2048]{1,0:T(8,128)(2,1)S(1)} %get-tuple-element.24), channel_id=1, source_target_pairs={{0,3},{1,0},{2,1},{3,2},{4,7},{5,4},{6,5},{7,6},{8,11},{9,8},{10,9... | collective-permute-start | bytes 393224 | tf_op jit(solution)/shard_map/ppermute | solution.py:29
  (23 other events, 288.1 us)
where the time goes:
time: 148 us; the launch traced here: 146 us
  waiting for transfers between devices  74.4 us (50%)
  starting transfers between devices  40.9 us (28%)
  local copies, waits for them, and re-layouts  15.6 us (11%)
  Pallas kernels  12.2 us (8%)
  other arithmetic  1.73 us (1%)
    ppermute x20, waiting for transfers between devices, shift(): return lax.ppermute(x, axis, [(i, (i + k) % n) for i in range(n)])  40.7 us
    ppermute x4, waiting for transfers between devices, step(): return lax.ppermute(v, ('z', 'c'), ring)  29.2 us
    ppermute x20, starting transfers between devices, shift(): return lax.ppermute(x, axis, [(i, (i + k) % n) for i in range(n)])  23.4 us
    ppermute x4, starting transfers between devices, step(): return lax.ppermute(v, ('z', 'c'), ring)  9.39 us
    unnamed x59, local copies, waits for them, and re-layouts  7.01 us
    pallas_call x1, Pallas kernels, attend(): pl.pallas_call(functools.partial(attend_kernel, nq, nk), out_shape=[jax.S...  5.25 us
    ppermute x1, starting transfers between devices, body(): edge = lax.ppermute(edge, SP, pairs)  4.48 us
    pallas_call x1, Pallas kernels, mixer(): pl.pallas_call(mixer_kernel, in_specs=[pl.BlockSpec(memory_space=pltpu.SM...  3.98 us
  transfers between devices with their start and end apart: 34, of which 17 were waited for; matrix products, arithmetic and copies ran while one was open for 7% of the time, Pallas kernels for 6%

commit v1 on v0

--- a/solution.py
+++ b/solution.py
@@ -15,6 +15,7 @@
 SP = ("z", "y", "c")
 SP_TP = ("z", "y", "c", "x")
 LOG2E = 1.4426950408889634
+MSG = 352
 ROWS = 144
 BF = jnp.bfloat16
 F32 = jnp.float32
@@ -36,18 +37,166 @@
 def tables(positions, width):
     half_width = width // 2
     frequency = 10000.0 ** (-jnp.arange(half_width, dtype=F32) / half_width)
-    angles = positions.astype(F32)[:, None] * frequency[None, :]
+    angles = positions.astype(F32)[None, :] * frequency[:, None]
     return (jnp.cos(angles), jnp.sin(angles))
 
 
-def rotate(vectors, cos_table, sine_table):
-    half_width = vectors.shape[-1] // 2
-    a = vectors[:, :half_width].astype(F32)
-    b = vectors[:, half_width:].astype(F32)
-    turned = jnp.concatenate(
-        [a * cos_table - b * sine_table, b * cos_table + a * sine_table], axis=1
-    )
-    return turned.astype(BF)
+def turn(a, b, cos, sin):
+    return [a * cos - b * sin, b * cos + a * sin]
+
+
+VM = pl.BlockSpec(memory_space=pltpu.VMEM)
+SM = pl.BlockSpec(memory_space=pltpu.SMEM)
+
+
+def pack_kernel(lat, down, key, out):
+    out[0:128, :] = lat[...]
+    out[128:160, :] = down[:, 0:512]
+    out[160:176, 0:256] = down[0:16, 512:768]
+    out[160:176, 256:512] = down[16:32, 512:768]
+    for i in range(4):
+        out[176:192, 128 * i : 128 * i + 128] = key[16 * i : 16 * i + 16, :]
+
+
+def pack(lat, down, key):
+    return pl.pallas_call(
+        pack_kernel,
+        in_specs=[VM] * 3,
+        out_shape=jax.ShapeDtypeStruct((192, 512), BF),
+        name="pack",
+        compiler_params=limit(4),
+    )(lat, down, key)
+
+
+def expand_kernel(own, other, weight, cos, sin, out):
+    lane = lax.broadcasted_iota(jnp.int32, (128, 128), 1)
+    tail = jnp.where(lane == 64, 1.0, 0.0)
+    for m, kv, down, at in ((own, 0, 128, 0), (other, 224, 176, 128)):
+        e = jnp.dot(m[0:128, :], weight[...], preferred_element_type=F32).astype(BF)
+        key = [m[176:192, 128 * i : 128 * i + 128].astype(F32) for i in range(4)]
+        a, b = jnp.concatenate(key[:2], axis=0), jnp.concatenate(key[2:], axis=0)
+        turned = turn(a, b, cos[:, at : at + 128], sin[:, at : at + 128])
+        turned = jnp.concatenate(turned + [jnp.zeros((64, 128), F32)], axis=0).T
+        narrow = pltpu.roll(e[:, 256:384].astype(F32), 64, 1)
+        rows = slice(kv, kv + 128)
+        out[rows, 0:128] = e[:, 0:128]
+        out[rows, 128:256] = jnp.where(lane < 64, turned, narrow).astype(BF)
+        out[rows, 256:384] = e[:, 128:256]
+        out[rows, 384:512] = jnp.where(lane < 64, narrow, tail).astype(BF)
+        out[down : down + 48, :] = m[128:176, :]
+
+
+def expand(own, other, weight, cos, sin):
+    return pl.pallas_call(
+        expand_kernel,
+        in_specs=[VM] * 5,
+        out_shape=jax.ShapeDtypeStruct((MSG, 512), BF),
+        name="expand",
+        compiler_params=limit(6),
+    )(own, other, weight, cos, sin)
+
+
+def queries_kernel(meta, q, cos, sin, gate, value, out, edge, keep, send):
+    c = meta[3]
+    f = q[...].astype(F32)
+    co, si = cos[:, 0:128], sin[:, 0:128]
+    wide = turn(f[192:224], f[224:256], co, si) + [jnp.zeros((64, 128), F32)]
+    narrow = turn(f[256:288], f[288:320], co, si) + [f[128:192]]
+    tiles = [f[0:128].T, jnp.concatenate(wide, axis=0).T, jnp.concatenate(narrow, axis=0).T]
+    row = lax.broadcasted_iota(jnp.int32, (128, 128), 0)
+    for i, tile in enumerate(tiles):
+        at = slice(128 * i, 128 * i + 128)
+        out[:, at] = tile.astype(BF)
+        line = jnp.sum(jnp.where(row == 127 * c, tile, 0.0), axis=0, keepdims=True)
+        edge[:, at] = line.astype(BF)
+
+    def halves(mine, others):
+        for i, m in enumerate((gate, value)):
+            keep[32 * i : 32 * i + 32, :] = m[:, mine]
+            send[32 * i : 32 * i + 32, :] = m[:, others]
+
+    pl.when(c == 0)(lambda: halves(slice(0, 384), slice(384, 768)))
+    pl.when(c == 1)(lambda: halves(slice(384, 768), slice(0, 384)))
+
+
+def turned_queries(meta, q, cos, sin, gate, value):
+    return pl.pallas_call(
+        queries_kernel,
+        in_specs=[SM] + [VM] * 5,
+        out_shape=[
+            jax.ShapeDtypeStruct((128, 384), BF),
+            jax.ShapeDtypeStruct((1, 384), BF),
+            jax.ShapeDtypeStruct((64, 384), BF),
+            jax.ShapeDtypeStruct((64, 384), BF),
+        ],
+        name="queries",
+        compiler_params=limit(6),
+    )(meta, q, cos, sin, gate, value)
+
+
+def lay_kernel(meta, q, edge, keep, got, out):
+    c = meta[3]
+    out[0:128, :] = q[...]
+    row = lax.broadcasted_iota(jnp.int32, (16, 384), 0)
+    out[128:144, :] = jnp.where(row == 0, edge[...].astype(F32), 0.0).astype(BF)
+    for i in range(2):
+        at = ROWS + 64 * i
+        rows = slice(32 * i, 32 * i + 32)
+        out[pl.ds(pl.multiple_of(at + 32 * c, 16), 32), :] = keep[rows, :]
+        out[pl.ds(pl.multiple_of(at + 32 - 32 * c, 16), 32), :] = got[rows, :]
+
+
+def lay(meta, q, edge, keep, got):
+    return pl.pallas_call(
+        lay_kernel,
+        in_specs=[SM] + [VM] * 4,
+        out_shape=jax.ShapeDtypeStruct((ROWS + 128, 384), BF),
+        name="lay",
+        compiler_params=limit(4),
+    )(meta, q, edge, keep, got)
+
+
+def lay_down_kernel(meta, *refs):
+    parts, out = refs[:-1], refs[-1]
+    z, c = meta[2], meta[3]
+
+    def lay_all(mine):
+        def put(ref, at, zz, core):
+            first = lax.rem(zz + 2 * Z, Z) * 64 + 32 * core
+            top = pl.ds(pl.multiple_of(first, 16), 16)
+            low = pl.ds(pl.multiple_of(first + 16, 16), 16)
+            if mine == 0:
+                out[top, :] = ref[at : at + 16, 0:384]
+                out[low, :] = ref[at + 16 : at + 32, 0:384]
+            else:
+                out[top, 0:128] = ref[at : at + 16, 384:512]
+                out[low, 0:128] = ref[at + 16 : at + 32, 384:512]
+                out[top, 128:384] = ref[at + 32 : at + 48, 0:256]
+                out[low, 128:384] = ref[at + 32 : at + 48, 256:512]
+
+        sign = 2 * mine - 1
+        put(parts[0], 128, z, mine)
+        put(parts[0], 176, z, 1 - mine)
+        for k in (1, 2, 3):
+            put(parts[k], 128, z + sign * k, mine)
+            put(parts[k], 176, z + sign * k, 1 - mine)
+            put(parts[4 + k], 128, z - sign * k, 1 - mine)
+            put(parts[4 + k], 176, z - sign * k, mine)
+        put(parts[4], 128, z + 4, mine)
+        put(parts[8], 128, z + 4, 1 - mine)
+
+    pl.when(c == 0)(lambda: lay_all(0))
+    pl.when(c == 1)(lambda: lay_all(1))
+
+
+def lay_down(meta, parts):
+    return pl.pallas_call(
+        lay_down_kernel,
+        in_specs=[SM] + [VM] * len(parts),
+        out_shape=jax.ShapeDtypeStruct((512, 384), BF),
+        name="lay_down",
+        compiler_params=limit(4),
+    )(meta, *parts)
 
 
 def split3(v):
@@ -60,18 +209,19 @@
 
 def attend_kernel(nq, nk, *refs):
     qs, ks, outs = refs[:nq], refs[nq : nq + nk], refs[nq + nk :]
-    keys = jnp.concatenate([k[:, 0:256] for k in ks], axis=0)
-    values = jnp.concatenate([k[:, 256:512] for k in ks], axis=0)
+    spans = [(k, at) for k in ks for at in ((0, 224) if k.shape[0] == MSG else (0,))]
+    keys = jnp.concatenate([k[at : at + 128, 0:256] for k, at in spans], axis=0)
+    values = jnp.concatenate([k[at : at + 128, 256:512] for k, at in spans], axis=0)
     cw = float((NOPE_A + ROPE) ** -0.5 * LOG2E)
     cn = float((NOPE_B + ROPE) ** -0.5 * LOG2E)
     nt = (((1,), (1,)), ((), ()))
     lane = lax.broadcasted_iota(jnp.int32, (ROWS, 128), 1)
     for q, o in zip(qs, outs):
-        sw = lax.dot_general(q[:, 0:256], keys, nt, preferred_element_type=F32)
+        sw = lax.dot_general(q[0:ROWS, 0:256], keys, nt, preferred_element_type=F32)
         mw = jnp.max(sw, axis=1, keepdims=True)
         pw = jnp.exp2((sw - mw) * cw).astype(BF)
         ow = jnp.dot(pw, values, preferred_element_type=F32)
-        sn = lax.dot_general(q[:, 256:384], keys[:, 128:256], nt, preferred_element_type=F32)
+        sn = lax.dot_general(q[0:ROWS, 256:384], keys[:, 128:256], nt, preferred_element_type=F32)
         mn = jnp.max(sn, axis=1, keepdims=True)
         pn = jnp.exp2((sn - mn) * cn).astype(BF)
         on = jnp.dot(pn, values[:, 128:256], preferred_element_type=F32)
@@ -157,15 +307,22 @@
 
 
 def mixer_kernel(meta, own, other, taps, *refs):
-    parts, (keep, send, gates, values, downs) = refs[:-5], refs[-5:]
+    n = len(OFFSETS)
+    parts, lower, (keep, send, gates, values, downs) = refs[:n], refs[n:-5], refs[-5:]
     z, c, y = meta[2], meta[3], meta[4]
+
+    def place(zz, dy):
+        at = (lax.rem(zz, Z) * Y + lax.rem(y + dy, Y)) * 64
+        return pl.ds(pl.multiple_of(at, 64), 64)
+
     for part, off in zip(parts, OFFSETS):
         for k in range(Y):
-            at = (lax.rem(z + off, Z) * Y + lax.rem(y + k, Y)) * 64
-            rows = pl.ds(pl.multiple_of(at, 64), 64)
-            for m, to in enumerate((gates, values, downs)):
-                first = k * 192 + m * 64
-                to[rows, :] = part[first : first + 64, :]
+            rows = place(z + off, k)
+            gates[rows, :] = part[128 * k : 128 * k + 64, :]
+            values[rows, :] = part[128 * k + 64 : 128 * k + 128, :]
+    for part, (dy, first) in zip(lower, ((0, 0), (1, 0), (2, 0), (2, 4), (3, 0))):
+        for i in range(part.shape[0] // 64):
+            downs[place(first + i, dy), :] = part[64 * i : 64 * i + 64, :]
     both = jnp.concatenate([own[...], other[...]], axis=0)
     gate = jnp.dot(both, gates[...], preferred_element_type=F32).astype(BF).astype(F32)
     value = jnp.dot(both, values[...], preferred_element_type=F32).astype(BF).astype(F32)
@@ -196,10 +353,9 @@
 
 
 def mixer(meta, own, other, taps, parts):
-    vmem = pl.BlockSpec(memory_space=pltpu.VMEM)
     return pl.pallas_call(
         mixer_kernel,
-        in_specs=[pl.BlockSpec(memory_space=pltpu.SMEM)] + [vmem] * (3 + len(parts)),
+        in_specs=[SM] + [VM] * (3 + len(parts)),
         out_shape=[
             jax.ShapeDtypeStruct((128, 2048), F32),
             jax.ShapeDtypeStruct((128, 2048), BF),
@@ -226,82 +382,51 @@
     z, y, c, x = (lax.axis_index(a) for a in ("z", "y", "c", "x"))
     s = lax.axis_index(SP)
     tok = queries.shape[0]
-    lat2 = jnp.concatenate([latents, swap(latents)], axis=0)
-    sk2 = jnp.concatenate([shared_key, swap(shared_key)], axis=0)
+    nsp = Z * Y * C
+    valid = jnp.where(c == 0, s > 0, s < nsp - 1).astype(jnp.int32)
+    meta = jnp.stack([x, valid, z, c, y]).astype(jnp.int32)
     own_pos = s * tok + jnp.arange(tok, dtype=jnp.int32)
     other_pos = (s + 1 - 2 * c) * tok + jnp.arange(tok, dtype=jnp.int32)
-    cos2, sin2 = tables(jnp.concatenate([own_pos, other_pos]), ROPE)
-    cos, sin = cos2[:tok], sin2[:tok]
-    ew = expand_weight
-    expanded = jnp.dot(lat2, ew, preferred_element_type=F32).astype(BF)
-    turned = rotate(sk2, cos2, sin2)
-    ones = jnp.broadcast_to(
-        (jnp.arange(64) == 0).astype(BF)[None, :], (2 * tok, 64)
-    )
-    kv = jnp.concatenate(
-        [
-            expanded[:, 0:128],
-            turned,
-            expanded[:, 256:320],
-            expanded[:, 128:256],
-            expanded[:, 320:384],
-            ones,
-        ],
-        axis=1,
-    )
-    rot0 = NOPE_A + NOPE_B
-    q = jnp.concatenate(
-        [
-            queries[:, 0:128],
-            rotate(queries[:, rot0 : rot0 + 64], cos, sin),
-            jnp.zeros((tok, 64), BF),
-            rotate(queries[:, rot0 + 64 : rot0 + 128], cos, sin),
-            queries[:, 128:192],
-        ],
-        axis=1,
-    )
-    nsp = Z * Y * C
-    pairs = [(i, i + 1) for i in range(1, nsp - 1, 2)] + [(i, i - 1) for i in range(2, nsp, 2)]
-    edge = jnp.concatenate([q, residual], axis=1)
-    edge = jnp.where(c == 1, edge[tok - 1 : tok], edge[0:1])
-    edge = lax.ppermute(edge, SP, pairs)
-    edge = jnp.pad(edge, ((0, 15), (0, 0)))
-    q = jnp.concatenate([q, edge[:, :384]], axis=0)
-    halo_res = edge[:, 384:]
+    cos, sin = tables(jnp.concatenate([own_pos, other_pos]), ROPE)
     ring = [(2 * i, 2 * ((i + 1) % Z)) for i in range(Z)]
     ring += [(2 * i + 1, 2 * ((i - 1) % Z) + 1) for i in range(Z)]
 
     def step(v):
         return lax.ppermute(v, ("z", "c"), ring)
 
-    r1 = step(kv)
-    mats = (gate_weight, value_weight, down_weight.T)
-    lo = jnp.concatenate([m[:, :384] for m in mats], axis=0)
-    hi = jnp.concatenate([m[:, 384:] for m in mats], axis=0)
-    wk = jnp.where(c == 0, lo, hi)
-    wr = swap(jnp.where(c == 0, hi, lo))
-    wa, wb = jnp.where(c == 0, wk, wr), jnp.where(c == 0, wr, wk)
-    w = jnp.concatenate([v[32 * m : 32 * m + 32] for m in range(3) for v in (wa, wb)], axis=0)
-    qw = jnp.concatenate([q, w], axis=0)
-    got = [qw] + [shift(qw, "y", k) for k in (1, 2, 3)]
-    q_blocks = [v[:ROWS] for v in got]
-    w = jnp.concatenate([got[-k % Y][ROWS:] for k in range(Y)], axis=0)
+    packed = pack(latents, down_weight.T, shared_key.T)
+    m0 = expand(packed, swap(packed), expand_weight, cos, sin)
+    r1 = step(m0)
+    q, edge, keep, send = turned_queries(meta, queries.T, cos, sin, gate_weight, value_weight)
+    got = swap(send)
+    pairs = [(i, i + 1) for i in range(1, nsp - 1, 2)] + [(i, i - 1) for i in range(2, nsp, 2)]
+    line = lax.dynamic_slice_in_dim(residual, c * (tok - 1), 1, 0)
+    edge = jnp.concatenate([edge, line], axis=1)
+    edge = lax.ppermute(edge, SP, pairs)
+    halo_res = jnp.pad(edge[:, 384:], ((0, 15), (0, 0)))
+    qw = lay(meta, q, edge[:, :384], keep, got)
+    y1, y3 = shift(qw, "y", 1), shift(qw, "y", -1)
     r2 = step(r1)
     r3 = step(r2)
-    r4 = step(r3[:tok])
-    k_blocks = [kv, r1, swap(r1), r2, swap(r2), r3, swap(r3)]
-    k_blocks += [r4, swap(r4)]
+    q2 = shift(y1[:ROWS], "y", 1)
+    w2 = shift(y3[ROWS:], "y", -1)
+    r4 = step(r3[:176])
+    q_blocks = [qw, y1, q2, y3]
+    w = jnp.concatenate([qw[ROWS:], y3[ROWS:], w2, y1[ROWS:]], axis=0)
+    messages = [m0, r1, r2, r3, r4]
+    messages += [swap(v) for k, v in enumerate(messages) if k > 0]
     f1, b1 = shift(w, "z", 1), shift(w, "z", -1)
     f2, b2 = shift(f1, "z", 1), shift(b1, "z", -1)
     f3, b3 = shift(f2, "z", 1), shift(b2, "z", -1)
-    o4 = jnp.concatenate([shift(f3[:384], "z", 1), shift(b3[384:], "z", -1)], axis=0)
-    ws = [w, f1, b1, f2, b2, f3, b3, o4]
-    o = attend(q_blocks, k_blocks)
+    o4 = jnp.concatenate([shift(f3[:256], "z", 1), shift(b3[256:], "z", -1)], axis=0)
+    d0 = lay_down(meta, messages)
+    d1, d3 = shift(d0, "y", 1), shift(d0, "y", -1)
+    da, db = shift(d1[:256], "y", 1), shift(d3[256:], "y", -1)
+    ws = [w, f1, b1, f2, b2, f3, b3, o4, d0, d3, da, db, d1]
+    o = attend(q_blocks, messages)
     parts = [o[0]] + [shift(o[k], "y", -k) for k in (1, 2, 3)]
     attended = join(parts)
     heads = [attended] + [shift(attended, "x", -k) for k in (1, 2, 3)]
-    valid = jnp.where(c == 0, s > 0, s < nsp - 1).astype(jnp.int32)
-    meta = jnp.stack([x, valid, z, c, y]).astype(jnp.int32)
     stream_own, normed = project(
         meta, heads, out_weight, residual, halo_res, norm_gain.reshape(1, -1)
     )

time: 148 us -> 120 us (0.81)
  the two profiles are of different devices: /device:TPU:32 before, /device:TPU:120 now
where the time goes in v1:
time: 120 us; the launch traced here: 119 us
  starting transfers between devices  53 us (44%)
  waiting for transfers between devices  45.8 us (38%)
  Pallas kernels  12 us (10%)
  local copies, waits for them, and re-layouts  6.98 us (6%)
  other arithmetic  1.21 us (1%)
    ppermute x25, starting transfers between devices, shift(): return lax.ppermute(x, axis, [(i, (i + k) % n) for i in range(n)])  34.2 us
    ppermute x25, waiting for transfers between devices, shift(): return lax.ppermute(x, axis, [(i, (i + k) % n) for i in range(n)])  33.8 us
    ppermute x4, starting transfers between devices, step(): return lax.ppermute(v, ('z', 'c'), ring)  11.7 us
    unnamed x22, local copies, waits for them, and re-layouts  5.92 us
    ppermute x4, waiting for transfers between devices, step(): return lax.ppermute(v, ('z', 'c'), ring)  5.66 us
    ppermute x8, starting transfers between devices, swap(): return lax.ppermute(x, 'c', [(0, 1), (1, 0)])  5.16 us
    pallas_call x1, Pallas kernels, attend(): pl.pallas_call(functools.partial(attend_kernel, nq, nk), out_shape=[jax.S...  4.69 us
    ppermute x8, waiting for transfers between devices, swap(): return lax.ppermute(x, 'c', [(0, 1), (1, 0)])  3.23 us
  transfers between devices with their start and end apart: 38, of which 17 were waited for; matrix products, arithmetic and copies ran while one was open for 1% of the time, Pallas kernels for 7%

profile of v1, /device:TPU:120, one launch (start us, length us, event | category | flops | bytes accessed | tf_op | source)
XLA Modules:
  0.0 119.4 jit_solution(3280891471474520048)
XLA Ops:
  9.1 3.2 %collective-permute-start.6 = (bf16[352,512]{1,0:T(8,128)(2,1)S(1)}, bf16[352,512]{1,0:T(8,128)(2,1)S(1)}, u32[]{:S(2)}, u32[]{:S(2)}) collective-permute-start(bf16[352,512]{1,0:T(8,128)(2,1)S(1)} %expand.1.refs_4_.refs_0_), channel_id=1, source_target_pairs={{0,32},{32,64},{64,96},{96,128},{128,160},{160,192},{192,224},{224... | collective-permute-start | bytes 1081352 | tf_op jit(solution)/shard_map/ppermute | solution.py:395
  12.3 1.9 %collective-permute-start = (bf16[1,2432]{1,0:T(2,128)(2,1)S(1)}, bf16[1,2432]{1,0:T(2,128)(2,1)S(1)}, u32[]{:S(2)}, u32[]{:S(2)}) collective-permute-start(bf16[1,2432]{1,0:T(2,128)(2,1)S(1)} %pad_maximum_fusion.2), channel_id=1, source_target_pairs={{4,8},{12,16},{20,24},{28,32},{36,40},{44,48},{52,56},{60,64},{68,... | collective-permute-start | bytes 14600 | tf_op jit(solution)/shard_map/ppermute | solution.py:405
  14.2 3.1 %collective-permute-done = bf16[1,2432]{1,0:T(2,128)(2,1)S(1)} collective-permute-done((bf16[1,2432]{1,0:T(2,128)(2,1)S(1)}, bf16[1,2432]{1,0:T(2,128)(2,1)S(1)}, u32[]{:S(2)}, u32[]{:S(2)}) %collective-permute-start) | collective-permute-done | bytes 4896 | tf_op jit(solution)/shard_map/ppermute | solution.py:405
  18.7 2.5 %collective-permute-start.2 = (bf16[272,384]{1,0:T(8,128)(2,1)S(1)}, bf16[272,384]{1,0:T(8,128)(2,1)S(1)}, u32[]{:S(2)}, u32[]{:S(2)}) collective-permute-start(bf16[272,384]{1,0:T(8,128)(2,1)S(1)} %lay.1.refs_0_), channel_id=1, source_target_pairs={{0,8},{8,16},{16,24},{24,0},{1,9},{9,17},{17,25},{25,1},{2,10},{10... | collective-permute-start | bytes 626696 | tf_op jit(solution)/shard_map/ppermute | solution.py:30
  22.7 4.1 %collective-permute-done.4.refs_3_ = bf16[272,384]{1,0:T(8,128)(2,1)S(1)} collective-permute-done((bf16[272,384]{1,0:T(8,128)(2,1)S(1)}, bf16[272,384]{1,0:T(8,128)(2,1)S(1)}, u32[]{:S(2)}, u32[]{:S(2)}) %collective-permute-start.4) | collective-permute-done | bytes 208928 | tf_op jit(solution)/shard_map/ppermute | solution.py:30
  27.0 5.8 %collective-permute-done.21 = bf16[128,384]{1,0:T(8,128)(2,1)S(1)} collective-permute-done((bf16[128,384]{1,0:T(8,128)(2,1)S(1)}, bf16[128,384]{1,0:T(8,128)(2,1)S(1)}, u32[]{:S(2)}, u32[]{:S(2)}) %collective-permute-start.21) | collective-permute-done | bytes 98336 | tf_op jit(solution)/shard_map/ppermute | solution.py:30
  32.9 3.2 %collective-permute-start.8 = (bf16[352,512]{1,0:T(8,128)(2,1)S(1)}, bf16[352,512]{1,0:T(8,128)(2,1)S(1)}, u32[]{:S(2)}, u32[]{:S(2)}) collective-permute-start(bf16[352,512]{1,0:T(8,128)(2,1)S(1)} %collective-permute-done.7.refs_6_.refs_2_), channel_id=1, source_target_pairs={{0,32},{32,64},{64,96},{96,128},{128,160},{160,192},{192,224},{224... | collective-permute-start | bytes 1081352 | tf_op jit(solution)/shard_map/ppermute | solution.py:395
  37.0 5.7 %collective-permute-done.8.refs_7_.refs_3_ = bf16[352,512]{1,0:T(8,128)(2,1)S(1)} collective-permute-done((bf16[352,512]{1,0:T(8,128)(2,1)S(1)}, bf16[352,512]{1,0:T(8,128)(2,1)S(1)}, u32[]{:S(2)}, u32[]{:S(2)}) %collective-permute-start.8) | collective-permute-done | bytes 360480 | tf_op jit(solution)/shard_map/ppermute | solution.py:395
  42.7 3.8 %collective-permute-start.9 = (bf16[176,512]{1,0:T(8,128)(2,1)S(1)}, bf16[176,512]{1,0:T(8,128)(2,1)S(1)}, u32[]{:S(2)}, u32[]{:S(2)}) collective-permute-start(bf16[176,512]{1,0:T(8,128)(2,1)S(1)} %slice.55), channel_id=1, source_target_pairs={{0,32},{32,64},{64,96},{96,128},{128,160},{160,192},{192,224},{224... | collective-permute-start | bytes 540680 | tf_op jit(solution)/shard_map/ppermute | solution.py:395
  48.1 2.8 %collective-permute-start.24 = (bf16[512,384]{1,0:T(8,128)(2,1)S(1)}, bf16[512,384]{1,0:T(8,128)(2,1)S(1)}, u32[]{:S(2)}, u32[]{:S(2)}) collective-permute-start(bf16[512,384]{1,0:T(8,128)(2,1)S(1)} %collective-permute-done.22.refs_1_), channel_id=1, source_target_pairs={{0,32},{32,64},{64,96},{96,128},{128,160},{160,192},{192,224},{224... | collective-permute-start | bytes 1179656 | tf_op jit(solution)/shard_map/ppermute | solution.py:30
  50.9 3.1 %collective-permute-start.13 = (bf16[176,512]{1,0:T(8,128)(2,1)S(1)}, bf16[176,512]{1,0:T(8,128)(2,1)S(1)}, u32[]{:S(2)}, u32[]{:S(2)}) collective-permute-start(bf16[176,512]{1,0:T(8,128)(2,1)S(1)} %collective-permute-done.9.refs_8_.refs_4_), channel_id=1, source_target_pairs={{0,4},{4,0},{1,5},{5,1},{2,6},{6,2},{3,7},{7,3},{8,12},{12,8},{9,1... | collective-permute-start | bytes 540680 | tf_op jit(solution)/shard_map/ppermute | solution.py:34
  55.1 4.7 %attend.1 = (bf16[144,256]{1,0:T(8,128)(2,1)S(1)}, bf16[144,256]{1,0:T(8,128)(2,1)S(1)}, bf16[144,256]{1,0:T(8,128)(2,1)S(1)}, bf16[144,256]{1,0:T(8,128)(2,1)S(1)}) custom-call(bf16[272,384]{1,0:T(8,128)(2,1)S(1)} %lay.1.refs_0_, bf16[272,384]{1,0:T(8,128)(2,1)S(1)} %collective-permute-done.2.refs_1_, bf16[144,384]{1,0:T(8,128)(2,1)S(1)} %collective-permute-done.3.refs_2_, ...), custom_call_target="tpu_custom_call" | custom-call | tf_op jit(solution)/shard_map/attend/pallas_call | solution.py:240
  61.3 1.9 %collective-permute-start.16 = (bf16[144,256]{1,0:T(8,128)(2,1)S(1)}, bf16[144,256]{1,0:T(8,128)(2,1)S(1)}, u32[]{:S(2)}, u32[]{:S(2)}) collective-permute-start(bf16[144,256]{1,0:T(8,128)(2,1)S(1)} %get-tuple-element.24), channel_id=1, source_target_pairs={{0,8},{8,16},{16,24},{24,0},{1,9},{9,17},{17,25},{25,1},{2,10},{10... | collective-permute-start | bytes 221192 | tf_op jit(solution)/shard_map/ppermute | solution.py:30
  63.1 4.1 %collective-permute-done.14.refs_1_ = bf16[144,256]{1,0:T(8,128)(2,1)S(1)} collective-permute-done((bf16[144,256]{1,0:T(8,128)(2,1)S(1)}, bf16[144,256]{1,0:T(8,128)(2,1)S(1)}, u32[]{:S(2)}, u32[]{:S(2)}) %collective-permute-start.14) | collective-permute-done | bytes 73760 | tf_op jit(solution)/shard_map/ppermute | solution.py:30
  69.8 3.2 %collective-permute-start.26 = (bf16[512,384]{1,0:T(8,128)(2,1)S(1)}, bf16[512,384]{1,0:T(8,128)(2,1)S(1)}, u32[]{:S(2)}, u32[]{:S(2)}) collective-permute-start(bf16[512,384]{1,0:T(8,128)(2,1)S(1)} %collective-permute-done.24.refs_3_), channel_id=1, source_target_pairs={{0,32},{32,64},{64,96},{96,128},{128,160},{160,192},{192,224},{224... | collective-permute-start | bytes 1179656 | tf_op jit(solution)/shard_map/ppermute | solution.py:30
  73.7 2.5 %collective-permute-start.31 = (bf16[512,384]{1,0:T(8,128)(2,1)S(1)}, bf16[512,384]{1,0:T(8,128)(2,1)S(1)}, u32[]{:S(2)}, u32[]{:S(2)}) collective-permute-start(bf16[512,384]{1,0:T(8,128)(2,1)S(1)} %lay_down.1.refs_8_), channel_id=1, source_target_pairs={{0,8},{8,16},{16,24},{24,0},{1,9},{9,17},{17,25},{25,1},{2,10},{10... | collective-permute-start | bytes 1179656 | tf_op jit(solution)/shard_map/ppermute | solution.py:30
  76.2 2.7 %collective-permute-start.18 = (bf16[144,256]{1,0:T(8,128)(2,1)S(1)}, bf16[144,256]{1,0:T(8,128)(2,1)S(1)}, u32[]{:S(2)}, u32[]{:S(2)}) collective-permute-start(bf16[144,256]{1,0:T(8,128)(2,1)S(1)} %join.1.refs_0_), channel_id=1, source_target_pairs={{0,2},{1,3},{2,0},{3,1},{4,6},{5,7},{6,4},{7,5},{8,10},{9,11},{10,... | collective-permute-start | bytes 221192 | tf_op jit(solution)/shard_map/ppermute | solution.py:30
  78.9 3.1 %collective-permute-done.18.refs_2_ = bf16[144,256]{1,0:T(8,128)(2,1)S(1)} collective-permute-done((bf16[144,256]{1,0:T(8,128)(2,1)S(1)}, bf16[144,256]{1,0:T(8,128)(2,1)S(1)}, u32[]{:S(2)}, u32[]{:S(2)}) %collective-permute-start.18) | collective-permute-done | bytes 73760 | tf_op jit(solution)/shard_map/ppermute | solution.py:30
  82.0 1.7 %collective-permute-start.17 = (bf16[144,256]{1,0:T(8,128)(2,1)S(1)}, bf16[144,256]{1,0:T(8,128)(2,1)S(1)}, u32[]{:S(2)}, u32[]{:S(2)}) collective-permute-start(bf16[144,256]{1,0:T(8,128)(2,1)S(1)} %join.1.refs_0_), channel_id=1, source_target_pairs={{0,3},{1,0},{2,1},{3,2},{4,7},{5,4},{6,5},{7,6},{8,11},{9,8},{10,9... | collective-permute-start | bytes 221192 | tf_op jit(solution)/shard_map/ppermute | solution.py:30
  83.8 2.6 %collective-permute-done.17.refs_1_ = bf16[144,256]{1,0:T(8,128)(2,1)S(1)} collective-permute-done((bf16[144,256]{1,0:T(8,128)(2,1)S(1)}, bf16[144,256]{1,0:T(8,128)(2,1)S(1)}, u32[]{:S(2)}, u32[]{:S(2)}) %collective-permute-start.17) | collective-permute-done | bytes 73760 | tf_op jit(solution)/shard_map/ppermute | solution.py:30
  86.4 1.6 %project.1 = (bf16[32,2048]{1,0:T(8,128)(2,1)S(1)}, bf16[144,2048]{1,0:T(8,128)(2,1)S(1)}) custom-call(s32[5]{0:T(128)S(1)} %stack.27.meta, bf16[144,256]{1,0:T(8,128)(2,1)S(1)} %join.1.refs_0_, bf16[144,256]{1,0:T(8,128)(2,1)S(1)} %collective-permute-done.17.refs_1_, bf16[144,256]{1,0:T(8,128)(2,1)S(1)} %collective-permute-done.18.refs_2_, ...), custom_call_target="tpu_custom_call" | custom-call | tf_op jit(solution)/shard_map/project/pallas_call | solution.py:297
  88.2 3.3 %collective-permute-start.28 = (bf16[256,384]{1,0:T(8,128)(2,1)S(1)}, bf16[256,384]{1,0:T(8,128)(2,1)S(1)}, u32[]{:S(2)}, u32[]{:S(2)}) collective-permute-start(bf16[256,384]{1,0:T(8,128)(2,1)S(1)} %slice.60), channel_id=1, source_target_pairs={{0,32},{32,64},{64,96},{96,128},{128,160},{160,192},{192,224},{224... | collective-permute-start | bytes 589832 | tf_op jit(solution)/shard_map/ppermute | solution.py:30
  91.6 3.3 %collective-permute-start.32 = (bf16[256,384]{1,0:T(8,128)(2,1)S(1)}, bf16[256,384]{1,0:T(8,128)(2,1)S(1)}, u32[]{:S(2)}, u32[]{:S(2)}) collective-permute-start(bf16[256,384]{1,0:T(8,128)(2,1)S(1)} %slice.62), channel_id=1, source_target_pairs={{0,8},{8,16},{16,24},{24,0},{1,9},{9,17},{17,25},{25,1},{2,10},{10... | collective-permute-start | bytes 589832 | tf_op jit(solution)/shard_map/ppermute | solution.py:30
  95.0 1.7 %collective-permute-done.29 = bf16[256,384]{1,0:T(8,128)(2,1)S(1)} collective-permute-done((bf16[256,384]{1,0:T(8,128)(2,1)S(1)}, bf16[256,384]{1,0:T(8,128)(2,1)S(1)}, u32[]{:S(2)}, u32[]{:S(2)}) %collective-permute-start.29) | collective-permute-done | bytes 196640 | tf_op jit(solution)/shard_map/ppermute | solution.py:30
  96.7 2.4 %collective-permute-done.32.refs_10_ = bf16[256,384]{1,0:T(8,128)(2,1)S(1)} collective-permute-done((bf16[256,384]{1,0:T(8,128)(2,1)S(1)}, bf16[256,384]{1,0:T(8,128)(2,1)S(1)}, u32[]{:S(2)}, u32[]{:S(2)}) %collective-permute-start.32) | collective-permute-done | bytes 196640 | tf_op jit(solution)/shard_map/ppermute | solution.py:30
  99.1 3.5 %collective-permute-done.33.refs_11_ = bf16[256,384]{1,0:T(8,128)(2,1)S(1)} collective-permute-done((bf16[256,384]{1,0:T(8,128)(2,1)S(1)}, bf16[256,384]{1,0:T(8,128)(2,1)S(1)}, u32[]{:S(2)}, u32[]{:S(2)}) %collective-permute-start.33) | collective-permute-done | bytes 196640 | tf_op jit(solution)/shard_map/ppermute | solution.py:30
  102.6 3.0 %mixer.1 = (f32[128,2048]{1,0:T(8,128)S(1)}, bf16[128,2048]{1,0:T(8,128)(2,1)S(1)}) custom-call(s32[5]{0:T(128)S(1)} %stack.27.meta, bf16[144,2048]{1,0:T(8,128)(2,1)S(1)} %get-tuple-element.26.own, bf16[144,2048]{1,0:T(8,128)(2,1)S(1)} %collective-permute-done.20.other, bf16[3,384]{1,0:T(4,128)(2,1)S(1)} %slice_select_fusion.taps, ...), custom_call_target="tpu_custom_call" | custom-call | tf_op jit(solution)/shard_map/mixer/pallas_call | solution.py:356
  105.8 1.9 %collective-permute-done.34 = bf16[128,2048]{1,0:T(8,128)(2,1)S(1)} collective-permute-done((bf16[128,2048]{1,0:T(8,128)(2,1)S(1)}, bf16[128,2048]{1,0:T(8,128)(2,1)S(1)}, u32[]{:S(2)}, u32[]{:S(2)}) %collective-permute-start.34) | collective-permute-done | bytes 524320 | tf_op jit(solution)/shard_map/ppermute | solution.py:34
  109.4 1.7 %collective-permute-start.37 = (bf16[32,2048]{1,0:T(8,128)(2,1)S(1)}, bf16[32,2048]{1,0:T(8,128)(2,1)S(1)}, u32[]{:S(2)}, u32[]{:S(2)}) collective-permute-start(bf16[32,2048]{1,0:T(8,128)(2,1)S(1)} %get-tuple-element.32), channel_id=1, source_target_pairs={{0,3},{1,0},{2,1},{3,2},{4,7},{5,4},{6,5},{7,6},{8,11},{9,8},{10,9... | collective-permute-start | bytes 393224 | tf_op jit(solution)/shard_map/ppermute | solution.py:30
  112.7 2.0 %collective-permute-done.35 = bf16[32,2048]{1,0:T(8,128)(2,1)S(1)} collective-permute-done((bf16[32,2048]{1,0:T(8,128)(2,1)S(1)}, bf16[32,2048]{1,0:T(8,128)(2,1)S(1)}, u32[]{:S(2)}, u32[]{:S(2)}) %collective-permute-start.35) | collective-permute-done | bytes 131104 | tf_op jit(solution)/shard_map/ppermute | solution.py:30
  114.7 2.2 %collective-permute-done.37 = bf16[32,2048]{1,0:T(8,128)(2,1)S(1)} collective-permute-done((bf16[32,2048]{1,0:T(8,128)(2,1)S(1)}, bf16[32,2048]{1,0:T(8,128)(2,1)S(1)}, u32[]{:S(2)}, u32[]{:S(2)}) %collective-permute-start.37) | collective-permute-done | bytes 131104 | tf_op jit(solution)/shard_map/ppermute | solution.py:30
  116.9 1.8 %collective-permute-done.36 = bf16[32,2048]{1,0:T(8,128)(2,1)S(1)} collective-permute-done((bf16[32,2048]{1,0:T(8,128)(2,1)S(1)}, bf16[32,2048]{1,0:T(8,128)(2,1)S(1)}, u32[]{:S(2)}, u32[]{:S(2)}) %collective-permute-start.36) | collective-permute-done | bytes 131104 | tf_op jit(solution)/shard_map/ppermute | solution.py:30
  (101 shorter events, 25.0 us)
Async XLA Ops:
  3.5 13.8 %collective-permute-start.1 = (bf16[64,384]{1,0:T(8,128)(2,1)S(1)}, bf16[64,384]{1,0:T(8,128)(2,1)S(1)}, u32[]{:S(2)}, u32[]{:S(2)}) collective-permute-start(bf16[64,384]{1,0:T(8,128)(2,1)S(1)} %get-tuple-element.20), channel_id=1, source_target_pairs={{0,4},{4,0},{1,5},{5,1},{2,6},{6,2},{3,7},{7,3},{8,12},{12,8},{9,1... | collective-permute-start | bytes 147464 | tf_op jit(solution)/shard_map/ppermute | solution.py:34
  9.1 12.1 %collective-permute-start.6 = (bf16[352,512]{1,0:T(8,128)(2,1)S(1)}, bf16[352,512]{1,0:T(8,128)(2,1)S(1)}, u32[]{:S(2)}, u32[]{:S(2)}) collective-permute-start(bf16[352,512]{1,0:T(8,128)(2,1)S(1)} %expand.1.refs_4_.refs_0_), channel_id=1, source_target_pairs={{0,32},{32,64},{64,96},{96,128},{128,160},{160,192},{192,224},{224... | collective-permute-start | bytes 1081352 | tf_op jit(solution)/shard_map/ppermute | solution.py:395
  17.9 8.9 %collective-permute-start.4 = (bf16[272,384]{1,0:T(8,128)(2,1)S(1)}, bf16[272,384]{1,0:T(8,128)(2,1)S(1)}, u32[]{:S(2)}, u32[]{:S(2)}) collective-permute-start(bf16[272,384]{1,0:T(8,128)(2,1)S(1)} %lay.1.refs_0_), channel_id=1, source_target_pairs={{0,24},{8,0},{16,8},{24,16},{1,25},{9,1},{17,9},{25,17},{2,26},{10... | collective-permute-start | bytes 626696 | tf_op jit(solution)/shard_map/ppermute | solution.py:30
  18.7 8.2 %collective-permute-start.2 = (bf16[272,384]{1,0:T(8,128)(2,1)S(1)}, bf16[272,384]{1,0:T(8,128)(2,1)S(1)}, u32[]{:S(2)}, u32[]{:S(2)}) collective-permute-start(bf16[272,384]{1,0:T(8,128)(2,1)S(1)} %lay.1.refs_0_), channel_id=1, source_target_pairs={{0,8},{8,16},{16,24},{24,0},{1,9},{9,17},{17,25},{25,1},{2,10},{10... | collective-permute-start | bytes 626696 | tf_op jit(solution)/shard_map/ppermute | solution.py:30
  21.2 11.7 %collective-permute-start.7 = (bf16[352,512]{1,0:T(8,128)(2,1)S(1)}, bf16[352,512]{1,0:T(8,128)(2,1)S(1)}, u32[]{:S(2)}, u32[]{:S(2)}) collective-permute-start(bf16[352,512]{1,0:T(8,128)(2,1)S(1)} %collective-permute-done.6.refs_5_.refs_1_), channel_id=1, source_target_pairs={{0,32},{32,64},{64,96},{96,128},{128,160},{160,192},{192,224},{224... | collective-permute-start | bytes 1081352 | tf_op jit(solution)/shard_map/ppermute | solution.py:395
  26.8 5.9 %collective-permute-start.21 = (bf16[128,384]{1,0:T(8,128)(2,1)S(1)}, bf16[128,384]{1,0:T(8,128)(2,1)S(1)}, u32[]{:S(2)}, u32[]{:S(2)}) collective-permute-start(bf16[128,384]{1,0:T(8,128)(2,1)S(1)} %slice.58), channel_id=1, source_target_pairs={{0,24},{8,0},{16,8},{24,16},{1,25},{9,1},{17,9},{25,17},{2,26},{10... | collective-permute-start | bytes 294920 | tf_op jit(solution)/shard_map/ppermute | solution.py:30
  32.8 14.8 %collective-permute-start.23 = (bf16[512,384]{1,0:T(8,128)(2,1)S(1)}, bf16[512,384]{1,0:T(8,128)(2,1)S(1)}, u32[]{:S(2)}, u32[]{:S(2)}) collective-permute-start(bf16[512,384]{1,0:T(8,128)(2,1)S(1)} %pad_maximum_fusion.refs_0_), channel_id=1, source_target_pairs={{0,224},{32,0},{64,32},{96,64},{128,96},{160,128},{192,160},{224,1... | collective-permute-start | bytes 1179656 | tf_op jit(solution)/shard_map/ppermute | solution.py:30
  32.9 9.8 %collective-permute-start.8 = (bf16[352,512]{1,0:T(8,128)(2,1)S(1)}, bf16[352,512]{1,0:T(8,128)(2,1)S(1)}, u32[]{:S(2)}, u32[]{:S(2)}) collective-permute-start(bf16[352,512]{1,0:T(8,128)(2,1)S(1)} %collective-permute-done.7.refs_6_.refs_2_), channel_id=1, source_target_pairs={{0,32},{32,64},{64,96},{96,128},{128,160},{160,192},{192,224},{224... | collective-permute-start | bytes 1081352 | tf_op jit(solution)/shard_map/ppermute | solution.py:395
  36.1 11.6 %collective-permute-start.22 = (bf16[512,384]{1,0:T(8,128)(2,1)S(1)}, bf16[512,384]{1,0:T(8,128)(2,1)S(1)}, u32[]{:S(2)}, u32[]{:S(2)}) collective-permute-start(bf16[512,384]{1,0:T(8,128)(2,1)S(1)} %pad_maximum_fusion.refs_0_), channel_id=1, source_target_pairs={{0,32},{32,64},{64,96},{96,128},{128,160},{160,192},{192,224},{224... | collective-permute-start | bytes 1179656 | tf_op jit(solution)/shard_map/ppermute | solution.py:30
  36.9 11.2 %collective-permute-start.10 = (bf16[352,512]{1,0:T(8,128)(2,1)S(1)}, bf16[352,512]{1,0:T(8,128)(2,1)S(1)}, u32[]{:S(2)}, u32[]{:S(2)}) collective-permute-start(bf16[352,512]{1,0:T(8,128)(2,1)S(1)} %collective-permute-done.6.refs_5_.refs_1_), channel_id=1, source_target_pairs={{0,4},{4,0},{1,5},{5,1},{2,6},{6,2},{3,7},{7,3},{8,12},{12,8},{9,1... | collective-permute-start | bytes 1081352 | tf_op jit(solution)/shard_map/ppermute | solution.py:34
  36.9 9.6 %collective-permute-start.3 = (bf16[144,384]{1,0:T(8,128)(2,1)S(1)}, bf16[144,384]{1,0:T(8,128)(2,1)S(1)}, u32[]{:S(2)}, u32[]{:S(2)}) collective-permute-start(bf16[144,384]{1,0:T(8,128)(2,1)S(1)} %slice.54), channel_id=1, source_target_pairs={{0,8},{8,16},{16,24},{24,0},{1,9},{9,17},{17,25},{25,1},{2,10},{10... | collective-permute-start | bytes 331784 | tf_op jit(solution)/shard_map/ppermute | solution.py:30
  42.7 8.2 %collective-permute-start.9 = (bf16[176,512]{1,0:T(8,128)(2,1)S(1)}, bf16[176,512]{1,0:T(8,128)(2,1)S(1)}, u32[]{:S(2)}, u32[]{:S(2)}) collective-permute-start(bf16[176,512]{1,0:T(8,128)(2,1)S(1)} %slice.55), channel_id=1, source_target_pairs={{0,32},{32,64},{64,96},{96,128},{128,160},{160,192},{192,224},{224... | collective-permute-start | bytes 540680 | tf_op jit(solution)/shard_map/ppermute | solution.py:395
  46.5 7.6 %collective-permute-start.11 = (bf16[352,512]{1,0:T(8,128)(2,1)S(1)}, bf16[352,512]{1,0:T(8,128)(2,1)S(1)}, u32[]{:S(2)}, u32[]{:S(2)}) collective-permute-start(bf16[352,512]{1,0:T(8,128)(2,1)S(1)} %collective-permute-done.7.refs_6_.refs_2_), channel_id=1, source_target_pairs={{0,4},{4,0},{1,5},{5,1},{2,6},{6,2},{3,7},{7,3},{8,12},{12,8},{9,1... | collective-permute-start | bytes 1081352 | tf_op jit(solution)/shard_map/ppermute | solution.py:34
  47.6 7.5 %collective-permute-start.12 = (bf16[352,512]{1,0:T(8,128)(2,1)S(1)}, bf16[352,512]{1,0:T(8,128)(2,1)S(1)}, u32[]{:S(2)}, u32[]{:S(2)}) collective-permute-start(bf16[352,512]{1,0:T(8,128)(2,1)S(1)} %collective-permute-done.8.refs_7_.refs_3_), channel_id=1, source_target_pairs={{0,4},{4,0},{1,5},{5,1},{2,6},{6,2},{3,7},{7,3},{8,12},{12,8},{9,1... | collective-permute-start | bytes 1081352 | tf_op jit(solution)/shard_map/ppermute | solution.py:34
  47.7 22.1 %collective-permute-start.25 = (bf16[512,384]{1,0:T(8,128)(2,1)S(1)}, bf16[512,384]{1,0:T(8,128)(2,1)S(1)}, u32[]{:S(2)}, u32[]{:S(2)}) collective-permute-start(bf16[512,384]{1,0:T(8,128)(2,1)S(1)} %collective-permute-done.23.refs_2_), channel_id=1, source_target_pairs={{0,224},{32,0},{64,32},{96,64},{128,96},{160,128},{192,160},{224,1... | collective-permute-start | bytes 1179656 | tf_op jit(solution)/shard_map/ppermute | solution.py:30
  48.1 21.7 %collective-permute-start.24 = (bf16[512,384]{1,0:T(8,128)(2,1)S(1)}, bf16[512,384]{1,0:T(8,128)(2,1)S(1)}, u32[]{:S(2)}, u32[]{:S(2)}) collective-permute-start(bf16[512,384]{1,0:T(8,128)(2,1)S(1)} %collective-permute-done.22.refs_1_), channel_id=1, source_target_pairs={{0,32},{32,64},{64,96},{96,128},{128,160},{160,192},{192,224},{224... | collective-permute-start | bytes 1179656 | tf_op jit(solution)/shard_map/ppermute | solution.py:30
  59.8 7.4 %collective-permute-start.14 = (bf16[144,256]{1,0:T(8,128)(2,1)S(1)}, bf16[144,256]{1,0:T(8,128)(2,1)S(1)}, u32[]{:S(2)}, u32[]{:S(2)}) collective-permute-start(bf16[144,256]{1,0:T(8,128)(2,1)S(1)} %get-tuple-element.22), channel_id=1, source_target_pairs={{0,24},{8,0},{16,8},{24,16},{1,25},{9,1},{17,9},{25,17},{2,26},{10... | collective-permute-start | bytes 221192 | tf_op jit(solution)/shard_map/ppermute | solution.py:30
  59.9 7.3 %collective-permute-start.15 = (bf16[144,256]{1,0:T(8,128)(2,1)S(1)}, bf16[144,256]{1,0:T(8,128)(2,1)S(1)}, u32[]{:S(2)}, u32[]{:S(2)}) collective-permute-start(bf16[144,256]{1,0:T(8,128)(2,1)S(1)} %get-tuple-element.23), channel_id=1, source_target_pairs={{0,16},{8,24},{16,0},{24,8},{1,17},{9,25},{17,1},{25,9},{2,18},{10... | collective-permute-start | bytes 221192 | tf_op jit(solution)/shard_map/ppermute | solution.py:30
  61.3 6.5 %collective-permute-start.16 = (bf16[144,256]{1,0:T(8,128)(2,1)S(1)}, bf16[144,256]{1,0:T(8,128)(2,1)S(1)}, u32[]{:S(2)}, u32[]{:S(2)}) collective-permute-start(bf16[144,256]{1,0:T(8,128)(2,1)S(1)} %get-tuple-element.24), channel_id=1, source_target_pairs={{0,8},{8,16},{16,24},{24,0},{1,9},{9,17},{17,25},{25,1},{2,10},{10... | collective-permute-start | bytes 221192 | tf_op jit(solution)/shard_map/ppermute | solution.py:30
  68.2 7.9 %collective-permute-start.19 = (bf16[144,256]{1,0:T(8,128)(2,1)S(1)}, bf16[144,256]{1,0:T(8,128)(2,1)S(1)}, u32[]{:S(2)}, u32[]{:S(2)}) collective-permute-start(bf16[144,256]{1,0:T(8,128)(2,1)S(1)} %join.1.refs_0_), channel_id=1, source_target_pairs={{0,1},{1,2},{2,3},{3,0},{4,5},{5,6},{6,7},{7,4},{8,9},{9,10},{10,1... | collective-permute-start | bytes 221192 | tf_op jit(solution)/shard_map/ppermute | solution.py:30
  69.8 18.3 %collective-permute-start.27 = (bf16[512,384]{1,0:T(8,128)(2,1)S(1)}, bf16[512,384]{1,0:T(8,128)(2,1)S(1)}, u32[]{:S(2)}, u32[]{:S(2)}) collective-permute-start(bf16[512,384]{1,0:T(8,128)(2,1)S(1)} %collective-permute-done.25.refs_4_), channel_id=1, source_target_pairs={{0,224},{32,0},{64,32},{96,64},{128,96},{160,128},{192,160},{224,1... | collective-permute-start | bytes 1179656 | tf_op jit(solution)/shard_map/ppermute | solution.py:30
  69.8 18.4 %collective-permute-start.26 = (bf16[512,384]{1,0:T(8,128)(2,1)S(1)}, bf16[512,384]{1,0:T(8,128)(2,1)S(1)}, u32[]{:S(2)}, u32[]{:S(2)}) collective-permute-start(bf16[512,384]{1,0:T(8,128)(2,1)S(1)} %collective-permute-done.24.refs_3_), channel_id=1, source_target_pairs={{0,32},{32,64},{64,96},{96,128},{128,160},{160,192},{192,224},{224... | collective-permute-start | bytes 1179656 | tf_op jit(solution)/shard_map/ppermute | solution.py:30
  73.7 17.8 %collective-permute-start.31 = (bf16[512,384]{1,0:T(8,128)(2,1)S(1)}, bf16[512,384]{1,0:T(8,128)(2,1)S(1)}, u32[]{:S(2)}, u32[]{:S(2)}) collective-permute-start(bf16[512,384]{1,0:T(8,128)(2,1)S(1)} %lay_down.1.refs_8_), channel_id=1, source_target_pairs={{0,8},{8,16},{16,24},{24,0},{1,9},{9,17},{17,25},{25,1},{2,10},{10... | collective-permute-start | bytes 1179656 | tf_op jit(solution)/shard_map/ppermute | solution.py:30
  76.2 18.7 %collective-permute-start.30 = (bf16[512,384]{1,0:T(8,128)(2,1)S(1)}, bf16[512,384]{1,0:T(8,128)(2,1)S(1)}, u32[]{:S(2)}, u32[]{:S(2)}) collective-permute-start(bf16[512,384]{1,0:T(8,128)(2,1)S(1)} %lay_down.1.refs_8_), channel_id=1, source_target_pairs={{0,24},{8,0},{16,8},{24,16},{1,25},{9,1},{17,9},{25,17},{2,26},{10... | collective-permute-start | bytes 1179656 | tf_op jit(solution)/shard_map/ppermute | solution.py:30
  88.0 14.7 %collective-permute-start.20 = (bf16[144,2048]{1,0:T(8,128)(2,1)S(1)}, bf16[144,2048]{1,0:T(8,128)(2,1)S(1)}, u32[]{:S(2)}, u32[]{:S(2)}) collective-permute-start(bf16[144,2048]{1,0:T(8,128)(2,1)S(1)} %get-tuple-element.26.own), channel_id=1, source_target_pairs={{0,4},{4,0},{1,5},{5,1},{2,6},{6,2},{3,7},{7,3},{8,12},{12,8},{9,1... | collective-permute-start | bytes 1769480 | tf_op jit(solution)/shard_map/ppermute | solution.py:34
  88.1 8.6 %collective-permute-start.29 = (bf16[256,384]{1,0:T(8,128)(2,1)S(1)}, bf16[256,384]{1,0:T(8,128)(2,1)S(1)}, u32[]{:S(2)}, u32[]{:S(2)}) collective-permute-start(bf16[256,384]{1,0:T(8,128)(2,1)S(1)} %slice.61), channel_id=1, source_target_pairs={{0,224},{32,0},{64,32},{96,64},{128,96},{160,128},{192,160},{224,1... | collective-permute-start | bytes 589832 | tf_op jit(solution)/shard_map/ppermute | solution.py:30
  88.2 8.5 %collective-permute-start.28 = (bf16[256,384]{1,0:T(8,128)(2,1)S(1)}, bf16[256,384]{1,0:T(8,128)(2,1)S(1)}, u32[]{:S(2)}, u32[]{:S(2)}) collective-permute-start(bf16[256,384]{1,0:T(8,128)(2,1)S(1)} %slice.60), channel_id=1, source_target_pairs={{0,32},{32,64},{64,96},{96,128},{128,160},{160,192},{192,224},{224... | collective-permute-start | bytes 589832 | tf_op jit(solution)/shard_map/ppermute | solution.py:30
  91.6 7.6 %collective-permute-start.32 = (bf16[256,384]{1,0:T(8,128)(2,1)S(1)}, bf16[256,384]{1,0:T(8,128)(2,1)S(1)}, u32[]{:S(2)}, u32[]{:S(2)}) collective-permute-start(bf16[256,384]{1,0:T(8,128)(2,1)S(1)} %slice.62), channel_id=1, source_target_pairs={{0,8},{8,16},{16,24},{24,0},{1,9},{9,17},{17,25},{25,1},{2,10},{10... | collective-permute-start | bytes 589832 | tf_op jit(solution)/shard_map/ppermute | solution.py:30
  94.9 7.7 %collective-permute-start.33 = (bf16[256,384]{1,0:T(8,128)(2,1)S(1)}, bf16[256,384]{1,0:T(8,128)(2,1)S(1)}, u32[]{:S(2)}, u32[]{:S(2)}) collective-permute-start(bf16[256,384]{1,0:T(8,128)(2,1)S(1)} %slice.63), channel_id=1, source_target_pairs={{0,24},{8,0},{16,8},{24,16},{1,25},{9,1},{17,9},{25,17},{2,26},{10... | collective-permute-start | bytes 589832 | tf_op jit(solution)/shard_map/ppermute | solution.py:30
  107.9 6.8 %collective-permute-start.35 = (bf16[32,2048]{1,0:T(8,128)(2,1)S(1)}, bf16[32,2048]{1,0:T(8,128)(2,1)S(1)}, u32[]{:S(2)}, u32[]{:S(2)}) collective-permute-start(bf16[32,2048]{1,0:T(8,128)(2,1)S(1)} %get-tuple-element.31), channel_id=1, source_target_pairs={{0,1},{1,2},{2,3},{3,0},{4,5},{5,6},{6,7},{7,4},{8,9},{9,10},{10,1... | collective-permute-start | bytes 393224 | tf_op jit(solution)/shard_map/ppermute | solution.py:30
  109.4 7.5 %collective-permute-start.37 = (bf16[32,2048]{1,0:T(8,128)(2,1)S(1)}, bf16[32,2048]{1,0:T(8,128)(2,1)S(1)}, u32[]{:S(2)}, u32[]{:S(2)}) collective-permute-start(bf16[32,2048]{1,0:T(8,128)(2,1)S(1)} %get-tuple-element.32), channel_id=1, source_target_pairs={{0,3},{1,0},{2,1},{3,2},{4,7},{5,4},{6,5},{7,6},{8,11},{9,8},{10,9... | collective-permute-start | bytes 393224 | tf_op jit(solution)/shard_map/ppermute | solution.py:30
  111.2 7.5 %collective-permute-start.36 = (bf16[32,2048]{1,0:T(8,128)(2,1)S(1)}, bf16[32,2048]{1,0:T(8,128)(2,1)S(1)}, u32[]{:S(2)}, u32[]{:S(2)}) collective-permute-start(bf16[32,2048]{1,0:T(8,128)(2,1)S(1)} %get-tuple-element.33), channel_id=1, source_target_pairs={{0,2},{1,3},{2,0},{3,1},{4,6},{5,7},{6,4},{7,5},{8,10},{9,11},{10,... | collective-permute-start | bytes 393224 | tf_op jit(solution)/shard_map/ppermute | solution.py:30
  (17 other events, 178.6 us)

commit v2 on v1

--- a/solution.py
+++ b/solution.py
@@ -47,25 +47,6 @@
 
 VM = pl.BlockSpec(memory_space=pltpu.VMEM)
 SM = pl.BlockSpec(memory_space=pltpu.SMEM)
-
-
-def pack_kernel(lat, down, key, out):
-    out[0:128, :] = lat[...]
-    out[128:160, :] = down[:, 0:512]
-    out[160:176, 0:256] = down[0:16, 512:768]
-    out[160:176, 256:512] = down[16:32, 512:768]
-    for i in range(4):
-        out[176:192, 128 * i : 128 * i + 128] = key[16 * i : 16 * i + 16, :]
-
-
-def pack(lat, down, key):
-    return pl.pallas_call(
-        pack_kernel,
-        in_specs=[VM] * 3,
-        out_shape=jax.ShapeDtypeStruct((192, 512), BF),
-        name="pack",
-        compiler_params=limit(4),
-    )(lat, down, key)
 
 
 def expand_kernel(own, other, weight, cos, sin, out):
@@ -96,9 +77,31 @@
     )(own, other, weight, cos, sin)
 
 
-def queries_kernel(meta, q, cos, sin, gate, value, out, edge, keep, send):
+def begin_kernel(meta, cos, sin, lat, down, key, q, gate, value, weight, *refs):
+    packed, out, edge, keep, send, near = refs[:6]
+    down_v, key_v, q_v, gate_v, value_v, sems = refs[6:]
     c = meta[3]
-    f = q[...].astype(F32)
+    pairs = (
+        (down, down_v),
+        (key, key_v),
+        (lat, packed.at[pl.ds(0, 128)]),
+        (q, q_v),
+        (gate, gate_v),
+        (value, value_v),
+        (weight, near),
+    )
+    copies = [pltpu.make_async_copy(a, b, sems.at[i]) for i, (a, b) in enumerate(pairs)]
+    for copy in copies:
+        copy.start()
+    copies[0].wait()
+    packed[128:160, :] = down_v[:, 0:512]
+    packed[160:176, 0:256] = down_v[0:16, 512:768]
+    packed[160:176, 256:512] = down_v[16:32, 512:768]
+    copies[1].wait()
+    for i in range(4):
+        packed[176:192, 128 * i : 128 * i + 128] = key_v[16 * i : 16 * i + 16, :]
+    copies[3].wait()
+    f = q_v[...].astype(F32)
     co, si = cos[:, 0:128], sin[:, 0:128]
     wide = turn(f[192:224], f[224:256], co, si) + [jnp.zeros((64, 128), F32)]
     narrow = turn(f[256:288], f[288:320], co, si) + [f[128:192]]
@@ -109,29 +112,32 @@
         out[:, at] = tile.astype(BF)
         line = jnp.sum(jnp.where(row == 127 * c, tile, 0.0), axis=0, keepdims=True)
         edge[:, at] = line.astype(BF)
+    copies[4].wait()
+    copies[5].wait()
 
     def halves(mine, others):
-        for i, m in enumerate((gate, value)):
+        for i, m in enumerate((gate_v, value_v)):
             keep[32 * i : 32 * i + 32, :] = m[:, mine]
             send[32 * i : 32 * i + 32, :] = m[:, others]
 
     pl.when(c == 0)(lambda: halves(slice(0, 384), slice(384, 768)))
     pl.when(c == 1)(lambda: halves(slice(384, 768), slice(0, 384)))
-
-
-def turned_queries(meta, q, cos, sin, gate, value):
-    return pl.pallas_call(
-        queries_kernel,
-        in_specs=[SM] + [VM] * 5,
-        out_shape=[
-            jax.ShapeDtypeStruct((128, 384), BF),
-            jax.ShapeDtypeStruct((1, 384), BF),
-            jax.ShapeDtypeStruct((64, 384), BF),
-            jax.ShapeDtypeStruct((64, 384), BF),
-        ],
-        name="queries",
-        compiler_params=limit(6),
-    )(meta, q, cos, sin, gate, value)
+    copies[2].wait()
+    copies[6].wait()
+
+
+def begin(meta, cos, sin, *far):
+    shapes = ((192, 512), (128, 384), (1, 384), (64, 384), (64, 384), (512, 384))
+    scratch = ((32, 768), (64, 128), (320, 128), (32, 768), (32, 768))
+    return pl.pallas_call(
+        begin_kernel,
+        in_specs=[SM, VM, VM] + [pl.BlockSpec(memory_space=pl.ANY)] * 7,
+        out_shape=[jax.ShapeDtypeStruct(shape, BF) for shape in shapes],
+        scratch_shapes=[pltpu.VMEM(shape, BF) for shape in scratch]
+        + [pltpu.SemaphoreType.DMA((7,))],
+        name="begin",
+        compiler_params=limit(8),
+    )(meta, cos, sin, *far)
 
 
 def lay_kernel(meta, q, edge, keep, got, out):
@@ -394,10 +400,20 @@
     def step(v):
         return lax.ppermute(v, ("z", "c"), ring)
 
-    packed = pack(latents, down_weight.T, shared_key.T)
-    m0 = expand(packed, swap(packed), expand_weight, cos, sin)
+    packed, q, edge, keep, send, near = begin(
+        meta,
+        cos,
+        sin,
+        latents,
+        down_weight.T,
+        shared_key.T,
+        queries.T,
+        gate_weight,
+        value_weight,
+        expand_weight,
+    )
+    m0 = expand(packed, swap(packed), near, cos, sin)
     r1 = step(m0)
-    q, edge, keep, send = turned_queries(meta, queries.T, cos, sin, gate_weight, value_weight)
     got = swap(send)
     pairs = [(i, i + 1) for i in range(1, nsp - 1, 2)] + [(i, i - 1) for i in range(2, nsp, 2)]
     line = lax.dynamic_slice_in_dim(residual, c * (tok - 1), 1, 0)

time: 120 us -> 120 us (level)
  no operation moved by 1% of the time
where the time goes in v2:
time: 120 us
  starting transfers between devices  52.8 us (44%)
  waiting for transfers between devices  45.8 us (38%)
  Pallas kernels  12.7 us (11%)
  local copies, waits for them, and re-layouts  6.99 us (6%)
  other arithmetic  1.21 us (1%)
    ppermute x25, starting transfers between devices, shift(): return lax.ppermute(x, axis, [(i, (i + k) % n) for i in range(n)])  34.4 us
    ppermute x25, waiting for transfers between devices, shift(): return lax.ppermute(x, axis, [(i, (i + k) % n) for i in range(n)])  33.8 us
    ppermute x4, starting transfers between devices, step(): return lax.ppermute(v, ('z', 'c'), ring)  11.7 us
    unnamed x22, local copies, waits for them, and re-layouts  5.92 us
    ppermute x4, waiting for transfers between devices, step(): return lax.ppermute(v, ('z', 'c'), ring)  5.67 us
    ppermute x8, starting transfers between devices, swap(): return lax.ppermute(x, 'c', [(0, 1), (1, 0)])  4.77 us
    pallas_call x1, Pallas kernels, attend(): pl.pallas_call(functools.partial(attend_kernel, nq, nk), out_shape=[jax.S...  4.69 us
    ppermute x8, waiting for transfers between devices, swap(): return lax.ppermute(x, 'c', [(0, 1), (1, 0)])  3.23 us
  transfers between devices with their start and end apart: 38, of which 17 were waited for; matrix products, arithmetic and copies ran while one was open for 1% of the time, Pallas kernels for 7%

profile of v2, /device:TPU:120, one launch (start us, length us, event | category | flops | bytes accessed | tf_op | source)
XLA Modules:
  0.0 119.9 jit_solution(9300866312921212311)
XLA Ops:
  9.7 3.2 %collective-permute-start.6 = (bf16[352,512]{1,0:T(8,128)(2,1)S(1)}, bf16[352,512]{1,0:T(8,128)(2,1)S(1)}, u32[]{:S(2)}, u32[]{:S(2)}) collective-permute-start(bf16[352,512]{1,0:T(8,128)(2,1)S(1)} %expand.1.refs_4_.refs_0_), channel_id=1, source_target_pairs={{0,32},{32,64},{64,96},{96,128},{128,160},{160,192},{192,224},{224... | collective-permute-start | bytes 1081352 | tf_op jit(solution)/shard_map/ppermute | solution.py:401
  13.0 1.9 %collective-permute-start = (bf16[1,2432]{1,0:T(2,128)(2,1)S(1)}, bf16[1,2432]{1,0:T(2,128)(2,1)S(1)}, u32[]{:S(2)}, u32[]{:S(2)}) collective-permute-start(bf16[1,2432]{1,0:T(2,128)(2,1)S(1)} %pad_maximum_fusion.2), channel_id=1, source_target_pairs={{4,8},{12,16},{20,24},{28,32},{36,40},{44,48},{52,56},{60,64},{68,... | collective-permute-start | bytes 14600 | tf_op jit(solution)/shard_map/ppermute | solution.py:421
  14.9 3.1 %collective-permute-done = bf16[1,2432]{1,0:T(2,128)(2,1)S(1)} collective-permute-done((bf16[1,2432]{1,0:T(2,128)(2,1)S(1)}, bf16[1,2432]{1,0:T(2,128)(2,1)S(1)}, u32[]{:S(2)}, u32[]{:S(2)}) %collective-permute-start) | collective-permute-done | bytes 4896 | tf_op jit(solution)/shard_map/ppermute | solution.py:421
  19.4 2.5 %collective-permute-start.2 = (bf16[272,384]{1,0:T(8,128)(2,1)S(1)}, bf16[272,384]{1,0:T(8,128)(2,1)S(1)}, u32[]{:S(2)}, u32[]{:S(2)}) collective-permute-start(bf16[272,384]{1,0:T(8,128)(2,1)S(1)} %lay.1.refs_0_), channel_id=1, source_target_pairs={{0,8},{8,16},{16,24},{24,0},{1,9},{9,17},{17,25},{25,1},{2,10},{10... | collective-permute-start | bytes 626696 | tf_op jit(solution)/shard_map/ppermute | solution.py:30
  23.4 4.1 %collective-permute-done.4.refs_3_ = bf16[272,384]{1,0:T(8,128)(2,1)S(1)} collective-permute-done((bf16[272,384]{1,0:T(8,128)(2,1)S(1)}, bf16[272,384]{1,0:T(8,128)(2,1)S(1)}, u32[]{:S(2)}, u32[]{:S(2)}) %collective-permute-start.4) | collective-permute-done | bytes 208928 | tf_op jit(solution)/shard_map/ppermute | solution.py:30
  27.6 5.8 %collective-permute-done.21 = bf16[128,384]{1,0:T(8,128)(2,1)S(1)} collective-permute-done((bf16[128,384]{1,0:T(8,128)(2,1)S(1)}, bf16[128,384]{1,0:T(8,128)(2,1)S(1)}, u32[]{:S(2)}, u32[]{:S(2)}) %collective-permute-start.21) | collective-permute-done | bytes 98336 | tf_op jit(solution)/shard_map/ppermute | solution.py:30
  33.5 3.2 %collective-permute-start.8 = (bf16[352,512]{1,0:T(8,128)(2,1)S(1)}, bf16[352,512]{1,0:T(8,128)(2,1)S(1)}, u32[]{:S(2)}, u32[]{:S(2)}) collective-permute-start(bf16[352,512]{1,0:T(8,128)(2,1)S(1)} %collective-permute-done.7.refs_6_.refs_2_), channel_id=1, source_target_pairs={{0,32},{32,64},{64,96},{96,128},{128,160},{160,192},{192,224},{224... | collective-permute-start | bytes 1081352 | tf_op jit(solution)/shard_map/ppermute | solution.py:401
  37.7 5.7 %collective-permute-done.8.refs_7_.refs_3_ = bf16[352,512]{1,0:T(8,128)(2,1)S(1)} collective-permute-done((bf16[352,512]{1,0:T(8,128)(2,1)S(1)}, bf16[352,512]{1,0:T(8,128)(2,1)S(1)}, u32[]{:S(2)}, u32[]{:S(2)}) %collective-permute-start.8) | collective-permute-done | bytes 360480 | tf_op jit(solution)/shard_map/ppermute | solution.py:401
  43.4 3.8 %collective-permute-start.9 = (bf16[176,512]{1,0:T(8,128)(2,1)S(1)}, bf16[176,512]{1,0:T(8,128)(2,1)S(1)}, u32[]{:S(2)}, u32[]{:S(2)}) collective-permute-start(bf16[176,512]{1,0:T(8,128)(2,1)S(1)} %slice.55), channel_id=1, source_target_pairs={{0,32},{32,64},{64,96},{96,128},{128,160},{160,192},{192,224},{224... | collective-permute-start | bytes 540680 | tf_op jit(solution)/shard_map/ppermute | solution.py:401
  48.7 3.0 %collective-permute-start.24 = (bf16[512,384]{1,0:T(8,128)(2,1)S(1)}, bf16[512,384]{1,0:T(8,128)(2,1)S(1)}, u32[]{:S(2)}, u32[]{:S(2)}) collective-permute-start(bf16[512,384]{1,0:T(8,128)(2,1)S(1)} %collective-permute-done.22.refs_1_), channel_id=1, source_target_pairs={{0,32},{32,64},{64,96},{96,128},{128,160},{160,192},{192,224},{224... | collective-permute-start | bytes 1179656 | tf_op jit(solution)/shard_map/ppermute | solution.py:30
  51.8 2.8 %collective-permute-start.13 = (bf16[176,512]{1,0:T(8,128)(2,1)S(1)}, bf16[176,512]{1,0:T(8,128)(2,1)S(1)}, u32[]{:S(2)}, u32[]{:S(2)}) collective-permute-start(bf16[176,512]{1,0:T(8,128)(2,1)S(1)} %collective-permute-done.9.refs_8_.refs_4_), channel_id=1, source_target_pairs={{0,4},{4,0},{1,5},{5,1},{2,6},{6,2},{3,7},{7,3},{8,12},{12,8},{9,1... | collective-permute-start | bytes 540680 | tf_op jit(solution)/shard_map/ppermute | solution.py:34
  55.6 4.7 %attend.1 = (bf16[144,256]{1,0:T(8,128)(2,1)S(1)}, bf16[144,256]{1,0:T(8,128)(2,1)S(1)}, bf16[144,256]{1,0:T(8,128)(2,1)S(1)}, bf16[144,256]{1,0:T(8,128)(2,1)S(1)}) custom-call(bf16[272,384]{1,0:T(8,128)(2,1)S(1)} %lay.1.refs_0_, bf16[272,384]{1,0:T(8,128)(2,1)S(1)} %collective-permute-done.2.refs_1_, bf16[144,384]{1,0:T(8,128)(2,1)S(1)} %collective-permute-done.3.refs_2_, ...), custom_call_target="tpu_custom_call" | custom-call | tf_op jit(solution)/shard_map/attend/pallas_call | solution.py:246
  61.8 1.9 %collective-permute-start.16 = (bf16[144,256]{1,0:T(8,128)(2,1)S(1)}, bf16[144,256]{1,0:T(8,128)(2,1)S(1)}, u32[]{:S(2)}, u32[]{:S(2)}) collective-permute-start(bf16[144,256]{1,0:T(8,128)(2,1)S(1)} %get-tuple-element.28), channel_id=1, source_target_pairs={{0,8},{8,16},{16,24},{24,0},{1,9},{9,17},{17,25},{25,1},{2,10},{10... | collective-permute-start | bytes 221192 | tf_op jit(solution)/shard_map/ppermute | solution.py:30
  63.6 4.1 %collective-permute-done.14.refs_1_ = bf16[144,256]{1,0:T(8,128)(2,1)S(1)} collective-permute-done((bf16[144,256]{1,0:T(8,128)(2,1)S(1)}, bf16[144,256]{1,0:T(8,128)(2,1)S(1)}, u32[]{:S(2)}, u32[]{:S(2)}) %collective-permute-start.14) | collective-permute-done | bytes 73760 | tf_op jit(solution)/shard_map/ppermute | solution.py:30
  70.3 3.2 %collective-permute-start.26 = (bf16[512,384]{1,0:T(8,128)(2,1)S(1)}, bf16[512,384]{1,0:T(8,128)(2,1)S(1)}, u32[]{:S(2)}, u32[]{:S(2)}) collective-permute-start(bf16[512,384]{1,0:T(8,128)(2,1)S(1)} %collective-permute-done.24.refs_3_), channel_id=1, source_target_pairs={{0,32},{32,64},{64,96},{96,128},{128,160},{160,192},{192,224},{224... | collective-permute-start | bytes 1179656 | tf_op jit(solution)/shard_map/ppermute | solution.py:30
  74.2 2.5 %collective-permute-start.31 = (bf16[512,384]{1,0:T(8,128)(2,1)S(1)}, bf16[512,384]{1,0:T(8,128)(2,1)S(1)}, u32[]{:S(2)}, u32[]{:S(2)}) collective-permute-start(bf16[512,384]{1,0:T(8,128)(2,1)S(1)} %lay_down.1.refs_8_), channel_id=1, source_target_pairs={{0,8},{8,16},{16,24},{24,0},{1,9},{9,17},{17,25},{25,1},{2,10},{10... | collective-permute-start | bytes 1179656 | tf_op jit(solution)/shard_map/ppermute | solution.py:30
  76.6 2.7 %collective-permute-start.18 = (bf16[144,256]{1,0:T(8,128)(2,1)S(1)}, bf16[144,256]{1,0:T(8,128)(2,1)S(1)}, u32[]{:S(2)}, u32[]{:S(2)}) collective-permute-start(bf16[144,256]{1,0:T(8,128)(2,1)S(1)} %join.1.refs_0_), channel_id=1, source_target_pairs={{0,2},{1,3},{2,0},{3,1},{4,6},{5,7},{6,4},{7,5},{8,10},{9,11},{10,... | collective-permute-start | bytes 221192 | tf_op jit(solution)/shard_map/ppermute | solution.py:30
  79.4 3.1 %collective-permute-done.18.refs_2_ = bf16[144,256]{1,0:T(8,128)(2,1)S(1)} collective-permute-done((bf16[144,256]{1,0:T(8,128)(2,1)S(1)}, bf16[144,256]{1,0:T(8,128)(2,1)S(1)}, u32[]{:S(2)}, u32[]{:S(2)}) %collective-permute-start.18) | collective-permute-done | bytes 73760 | tf_op jit(solution)/shard_map/ppermute | solution.py:30
  82.5 1.7 %collective-permute-start.17 = (bf16[144,256]{1,0:T(8,128)(2,1)S(1)}, bf16[144,256]{1,0:T(8,128)(2,1)S(1)}, u32[]{:S(2)}, u32[]{:S(2)}) collective-permute-start(bf16[144,256]{1,0:T(8,128)(2,1)S(1)} %join.1.refs_0_), channel_id=1, source_target_pairs={{0,3},{1,0},{2,1},{3,2},{4,7},{5,4},{6,5},{7,6},{8,11},{9,8},{10,9... | collective-permute-start | bytes 221192 | tf_op jit(solution)/shard_map/ppermute | solution.py:30
  84.3 2.6 %collective-permute-done.17.refs_1_ = bf16[144,256]{1,0:T(8,128)(2,1)S(1)} collective-permute-done((bf16[144,256]{1,0:T(8,128)(2,1)S(1)}, bf16[144,256]{1,0:T(8,128)(2,1)S(1)}, u32[]{:S(2)}, u32[]{:S(2)}) %collective-permute-start.17) | collective-permute-done | bytes 73760 | tf_op jit(solution)/shard_map/ppermute | solution.py:30
  86.9 1.6 %project.1 = (bf16[32,2048]{1,0:T(8,128)(2,1)S(1)}, bf16[144,2048]{1,0:T(8,128)(2,1)S(1)}) custom-call(s32[5]{0:T(128)S(1)} %stack.27.meta, bf16[144,256]{1,0:T(8,128)(2,1)S(1)} %join.1.refs_0_, bf16[144,256]{1,0:T(8,128)(2,1)S(1)} %collective-permute-done.17.refs_1_, bf16[144,256]{1,0:T(8,128)(2,1)S(1)} %collective-permute-done.18.refs_2_, ...), custom_call_target="tpu_custom_call" | custom-call | tf_op jit(solution)/shard_map/project/pallas_call | solution.py:303
  88.7 3.3 %collective-permute-start.28 = (bf16[256,384]{1,0:T(8,128)(2,1)S(1)}, bf16[256,384]{1,0:T(8,128)(2,1)S(1)}, u32[]{:S(2)}, u32[]{:S(2)}) collective-permute-start(bf16[256,384]{1,0:T(8,128)(2,1)S(1)} %slice.60), channel_id=1, source_target_pairs={{0,32},{32,64},{64,96},{96,128},{128,160},{160,192},{192,224},{224... | collective-permute-start | bytes 589832 | tf_op jit(solution)/shard_map/ppermute | solution.py:30
  92.1 3.3 %collective-permute-start.32 = (bf16[256,384]{1,0:T(8,128)(2,1)S(1)}, bf16[256,384]{1,0:T(8,128)(2,1)S(1)}, u32[]{:S(2)}, u32[]{:S(2)}) collective-permute-start(bf16[256,384]{1,0:T(8,128)(2,1)S(1)} %slice.62), channel_id=1, source_target_pairs={{0,8},{8,16},{16,24},{24,0},{1,9},{9,17},{17,25},{25,1},{2,10},{10... | collective-permute-start | bytes 589832 | tf_op jit(solution)/shard_map/ppermute | solution.py:30
  95.5 1.7 %collective-permute-done.29 = bf16[256,384]{1,0:T(8,128)(2,1)S(1)} collective-permute-done((bf16[256,384]{1,0:T(8,128)(2,1)S(1)}, bf16[256,384]{1,0:T(8,128)(2,1)S(1)}, u32[]{:S(2)}, u32[]{:S(2)}) %collective-permute-start.29) | collective-permute-done | bytes 196640 | tf_op jit(solution)/shard_map/ppermute | solution.py:30
  97.2 2.4 %collective-permute-done.32.refs_10_ = bf16[256,384]{1,0:T(8,128)(2,1)S(1)} collective-permute-done((bf16[256,384]{1,0:T(8,128)(2,1)S(1)}, bf16[256,384]{1,0:T(8,128)(2,1)S(1)}, u32[]{:S(2)}, u32[]{:S(2)}) %collective-permute-start.32) | collective-permute-done | bytes 196640 | tf_op jit(solution)/shard_map/ppermute | solution.py:30
  99.6 3.5 %collective-permute-done.33.refs_11_ = bf16[256,384]{1,0:T(8,128)(2,1)S(1)} collective-permute-done((bf16[256,384]{1,0:T(8,128)(2,1)S(1)}, bf16[256,384]{1,0:T(8,128)(2,1)S(1)}, u32[]{:S(2)}, u32[]{:S(2)}) %collective-permute-start.33) | collective-permute-done | bytes 196640 | tf_op jit(solution)/shard_map/ppermute | solution.py:30
  103.1 3.0 %mixer.1 = (f32[128,2048]{1,0:T(8,128)S(1)}, bf16[128,2048]{1,0:T(8,128)(2,1)S(1)}) custom-call(s32[5]{0:T(128)S(1)} %stack.27.meta, bf16[144,2048]{1,0:T(8,128)(2,1)S(1)} %get-tuple-element.30.own, bf16[144,2048]{1,0:T(8,128)(2,1)S(1)} %collective-permute-done.20.other, bf16[3,384]{1,0:T(4,128)(2,1)S(1)} %slice_select_fusion.taps, ...), custom_call_target="tpu_custom_call" | custom-call | tf_op jit(solution)/shard_map/mixer/pallas_call | solution.py:362
  106.3 1.9 %collective-permute-done.34 = bf16[128,2048]{1,0:T(8,128)(2,1)S(1)} collective-permute-done((bf16[128,2048]{1,0:T(8,128)(2,1)S(1)}, bf16[128,2048]{1,0:T(8,128)(2,1)S(1)}, u32[]{:S(2)}, u32[]{:S(2)}) %collective-permute-start.34) | collective-permute-done | bytes 524320 | tf_op jit(solution)/shard_map/ppermute | solution.py:34
  109.9 1.7 %collective-permute-start.37 = (bf16[32,2048]{1,0:T(8,128)(2,1)S(1)}, bf16[32,2048]{1,0:T(8,128)(2,1)S(1)}, u32[]{:S(2)}, u32[]{:S(2)}) collective-permute-start(bf16[32,2048]{1,0:T(8,128)(2,1)S(1)} %get-tuple-element.36), channel_id=1, source_target_pairs={{0,3},{1,0},{2,1},{3,2},{4,7},{5,4},{6,5},{7,6},{8,11},{9,8},{10,9... | collective-permute-start | bytes 393224 | tf_op jit(solution)/shard_map/ppermute | solution.py:30
  113.2 2.0 %collective-permute-done.35 = bf16[32,2048]{1,0:T(8,128)(2,1)S(1)} collective-permute-done((bf16[32,2048]{1,0:T(8,128)(2,1)S(1)}, bf16[32,2048]{1,0:T(8,128)(2,1)S(1)}, u32[]{:S(2)}, u32[]{:S(2)}) %collective-permute-start.35) | collective-permute-done | bytes 131104 | tf_op jit(solution)/shard_map/ppermute | solution.py:30
  115.2 2.2 %collective-permute-done.37 = bf16[32,2048]{1,0:T(8,128)(2,1)S(1)} collective-permute-done((bf16[32,2048]{1,0:T(8,128)(2,1)S(1)}, bf16[32,2048]{1,0:T(8,128)(2,1)S(1)}, u32[]{:S(2)}, u32[]{:S(2)}) %collective-permute-start.37) | collective-permute-done | bytes 131104 | tf_op jit(solution)/shard_map/ppermute | solution.py:30
  117.4 1.8 %collective-permute-done.36 = bf16[32,2048]{1,0:T(8,128)(2,1)S(1)} collective-permute-done((bf16[32,2048]{1,0:T(8,128)(2,1)S(1)}, bf16[32,2048]{1,0:T(8,128)(2,1)S(1)}, u32[]{:S(2)}, u32[]{:S(2)}) %collective-permute-start.36) | collective-permute-done | bytes 131104 | tf_op jit(solution)/shard_map/ppermute | solution.py:30
  (100 shorter events, 25.6 us)
Async XLA Ops:
  7.7 10.2 %collective-permute-start.1 = (bf16[64,384]{1,0:T(8,128)(2,1)S(1)}, bf16[64,384]{1,0:T(8,128)(2,1)S(1)}, u32[]{:S(2)}, u32[]{:S(2)}) collective-permute-start(bf16[64,384]{1,0:T(8,128)(2,1)S(1)} %get-tuple-element.22), channel_id=1, source_target_pairs={{0,4},{4,0},{1,5},{5,1},{2,6},{6,2},{3,7},{7,3},{8,12},{12,8},{9,1... | collective-permute-start | bytes 147464 | tf_op jit(solution)/shard_map/ppermute | solution.py:34
  9.7 12.1 %collective-permute-start.6 = (bf16[352,512]{1,0:T(8,128)(2,1)S(1)}, bf16[352,512]{1,0:T(8,128)(2,1)S(1)}, u32[]{:S(2)}, u32[]{:S(2)}) collective-permute-start(bf16[352,512]{1,0:T(8,128)(2,1)S(1)} %expand.1.refs_4_.refs_0_), channel_id=1, source_target_pairs={{0,32},{32,64},{64,96},{96,128},{128,160},{160,192},{192,224},{224... | collective-permute-start | bytes 1081352 | tf_op jit(solution)/shard_map/ppermute | solution.py:401
  18.5 8.9 %collective-permute-start.4 = (bf16[272,384]{1,0:T(8,128)(2,1)S(1)}, bf16[272,384]{1,0:T(8,128)(2,1)S(1)}, u32[]{:S(2)}, u32[]{:S(2)}) collective-permute-start(bf16[272,384]{1,0:T(8,128)(2,1)S(1)} %lay.1.refs_0_), channel_id=1, source_target_pairs={{0,24},{8,0},{16,8},{24,16},{1,25},{9,1},{17,9},{25,17},{2,26},{10... | collective-permute-start | bytes 626696 | tf_op jit(solution)/shard_map/ppermute | solution.py:30
  19.4 8.2 %collective-permute-start.2 = (bf16[272,384]{1,0:T(8,128)(2,1)S(1)}, bf16[272,384]{1,0:T(8,128)(2,1)S(1)}, u32[]{:S(2)}, u32[]{:S(2)}) collective-permute-start(bf16[272,384]{1,0:T(8,128)(2,1)S(1)} %lay.1.refs_0_), channel_id=1, source_target_pairs={{0,8},{8,16},{16,24},{24,0},{1,9},{9,17},{17,25},{25,1},{2,10},{10... | collective-permute-start | bytes 626696 | tf_op jit(solution)/shard_map/ppermute | solution.py:30
  21.8 11.7 %collective-permute-start.7 = (bf16[352,512]{1,0:T(8,128)(2,1)S(1)}, bf16[352,512]{1,0:T(8,128)(2,1)S(1)}, u32[]{:S(2)}, u32[]{:S(2)}) collective-permute-start(bf16[352,512]{1,0:T(8,128)(2,1)S(1)} %collective-permute-done.6.refs_5_.refs_1_), channel_id=1, source_target_pairs={{0,32},{32,64},{64,96},{96,128},{128,160},{160,192},{192,224},{224... | collective-permute-start | bytes 1081352 | tf_op jit(solution)/shard_map/ppermute | solution.py:401
  27.5 5.9 %collective-permute-start.21 = (bf16[128,384]{1,0:T(8,128)(2,1)S(1)}, bf16[128,384]{1,0:T(8,128)(2,1)S(1)}, u32[]{:S(2)}, u32[]{:S(2)}) collective-permute-start(bf16[128,384]{1,0:T(8,128)(2,1)S(1)} %slice.58), channel_id=1, source_target_pairs={{0,24},{8,0},{16,8},{24,16},{1,25},{9,1},{17,9},{25,17},{2,26},{10... | collective-permute-start | bytes 294920 | tf_op jit(solution)/shard_map/ppermute | solution.py:30
  33.4 14.8 %collective-permute-start.23 = (bf16[512,384]{1,0:T(8,128)(2,1)S(1)}, bf16[512,384]{1,0:T(8,128)(2,1)S(1)}, u32[]{:S(2)}, u32[]{:S(2)}) collective-permute-start(bf16[512,384]{1,0:T(8,128)(2,1)S(1)} %pad_maximum_fusion.refs_0_), channel_id=1, source_target_pairs={{0,224},{32,0},{64,32},{96,64},{128,96},{160,128},{192,160},{224,1... | collective-permute-start | bytes 1179656 | tf_op jit(solution)/shard_map/ppermute | solution.py:30
  33.5 9.8 %collective-permute-start.8 = (bf16[352,512]{1,0:T(8,128)(2,1)S(1)}, bf16[352,512]{1,0:T(8,128)(2,1)S(1)}, u32[]{:S(2)}, u32[]{:S(2)}) collective-permute-start(bf16[352,512]{1,0:T(8,128)(2,1)S(1)} %collective-permute-done.7.refs_6_.refs_2_), channel_id=1, source_target_pairs={{0,32},{32,64},{64,96},{96,128},{128,160},{160,192},{192,224},{224... | collective-permute-start | bytes 1081352 | tf_op jit(solution)/shard_map/ppermute | solution.py:401
  36.8 11.6 %collective-permute-start.22 = (bf16[512,384]{1,0:T(8,128)(2,1)S(1)}, bf16[512,384]{1,0:T(8,128)(2,1)S(1)}, u32[]{:S(2)}, u32[]{:S(2)}) collective-permute-start(bf16[512,384]{1,0:T(8,128)(2,1)S(1)} %pad_maximum_fusion.refs_0_), channel_id=1, source_target_pairs={{0,32},{32,64},{64,96},{96,128},{128,160},{160,192},{192,224},{224... | collective-permute-start | bytes 1179656 | tf_op jit(solution)/shard_map/ppermute | solution.py:30
  37.6 11.2 %collective-permute-start.10 = (bf16[352,512]{1,0:T(8,128)(2,1)S(1)}, bf16[352,512]{1,0:T(8,128)(2,1)S(1)}, u32[]{:S(2)}, u32[]{:S(2)}) collective-permute-start(bf16[352,512]{1,0:T(8,128)(2,1)S(1)} %collective-permute-done.6.refs_5_.refs_1_), channel_id=1, source_target_pairs={{0,4},{4,0},{1,5},{5,1},{2,6},{6,2},{3,7},{7,3},{8,12},{12,8},{9,1... | collective-permute-start | bytes 1081352 | tf_op jit(solution)/shard_map/ppermute | solution.py:34
  37.6 9.6 %collective-permute-start.3 = (bf16[144,384]{1,0:T(8,128)(2,1)S(1)}, bf16[144,384]{1,0:T(8,128)(2,1)S(1)}, u32[]{:S(2)}, u32[]{:S(2)}) collective-permute-start(bf16[144,384]{1,0:T(8,128)(2,1)S(1)} %slice.54), channel_id=1, source_target_pairs={{0,8},{8,16},{16,24},{24,0},{1,9},{9,17},{17,25},{25,1},{2,10},{10... | collective-permute-start | bytes 331784 | tf_op jit(solution)/shard_map/ppermute | solution.py:30
  43.4 8.4 %collective-permute-start.9 = (bf16[176,512]{1,0:T(8,128)(2,1)S(1)}, bf16[176,512]{1,0:T(8,128)(2,1)S(1)}, u32[]{:S(2)}, u32[]{:S(2)}) collective-permute-start(bf16[176,512]{1,0:T(8,128)(2,1)S(1)} %slice.55), channel_id=1, source_target_pairs={{0,32},{32,64},{64,96},{96,128},{128,160},{160,192},{192,224},{224... | collective-permute-start | bytes 540680 | tf_op jit(solution)/shard_map/ppermute | solution.py:401
  47.2 7.4 %collective-permute-start.11 = (bf16[352,512]{1,0:T(8,128)(2,1)S(1)}, bf16[352,512]{1,0:T(8,128)(2,1)S(1)}, u32[]{:S(2)}, u32[]{:S(2)}) collective-permute-start(bf16[352,512]{1,0:T(8,128)(2,1)S(1)} %collective-permute-done.7.refs_6_.refs_2_), channel_id=1, source_target_pairs={{0,4},{4,0},{1,5},{5,1},{2,6},{6,2},{3,7},{7,3},{8,12},{12,8},{9,1... | collective-permute-start | bytes 1081352 | tf_op jit(solution)/shard_map/ppermute | solution.py:34
  48.2 7.4 %collective-permute-start.12 = (bf16[352,512]{1,0:T(8,128)(2,1)S(1)}, bf16[352,512]{1,0:T(8,128)(2,1)S(1)}, u32[]{:S(2)}, u32[]{:S(2)}) collective-permute-start(bf16[352,512]{1,0:T(8,128)(2,1)S(1)} %collective-permute-done.8.refs_7_.refs_3_), channel_id=1, source_target_pairs={{0,4},{4,0},{1,5},{5,1},{2,6},{6,2},{3,7},{7,3},{8,12},{12,8},{9,1... | collective-permute-start | bytes 1081352 | tf_op jit(solution)/shard_map/ppermute | solution.py:34
  48.4 22.0 %collective-permute-start.25 = (bf16[512,384]{1,0:T(8,128)(2,1)S(1)}, bf16[512,384]{1,0:T(8,128)(2,1)S(1)}, u32[]{:S(2)}, u32[]{:S(2)}) collective-permute-start(bf16[512,384]{1,0:T(8,128)(2,1)S(1)} %collective-permute-done.23.refs_2_), channel_id=1, source_target_pairs={{0,224},{32,0},{64,32},{96,64},{128,96},{160,128},{192,160},{224,1... | collective-permute-start | bytes 1179656 | tf_op jit(solution)/shard_map/ppermute | solution.py:30
  48.7 21.6 %collective-permute-start.24 = (bf16[512,384]{1,0:T(8,128)(2,1)S(1)}, bf16[512,384]{1,0:T(8,128)(2,1)S(1)}, u32[]{:S(2)}, u32[]{:S(2)}) collective-permute-start(bf16[512,384]{1,0:T(8,128)(2,1)S(1)} %collective-permute-done.22.refs_1_), channel_id=1, source_target_pairs={{0,32},{32,64},{64,96},{96,128},{128,160},{160,192},{192,224},{224... | collective-permute-start | bytes 1179656 | tf_op jit(solution)/shard_map/ppermute | solution.py:30
  60.3 7.4 %collective-permute-start.14 = (bf16[144,256]{1,0:T(8,128)(2,1)S(1)}, bf16[144,256]{1,0:T(8,128)(2,1)S(1)}, u32[]{:S(2)}, u32[]{:S(2)}) collective-permute-start(bf16[144,256]{1,0:T(8,128)(2,1)S(1)} %get-tuple-element.26), channel_id=1, source_target_pairs={{0,24},{8,0},{16,8},{24,16},{1,25},{9,1},{17,9},{25,17},{2,26},{10... | collective-permute-start | bytes 221192 | tf_op jit(solution)/shard_map/ppermute | solution.py:30
  60.4 7.3 %collective-permute-start.15 = (bf16[144,256]{1,0:T(8,128)(2,1)S(1)}, bf16[144,256]{1,0:T(8,128)(2,1)S(1)}, u32[]{:S(2)}, u32[]{:S(2)}) collective-permute-start(bf16[144,256]{1,0:T(8,128)(2,1)S(1)} %get-tuple-element.27), channel_id=1, source_target_pairs={{0,16},{8,24},{16,0},{24,8},{1,17},{9,25},{17,1},{25,9},{2,18},{10... | collective-permute-start | bytes 221192 | tf_op jit(solution)/shard_map/ppermute | solution.py:30
  61.8 6.5 %collective-permute-start.16 = (bf16[144,256]{1,0:T(8,128)(2,1)S(1)}, bf16[144,256]{1,0:T(8,128)(2,1)S(1)}, u32[]{:S(2)}, u32[]{:S(2)}) collective-permute-start(bf16[144,256]{1,0:T(8,128)(2,1)S(1)} %get-tuple-element.28), channel_id=1, source_target_pairs={{0,8},{8,16},{16,24},{24,0},{1,9},{9,17},{17,25},{25,1},{2,10},{10... | collective-permute-start | bytes 221192 | tf_op jit(solution)/shard_map/ppermute | solution.py:30
  68.7 7.9 %collective-permute-start.19 = (bf16[144,256]{1,0:T(8,128)(2,1)S(1)}, bf16[144,256]{1,0:T(8,128)(2,1)S(1)}, u32[]{:S(2)}, u32[]{:S(2)}) collective-permute-start(bf16[144,256]{1,0:T(8,128)(2,1)S(1)} %join.1.refs_0_), channel_id=1, source_target_pairs={{0,1},{1,2},{2,3},{3,0},{4,5},{5,6},{6,7},{7,4},{8,9},{9,10},{10,1... | collective-permute-start | bytes 221192 | tf_op jit(solution)/shard_map/ppermute | solution.py:30
  70.3 18.3 %collective-permute-start.27 = (bf16[512,384]{1,0:T(8,128)(2,1)S(1)}, bf16[512,384]{1,0:T(8,128)(2,1)S(1)}, u32[]{:S(2)}, u32[]{:S(2)}) collective-permute-start(bf16[512,384]{1,0:T(8,128)(2,1)S(1)} %collective-permute-done.25.refs_4_), channel_id=1, source_target_pairs={{0,224},{32,0},{64,32},{96,64},{128,96},{160,128},{192,160},{224,1... | collective-permute-start | bytes 1179656 | tf_op jit(solution)/shard_map/ppermute | solution.py:30
  70.3 18.4 %collective-permute-start.26 = (bf16[512,384]{1,0:T(8,128)(2,1)S(1)}, bf16[512,384]{1,0:T(8,128)(2,1)S(1)}, u32[]{:S(2)}, u32[]{:S(2)}) collective-permute-start(bf16[512,384]{1,0:T(8,128)(2,1)S(1)} %collective-permute-done.24.refs_3_), channel_id=1, source_target_pairs={{0,32},{32,64},{64,96},{96,128},{128,160},{160,192},{192,224},{224... | collective-permute-start | bytes 1179656 | tf_op jit(solution)/shard_map/ppermute | solution.py:30
  74.2 17.8 %collective-permute-start.31 = (bf16[512,384]{1,0:T(8,128)(2,1)S(1)}, bf16[512,384]{1,0:T(8,128)(2,1)S(1)}, u32[]{:S(2)}, u32[]{:S(2)}) collective-permute-start(bf16[512,384]{1,0:T(8,128)(2,1)S(1)} %lay_down.1.refs_8_), channel_id=1, source_target_pairs={{0,8},{8,16},{16,24},{24,0},{1,9},{9,17},{17,25},{25,1},{2,10},{10... | collective-permute-start | bytes 1179656 | tf_op jit(solution)/shard_map/ppermute | solution.py:30
  76.6 18.7 %collective-permute-start.30 = (bf16[512,384]{1,0:T(8,128)(2,1)S(1)}, bf16[512,384]{1,0:T(8,128)(2,1)S(1)}, u32[]{:S(2)}, u32[]{:S(2)}) collective-permute-start(bf16[512,384]{1,0:T(8,128)(2,1)S(1)} %lay_down.1.refs_8_), channel_id=1, source_target_pairs={{0,24},{8,0},{16,8},{24,16},{1,25},{9,1},{17,9},{25,17},{2,26},{10... | collective-permute-start | bytes 1179656 | tf_op jit(solution)/shard_map/ppermute | solution.py:30
  88.5 14.7 %collective-permute-start.20 = (bf16[144,2048]{1,0:T(8,128)(2,1)S(1)}, bf16[144,2048]{1,0:T(8,128)(2,1)S(1)}, u32[]{:S(2)}, u32[]{:S(2)}) collective-permute-start(bf16[144,2048]{1,0:T(8,128)(2,1)S(1)} %get-tuple-element.30.own), channel_id=1, source_target_pairs={{0,4},{4,0},{1,5},{5,1},{2,6},{6,2},{3,7},{7,3},{8,12},{12,8},{9,1... | collective-permute-start | bytes 1769480 | tf_op jit(solution)/shard_map/ppermute | solution.py:34
  88.6 8.6 %collective-permute-start.29 = (bf16[256,384]{1,0:T(8,128)(2,1)S(1)}, bf16[256,384]{1,0:T(8,128)(2,1)S(1)}, u32[]{:S(2)}, u32[]{:S(2)}) collective-permute-start(bf16[256,384]{1,0:T(8,128)(2,1)S(1)} %slice.61), channel_id=1, source_target_pairs={{0,224},{32,0},{64,32},{96,64},{128,96},{160,128},{192,160},{224,1... | collective-permute-start | bytes 589832 | tf_op jit(solution)/shard_map/ppermute | solution.py:30
  88.7 8.5 %collective-permute-start.28 = (bf16[256,384]{1,0:T(8,128)(2,1)S(1)}, bf16[256,384]{1,0:T(8,128)(2,1)S(1)}, u32[]{:S(2)}, u32[]{:S(2)}) collective-permute-start(bf16[256,384]{1,0:T(8,128)(2,1)S(1)} %slice.60), channel_id=1, source_target_pairs={{0,32},{32,64},{64,96},{96,128},{128,160},{160,192},{192,224},{224... | collective-permute-start | bytes 589832 | tf_op jit(solution)/shard_map/ppermute | solution.py:30
  92.1 7.6 %collective-permute-start.32 = (bf16[256,384]{1,0:T(8,128)(2,1)S(1)}, bf16[256,384]{1,0:T(8,128)(2,1)S(1)}, u32[]{:S(2)}, u32[]{:S(2)}) collective-permute-start(bf16[256,384]{1,0:T(8,128)(2,1)S(1)} %slice.62), channel_id=1, source_target_pairs={{0,8},{8,16},{16,24},{24,0},{1,9},{9,17},{17,25},{25,1},{2,10},{10... | collective-permute-start | bytes 589832 | tf_op jit(solution)/shard_map/ppermute | solution.py:30
  95.4 7.7 %collective-permute-start.33 = (bf16[256,384]{1,0:T(8,128)(2,1)S(1)}, bf16[256,384]{1,0:T(8,128)(2,1)S(1)}, u32[]{:S(2)}, u32[]{:S(2)}) collective-permute-start(bf16[256,384]{1,0:T(8,128)(2,1)S(1)} %slice.63), channel_id=1, source_target_pairs={{0,24},{8,0},{16,8},{24,16},{1,25},{9,1},{17,9},{25,17},{2,26},{10... | collective-permute-start | bytes 589832 | tf_op jit(solution)/shard_map/ppermute | solution.py:30
  108.3 6.8 %collective-permute-start.35 = (bf16[32,2048]{1,0:T(8,128)(2,1)S(1)}, bf16[32,2048]{1,0:T(8,128)(2,1)S(1)}, u32[]{:S(2)}, u32[]{:S(2)}) collective-permute-start(bf16[32,2048]{1,0:T(8,128)(2,1)S(1)} %get-tuple-element.35), channel_id=1, source_target_pairs={{0,1},{1,2},{2,3},{3,0},{4,5},{5,6},{6,7},{7,4},{8,9},{9,10},{10,1... | collective-permute-start | bytes 393224 | tf_op jit(solution)/shard_map/ppermute | solution.py:30
  109.9 7.5 %collective-permute-start.37 = (bf16[32,2048]{1,0:T(8,128)(2,1)S(1)}, bf16[32,2048]{1,0:T(8,128)(2,1)S(1)}, u32[]{:S(2)}, u32[]{:S(2)}) collective-permute-start(bf16[32,2048]{1,0:T(8,128)(2,1)S(1)} %get-tuple-element.36), channel_id=1, source_target_pairs={{0,3},{1,0},{2,1},{3,2},{4,7},{5,4},{6,5},{7,6},{8,11},{9,8},{10,9... | collective-permute-start | bytes 393224 | tf_op jit(solution)/shard_map/ppermute | solution.py:30
  111.7 7.5 %collective-permute-start.36 = (bf16[32,2048]{1,0:T(8,128)(2,1)S(1)}, bf16[32,2048]{1,0:T(8,128)(2,1)S(1)}, u32[]{:S(2)}, u32[]{:S(2)}) collective-permute-start(bf16[32,2048]{1,0:T(8,128)(2,1)S(1)} %get-tuple-element.37), channel_id=1, source_target_pairs={{0,2},{1,3},{2,0},{3,1},{4,6},{5,7},{6,4},{7,5},{8,10},{9,11},{10,... | collective-permute-start | bytes 393224 | tf_op jit(solution)/shard_map/ppermute | solution.py:30
  (17 other events, 177.7 us)

commit v3 on v2

--- a/solution.py
+++ b/solution.py
@@ -77,9 +77,9 @@
     )(own, other, weight, cos, sin)
 
 
-def begin_kernel(meta, cos, sin, lat, down, key, q, gate, value, weight, *refs):
+def begin_kernel(meta, cos, sin, lat, down, key, q, gate, value, weight, res, *refs):
     packed, out, edge, keep, send, near = refs[:6]
-    down_v, key_v, q_v, gate_v, value_v, sems = refs[6:]
+    down_v, key_v, q_v, gate_v, value_v, res_v, sems = refs[6:]
     c = meta[3]
     pairs = (
         (down, down_v),
@@ -89,6 +89,7 @@
         (gate, gate_v),
         (value, value_v),
         (weight, near),
+        (res.at[pl.ds(pl.multiple_of(112 * c, 16), 16)], res_v),
     )
     copies = [pltpu.make_async_copy(a, b, sems.at[i]) for i, (a, b) in enumerate(pairs)]
     for copy in copies:
@@ -122,19 +123,24 @@
 
     pl.when(c == 0)(lambda: halves(slice(0, 384), slice(384, 768)))
     pl.when(c == 1)(lambda: halves(slice(384, 768), slice(0, 384)))
+    copies[7].wait()
+    edge[:, 384:2432] = jnp.where(
+        c == 1, res_v[15:16, :].astype(F32), res_v[0:1, :].astype(F32)
+    ).astype(BF)
     copies[2].wait()
     copies[6].wait()
 
 
 def begin(meta, cos, sin, *far):
-    shapes = ((192, 512), (128, 384), (1, 384), (64, 384), (64, 384), (512, 384))
-    scratch = ((32, 768), (64, 128), (320, 128), (32, 768), (32, 768))
+    shapes = ((192, 512), (128, 384), (1, 2432), (64, 384), (64, 384), (512, 384))
+    scratch = ((32, 768), (64, 128), (320, 128), (32, 768), (32, 768), (16, 2048))
+    far = [pltpu.with_memory_space_constraint(v, pltpu.HBM) for v in far]
     return pl.pallas_call(
         begin_kernel,
-        in_specs=[SM, VM, VM] + [pl.BlockSpec(memory_space=pl.ANY)] * 7,
+        in_specs=[SM, VM, VM] + [pl.BlockSpec(memory_space=pltpu.HBM)] * 8,
         out_shape=[jax.ShapeDtypeStruct(shape, BF) for shape in shapes],
         scratch_shapes=[pltpu.VMEM(shape, BF) for shape in scratch]
-        + [pltpu.SemaphoreType.DMA((7,))],
+        + [pltpu.SemaphoreType.DMA((8,))],
         name="begin",
         compiler_params=limit(8),
     )(meta, cos, sin, *far)
@@ -411,13 +417,12 @@
         gate_weight,
         value_weight,
         expand_weight,
+        residual,
     )
     m0 = expand(packed, swap(packed), near, cos, sin)
     r1 = step(m0)
     got = swap(send)
     pairs = [(i, i + 1) for i in range(1, nsp - 1, 2)] + [(i, i - 1) for i in range(2, nsp, 2)]
-    line = lax.dynamic_slice_in_dim(residual, c * (tok - 1), 1, 0)
-    edge = jnp.concatenate([edge, line], axis=1)
     edge = lax.ppermute(edge, SP, pairs)
     halo_res = jnp.pad(edge[:, 384:], ((0, 15), (0, 0)))
     qw = lay(meta, q, edge[:, :384], keep, got)

time: 120 us -> 116 us (0.967)
  the two profiles are of different devices: /device:TPU:120 before, /device:TPU:1 now
where the time goes in v3:
time: 116 us; the launch traced here: 115 us
  starting transfers between devices  53.8 us (46%)
  waiting for transfers between devices  46.8 us (40%)
  Pallas kernels  13.1 us (11%)
  other arithmetic  1.2 us (1%)
    ppermute x25, starting transfers between devices, shift(): return lax.ppermute(x, axis, [(i, (i + k) % n) for i in range(n)])  34.5 us
    ppermute x25, waiting for transfers between devices, shift(): return lax.ppermute(x, axis, [(i, (i + k) % n) for i in range(n)])  26.9 us
    ppermute x4, waiting for transfers between devices, step(): return lax.ppermute(v, ('z', 'c'), ring)  14.2 us
    ppermute x8, starting transfers between devices, swap(): return lax.ppermute(x, 'c', [(0, 1), (1, 0)])  9.56 us
    ppermute x4, starting transfers between devices, step(): return lax.ppermute(v, ('z', 'c'), ring)  6.06 us
    pallas_call x1, Pallas kernels, attend(): pl.pallas_call(functools.partial(attend_kernel, nq, nk), out_shape=[jax.S...  4.69 us
    ppermute x8, waiting for transfers between devices, swap(): return lax.ppermute(x, 'c', [(0, 1), (1, 0)])  4.03 us
    ppermute x1, starting transfers between devices, body(): edge = lax.ppermute(edge, SP, pairs)  3.59 us
  transfers between devices with their start and end apart: 38, of which 18 were waited for; matrix products, arithmetic and copies ran while one was open for 0% of the time, Pallas kernels for 7%

profile of v3, /device:TPU:1, one launch (start us, length us, event | category | flops | bytes accessed | tf_op | source)
XLA Modules:
  0.0 115.5 jit_solution(7937354304758497044)
XLA Ops:
  0.4 1.8 %begin.1 = (bf16[192,512]{1,0:T(8,128)(2,1)S(1)}, bf16[128,384]{1,0:T(8,128)(2,1)S(1)}, bf16[1,2432]{1,0:T(2,128)(2,1)S(1)}, bf16[64,384]{1,0:T(8,128)(2,1)S(1)}...) custom-call(s32[5]{0:T(128)S(1)} %stack.27.meta, f32[32,256]{1,0:T(8,128)S(1)} %get-tuple-element.39.cos, ...), custom_call_target="tpu_custom_call" | custom-call | tf_op jit(solution)/shard_map/begin/pallas_call | solution.py:138
  2.2 3.3 %collective-permute-start.5 = (bf16[192,512]{1,0:T(8,128)(2,1)S(1)}, bf16[192,512]{1,0:T(8,128)(2,1)S(1)}, u32[]{:S(2)}, u32[]{:S(2)}) collective-permute-start(bf16[192,512]{1,0:T(8,128)(2,1)S(1)} %get-tuple-element.23.own), channel_id=1, source_target_pairs={{0,4},{4,0},{1,5},{5,1},{2,6},{6,2},{3,7},{7,3},{8,12},{12,8},{9,1... | collective-permute-start | bytes 589832 | tf_op jit(solution)/shard_map/ppermute | solution.py:34
  6.9 4.0 %collective-permute-start.6 = (bf16[352,512]{1,0:T(8,128)(2,1)S(1)}, bf16[352,512]{1,0:T(8,128)(2,1)S(1)}, u32[]{:S(2)}, u32[]{:S(2)}) collective-permute-start(bf16[352,512]{1,0:T(8,128)(2,1)S(1)} %expand.1.refs_4_.refs_0_), channel_id=1, source_target_pairs={{0,32},{32,64},{64,96},{96,128},{128,160},{160,192},{192,224},{224... | collective-permute-start | bytes 1081352 | tf_op jit(solution)/shard_map/ppermute | solution.py:407
  10.8 3.6 %collective-permute-start = (bf16[1,2432]{1,0:T(2,128)(2,1)S(1)}, bf16[1,2432]{1,0:T(2,128)(2,1)S(1)}, u32[]{:S(2)}, u32[]{:S(2)}) collective-permute-start(bf16[1,2432]{1,0:T(2,128)(2,1)S(1)} %get-tuple-element.20), channel_id=1, source_target_pairs={{4,8},{12,16},{20,24},{28,32},{36,40},{44,48},{52,56},{60,64},{68,... | collective-permute-start | bytes 14600 | tf_op jit(solution)/shard_map/ppermute | solution.py:426
  14.4 1.7 %collective-permute-done = bf16[1,2432]{1,0:T(2,128)(2,1)S(1)} collective-permute-done((bf16[1,2432]{1,0:T(2,128)(2,1)S(1)}, bf16[1,2432]{1,0:T(2,128)(2,1)S(1)}, u32[]{:S(2)}, u32[]{:S(2)}) %collective-permute-start) | collective-permute-done | bytes 4896 | tf_op jit(solution)/shard_map/ppermute | solution.py:426
  16.7 4.6 %collective-permute-start.4 = (bf16[272,384]{1,0:T(8,128)(2,1)S(1)}, bf16[272,384]{1,0:T(8,128)(2,1)S(1)}, u32[]{:S(2)}, u32[]{:S(2)}) collective-permute-start(bf16[272,384]{1,0:T(8,128)(2,1)S(1)} %lay.1.refs_0_), channel_id=1, source_target_pairs={{0,24},{8,0},{16,8},{24,16},{1,25},{9,1},{17,9},{25,17},{2,26},{10... | collective-permute-start | bytes 626696 | tf_op jit(solution)/shard_map/ppermute | solution.py:30
  21.3 3.8 %collective-permute-done.4.refs_3_ = bf16[272,384]{1,0:T(8,128)(2,1)S(1)} collective-permute-done((bf16[272,384]{1,0:T(8,128)(2,1)S(1)}, bf16[272,384]{1,0:T(8,128)(2,1)S(1)}, u32[]{:S(2)}, u32[]{:S(2)}) %collective-permute-start.4) | collective-permute-done | bytes 208928 | tf_op jit(solution)/shard_map/ppermute | solution.py:30
  25.2 3.5 %collective-permute-start.21 = (bf16[128,384]{1,0:T(8,128)(2,1)S(1)}, bf16[128,384]{1,0:T(8,128)(2,1)S(1)}, u32[]{:S(2)}, u32[]{:S(2)}) collective-permute-start(bf16[128,384]{1,0:T(8,128)(2,1)S(1)} %slice.58), channel_id=1, source_target_pairs={{0,24},{8,0},{16,8},{24,16},{1,25},{9,1},{17,9},{25,17},{2,26},{10... | collective-permute-start | bytes 294920 | tf_op jit(solution)/shard_map/ppermute | solution.py:30
  28.7 2.3 %collective-permute-done.21 = bf16[128,384]{1,0:T(8,128)(2,1)S(1)} collective-permute-done((bf16[128,384]{1,0:T(8,128)(2,1)S(1)}, bf16[128,384]{1,0:T(8,128)(2,1)S(1)}, u32[]{:S(2)}, u32[]{:S(2)}) %collective-permute-start.21) | collective-permute-done | bytes 98336 | tf_op jit(solution)/shard_map/ppermute | solution.py:30
  33.4 12.7 %collective-permute-done.8.refs_7_.refs_3_ = bf16[352,512]{1,0:T(8,128)(2,1)S(1)} collective-permute-done((bf16[352,512]{1,0:T(8,128)(2,1)S(1)}, bf16[352,512]{1,0:T(8,128)(2,1)S(1)}, u32[]{:S(2)}, u32[]{:S(2)}) %collective-permute-start.8) | collective-permute-done | bytes 360480 | tf_op jit(solution)/shard_map/ppermute | solution.py:407
  49.1 1.4 %collective-permute-done.9.refs_8_.refs_4_ = bf16[176,512]{1,0:T(8,128)(2,1)S(1)} collective-permute-done((bf16[176,512]{1,0:T(8,128)(2,1)S(1)}, bf16[176,512]{1,0:T(8,128)(2,1)S(1)}, u32[]{:S(2)}, u32[]{:S(2)}) %collective-permute-start.9) | collective-permute-done | bytes 180256 | tf_op jit(solution)/shard_map/ppermute | solution.py:407
  52.0 4.7 %attend.1 = (bf16[144,256]{1,0:T(8,128)(2,1)S(1)}, bf16[144,256]{1,0:T(8,128)(2,1)S(1)}, bf16[144,256]{1,0:T(8,128)(2,1)S(1)}, bf16[144,256]{1,0:T(8,128)(2,1)S(1)}) custom-call(bf16[272,384]{1,0:T(8,128)(2,1)S(1)} %lay.1.refs_0_, bf16[272,384]{1,0:T(8,128)(2,1)S(1)} %collective-permute-done.2.refs_1_, bf16[144,384]{1,0:T(8,128)(2,1)S(1)} %collective-permute-done.3.refs_2_, ...), custom_call_target="tpu_custom_call" | custom-call | tf_op jit(solution)/shard_map/attend/pallas_call | solution.py:252
  56.7 3.2 %collective-permute-start.14 = (bf16[144,256]{1,0:T(8,128)(2,1)S(1)}, bf16[144,256]{1,0:T(8,128)(2,1)S(1)}, u32[]{:S(2)}, u32[]{:S(2)}) collective-permute-start(bf16[144,256]{1,0:T(8,128)(2,1)S(1)} %get-tuple-element.26), channel_id=1, source_target_pairs={{0,24},{8,0},{16,8},{24,16},{1,25},{9,1},{17,9},{25,17},{2,26},{10... | collective-permute-start | bytes 221192 | tf_op jit(solution)/shard_map/ppermute | solution.py:30
  60.6 2.4 %collective-permute-done.14.refs_1_ = bf16[144,256]{1,0:T(8,128)(2,1)S(1)} collective-permute-done((bf16[144,256]{1,0:T(8,128)(2,1)S(1)}, bf16[144,256]{1,0:T(8,128)(2,1)S(1)}, u32[]{:S(2)}, u32[]{:S(2)}) %collective-permute-start.14) | collective-permute-done | bytes 73760 | tf_op jit(solution)/shard_map/ppermute | solution.py:30
  62.9 1.8 %collective-permute-done.15.refs_2_ = bf16[144,256]{1,0:T(8,128)(2,1)S(1)} collective-permute-done((bf16[144,256]{1,0:T(8,128)(2,1)S(1)}, bf16[144,256]{1,0:T(8,128)(2,1)S(1)}, u32[]{:S(2)}, u32[]{:S(2)}) %collective-permute-start.15) | collective-permute-done | bytes 73760 | tf_op jit(solution)/shard_map/ppermute | solution.py:30
  64.7 1.9 %collective-permute-done.16.refs_3_ = bf16[144,256]{1,0:T(8,128)(2,1)S(1)} collective-permute-done((bf16[144,256]{1,0:T(8,128)(2,1)S(1)}, bf16[144,256]{1,0:T(8,128)(2,1)S(1)}, u32[]{:S(2)}, u32[]{:S(2)}) %collective-permute-start.16) | collective-permute-done | bytes 73760 | tf_op jit(solution)/shard_map/ppermute | solution.py:30
  68.3 2.6 %collective-permute-start.27 = (bf16[512,384]{1,0:T(8,128)(2,1)S(1)}, bf16[512,384]{1,0:T(8,128)(2,1)S(1)}, u32[]{:S(2)}, u32[]{:S(2)}) collective-permute-start(bf16[512,384]{1,0:T(8,128)(2,1)S(1)} %collective-permute-done.25.refs_4_), channel_id=1, source_target_pairs={{0,224},{32,0},{64,32},{96,64},{128,96},{160,128},{192,160},{224,1... | collective-permute-start | bytes 1179656 | tf_op jit(solution)/shard_map/ppermute | solution.py:30
  71.7 2.7 %collective-permute-start.30 = (bf16[512,384]{1,0:T(8,128)(2,1)S(1)}, bf16[512,384]{1,0:T(8,128)(2,1)S(1)}, u32[]{:S(2)}, u32[]{:S(2)}) collective-permute-start(bf16[512,384]{1,0:T(8,128)(2,1)S(1)} %lay_down.1.refs_8_), channel_id=1, source_target_pairs={{0,24},{8,0},{16,8},{24,16},{1,25},{9,1},{17,9},{25,17},{2,26},{10... | collective-permute-start | bytes 1179656 | tf_op jit(solution)/shard_map/ppermute | solution.py:30
  74.3 2.5 %collective-permute-start.18 = (bf16[144,256]{1,0:T(8,128)(2,1)S(1)}, bf16[144,256]{1,0:T(8,128)(2,1)S(1)}, u32[]{:S(2)}, u32[]{:S(2)}) collective-permute-start(bf16[144,256]{1,0:T(8,128)(2,1)S(1)} %join.1.refs_0_), channel_id=1, source_target_pairs={{0,2},{1,3},{2,0},{3,1},{4,6},{5,7},{6,4},{7,5},{8,10},{9,11},{10,... | collective-permute-start | bytes 221192 | tf_op jit(solution)/shard_map/ppermute | solution.py:30
  76.8 2.3 %collective-permute-done.18.refs_2_ = bf16[144,256]{1,0:T(8,128)(2,1)S(1)} collective-permute-done((bf16[144,256]{1,0:T(8,128)(2,1)S(1)}, bf16[144,256]{1,0:T(8,128)(2,1)S(1)}, u32[]{:S(2)}, u32[]{:S(2)}) %collective-permute-start.18) | collective-permute-done | bytes 73760 | tf_op jit(solution)/shard_map/ppermute | solution.py:30
  79.0 1.5 %collective-permute-start.17 = (bf16[144,256]{1,0:T(8,128)(2,1)S(1)}, bf16[144,256]{1,0:T(8,128)(2,1)S(1)}, u32[]{:S(2)}, u32[]{:S(2)}) collective-permute-start(bf16[144,256]{1,0:T(8,128)(2,1)S(1)} %join.1.refs_0_), channel_id=1, source_target_pairs={{0,3},{1,0},{2,1},{3,2},{4,7},{5,4},{6,5},{7,6},{8,11},{9,8},{10,9... | collective-permute-start | bytes 221192 | tf_op jit(solution)/shard_map/ppermute | solution.py:30
  80.6 2.0 %collective-permute-done.17.refs_1_ = bf16[144,256]{1,0:T(8,128)(2,1)S(1)} collective-permute-done((bf16[144,256]{1,0:T(8,128)(2,1)S(1)}, bf16[144,256]{1,0:T(8,128)(2,1)S(1)}, u32[]{:S(2)}, u32[]{:S(2)}) %collective-permute-start.17) | collective-permute-done | bytes 73760 | tf_op jit(solution)/shard_map/ppermute | solution.py:30
  82.6 1.6 %project.1 = (bf16[32,2048]{1,0:T(8,128)(2,1)S(1)}, bf16[144,2048]{1,0:T(8,128)(2,1)S(1)}) custom-call(s32[5]{0:T(128)S(1)} %stack.27.meta, bf16[144,256]{1,0:T(8,128)(2,1)S(1)} %join.1.refs_0_, bf16[144,256]{1,0:T(8,128)(2,1)S(1)} %collective-permute-done.17.refs_1_, bf16[144,256]{1,0:T(8,128)(2,1)S(1)} %collective-permute-done.18.refs_2_, ...), custom_call_target="tpu_custom_call" | custom-call | tf_op jit(solution)/shard_map/project/pallas_call | solution.py:309
  84.2 4.0 %collective-permute-start.20 = (bf16[144,2048]{1,0:T(8,128)(2,1)S(1)}, bf16[144,2048]{1,0:T(8,128)(2,1)S(1)}, u32[]{:S(2)}, u32[]{:S(2)}) collective-permute-start(bf16[144,2048]{1,0:T(8,128)(2,1)S(1)} %get-tuple-element.30.own), channel_id=1, source_target_pairs={{0,4},{4,0},{1,5},{5,1},{2,6},{6,2},{3,7},{7,3},{8,12},{12,8},{9,1... | collective-permute-start | bytes 1769480 | tf_op jit(solution)/shard_map/ppermute | solution.py:34
  88.2 3.0 %collective-permute-start.29 = (bf16[256,384]{1,0:T(8,128)(2,1)S(1)}, bf16[256,384]{1,0:T(8,128)(2,1)S(1)}, u32[]{:S(2)}, u32[]{:S(2)}) collective-permute-start(bf16[256,384]{1,0:T(8,128)(2,1)S(1)} %slice.61), channel_id=1, source_target_pairs={{0,224},{32,0},{64,32},{96,64},{128,96},{160,128},{192,160},{224,1... | collective-permute-start | bytes 589832 | tf_op jit(solution)/shard_map/ppermute | solution.py:30
  91.5 2.7 %collective-permute-start.33 = (bf16[256,384]{1,0:T(8,128)(2,1)S(1)}, bf16[256,384]{1,0:T(8,128)(2,1)S(1)}, u32[]{:S(2)}, u32[]{:S(2)}) collective-permute-start(bf16[256,384]{1,0:T(8,128)(2,1)S(1)} %slice.63), channel_id=1, source_target_pairs={{0,24},{8,0},{16,8},{24,16},{1,25},{9,1},{17,9},{25,17},{2,26},{10... | collective-permute-start | bytes 589832 | tf_op jit(solution)/shard_map/ppermute | solution.py:30
  95.4 3.2 %collective-permute-done.28 = bf16[256,384]{1,0:T(8,128)(2,1)S(1)} collective-permute-done((bf16[256,384]{1,0:T(8,128)(2,1)S(1)}, bf16[256,384]{1,0:T(8,128)(2,1)S(1)}, u32[]{:S(2)}, u32[]{:S(2)}) %collective-permute-start.28) | collective-permute-done | bytes 196640 | tf_op jit(solution)/shard_map/ppermute | solution.py:30
  98.8 3.0 %mixer.1 = (f32[128,2048]{1,0:T(8,128)S(1)}, bf16[128,2048]{1,0:T(8,128)(2,1)S(1)}) custom-call(s32[5]{0:T(128)S(1)} %stack.27.meta, bf16[144,2048]{1,0:T(8,128)(2,1)S(1)} %get-tuple-element.30.own, bf16[144,2048]{1,0:T(8,128)(2,1)S(1)} %collective-permute-done.20.other, bf16[3,384]{1,0:T(4,128)(2,1)S(1)} %slice_select_fusion.taps, ...), custom_call_target="tpu_custom_call" | custom-call | tf_op jit(solution)/shard_map/mixer/pallas_call | solution.py:368
  103.1 1.5 %collective-permute-done.34 = bf16[128,2048]{1,0:T(8,128)(2,1)S(1)} collective-permute-done((bf16[128,2048]{1,0:T(8,128)(2,1)S(1)}, bf16[128,2048]{1,0:T(8,128)(2,1)S(1)}, u32[]{:S(2)}, u32[]{:S(2)}) %collective-permute-start.34) | collective-permute-done | bytes 524320 | tf_op jit(solution)/shard_map/ppermute | solution.py:34
  106.1 1.6 %collective-permute-start.37 = (bf16[32,2048]{1,0:T(8,128)(2,1)S(1)}, bf16[32,2048]{1,0:T(8,128)(2,1)S(1)}, u32[]{:S(2)}, u32[]{:S(2)}) collective-permute-start(bf16[32,2048]{1,0:T(8,128)(2,1)S(1)} %get-tuple-element.36), channel_id=1, source_target_pairs={{0,3},{1,0},{2,1},{3,2},{4,7},{5,4},{6,5},{7,6},{8,11},{9,8},{10,9... | collective-permute-start | bytes 393224 | tf_op jit(solution)/shard_map/ppermute | solution.py:30
  108.8 2.0 %collective-permute-done.35 = bf16[32,2048]{1,0:T(8,128)(2,1)S(1)} collective-permute-done((bf16[32,2048]{1,0:T(8,128)(2,1)S(1)}, bf16[32,2048]{1,0:T(8,128)(2,1)S(1)}, u32[]{:S(2)}, u32[]{:S(2)}) %collective-permute-start.35) | collective-permute-done | bytes 131104 | tf_op jit(solution)/shard_map/ppermute | solution.py:30
  110.8 4.0 %collective-permute-done.36 = bf16[32,2048]{1,0:T(8,128)(2,1)S(1)} collective-permute-done((bf16[32,2048]{1,0:T(8,128)(2,1)S(1)}, bf16[32,2048]{1,0:T(8,128)(2,1)S(1)}, u32[]{:S(2)}, u32[]{:S(2)}) %collective-permute-start.36) | collective-permute-done | bytes 131104 | tf_op jit(solution)/shard_map/ppermute | solution.py:30
  (84 shorter events, 18.5 us)
Async XLA Ops:
  6.9 14.5 %collective-permute-start.6 = (bf16[352,512]{1,0:T(8,128)(2,1)S(1)}, bf16[352,512]{1,0:T(8,128)(2,1)S(1)}, u32[]{:S(2)}, u32[]{:S(2)}) collective-permute-start(bf16[352,512]{1,0:T(8,128)(2,1)S(1)} %expand.1.refs_4_.refs_0_), channel_id=1, source_target_pairs={{0,32},{32,64},{64,96},{96,128},{128,160},{160,192},{192,224},{224... | collective-permute-start | bytes 1081352 | tf_op jit(solution)/shard_map/ppermute | solution.py:407
  10.8 5.3 %collective-permute-start.1 = (bf16[64,384]{1,0:T(8,128)(2,1)S(1)}, bf16[64,384]{1,0:T(8,128)(2,1)S(1)}, u32[]{:S(2)}, u32[]{:S(2)}) collective-permute-start(bf16[64,384]{1,0:T(8,128)(2,1)S(1)} %get-tuple-element.22), channel_id=1, source_target_pairs={{0,4},{4,0},{1,5},{5,1},{2,6},{6,2},{3,7},{7,3},{8,12},{12,8},{9,1... | collective-permute-start | bytes 147464 | tf_op jit(solution)/shard_map/ppermute | solution.py:34
  10.8 5.3 %collective-permute-start = (bf16[1,2432]{1,0:T(2,128)(2,1)S(1)}, bf16[1,2432]{1,0:T(2,128)(2,1)S(1)}, u32[]{:S(2)}, u32[]{:S(2)}) collective-permute-start(bf16[1,2432]{1,0:T(2,128)(2,1)S(1)} %get-tuple-element.20), channel_id=1, source_target_pairs={{4,8},{12,16},{20,24},{28,32},{36,40},{44,48},{52,56},{60,64},{68,... | collective-permute-start | bytes 14600 | tf_op jit(solution)/shard_map/ppermute | solution.py:426
  16.7 8.5 %collective-permute-start.4 = (bf16[272,384]{1,0:T(8,128)(2,1)S(1)}, bf16[272,384]{1,0:T(8,128)(2,1)S(1)}, u32[]{:S(2)}, u32[]{:S(2)}) collective-permute-start(bf16[272,384]{1,0:T(8,128)(2,1)S(1)} %lay.1.refs_0_), channel_id=1, source_target_pairs={{0,24},{8,0},{16,8},{24,16},{1,25},{9,1},{17,9},{25,17},{2,26},{10... | collective-permute-start | bytes 626696 | tf_op jit(solution)/shard_map/ppermute | solution.py:30
  21.3 7.4 %collective-permute-start.2 = (bf16[272,384]{1,0:T(8,128)(2,1)S(1)}, bf16[272,384]{1,0:T(8,128)(2,1)S(1)}, u32[]{:S(2)}, u32[]{:S(2)}) collective-permute-start(bf16[272,384]{1,0:T(8,128)(2,1)S(1)} %lay.1.refs_0_), channel_id=1, source_target_pairs={{0,8},{8,16},{16,24},{24,0},{1,9},{9,17},{17,25},{25,1},{2,10},{10... | collective-permute-start | bytes 626696 | tf_op jit(solution)/shard_map/ppermute | solution.py:30
  21.3 9.8 %collective-permute-start.7 = (bf16[352,512]{1,0:T(8,128)(2,1)S(1)}, bf16[352,512]{1,0:T(8,128)(2,1)S(1)}, u32[]{:S(2)}, u32[]{:S(2)}) collective-permute-start(bf16[352,512]{1,0:T(8,128)(2,1)S(1)} %collective-permute-done.6.refs_5_.refs_1_), channel_id=1, source_target_pairs={{0,32},{32,64},{64,96},{96,128},{128,160},{160,192},{192,224},{224... | collective-permute-start | bytes 1081352 | tf_op jit(solution)/shard_map/ppermute | solution.py:407
  25.2 5.8 %collective-permute-start.21 = (bf16[128,384]{1,0:T(8,128)(2,1)S(1)}, bf16[128,384]{1,0:T(8,128)(2,1)S(1)}, u32[]{:S(2)}, u32[]{:S(2)}) collective-permute-start(bf16[128,384]{1,0:T(8,128)(2,1)S(1)} %slice.58), channel_id=1, source_target_pairs={{0,24},{8,0},{16,8},{24,16},{1,25},{9,1},{17,9},{25,17},{2,26},{10... | collective-permute-start | bytes 294920 | tf_op jit(solution)/shard_map/ppermute | solution.py:30
  31.0 16.1 %collective-permute-start.23 = (bf16[512,384]{1,0:T(8,128)(2,1)S(1)}, bf16[512,384]{1,0:T(8,128)(2,1)S(1)}, u32[]{:S(2)}, u32[]{:S(2)}) collective-permute-start(bf16[512,384]{1,0:T(8,128)(2,1)S(1)} %pad_maximum_fusion.refs_0_), channel_id=1, source_target_pairs={{0,224},{32,0},{64,32},{96,64},{128,96},{160,128},{192,160},{224,1... | collective-permute-start | bytes 1179656 | tf_op jit(solution)/shard_map/ppermute | solution.py:30
  31.1 15.0 %collective-permute-start.8 = (bf16[352,512]{1,0:T(8,128)(2,1)S(1)}, bf16[352,512]{1,0:T(8,128)(2,1)S(1)}, u32[]{:S(2)}, u32[]{:S(2)}) collective-permute-start(bf16[352,512]{1,0:T(8,128)(2,1)S(1)} %collective-permute-done.7.refs_6_.refs_2_), channel_id=1, source_target_pairs={{0,32},{32,64},{64,96},{96,128},{128,160},{160,192},{192,224},{224... | collective-permute-start | bytes 1081352 | tf_op jit(solution)/shard_map/ppermute | solution.py:407
  32.2 15.5 %collective-permute-start.22 = (bf16[512,384]{1,0:T(8,128)(2,1)S(1)}, bf16[512,384]{1,0:T(8,128)(2,1)S(1)}, u32[]{:S(2)}, u32[]{:S(2)}) collective-permute-start(bf16[512,384]{1,0:T(8,128)(2,1)S(1)} %pad_maximum_fusion.refs_0_), channel_id=1, source_target_pairs={{0,32},{32,64},{64,96},{96,128},{128,160},{160,192},{192,224},{224... | collective-permute-start | bytes 1179656 | tf_op jit(solution)/shard_map/ppermute | solution.py:30
  32.7 15.2 %collective-permute-start.10 = (bf16[352,512]{1,0:T(8,128)(2,1)S(1)}, bf16[352,512]{1,0:T(8,128)(2,1)S(1)}, u32[]{:S(2)}, u32[]{:S(2)}) collective-permute-start(bf16[352,512]{1,0:T(8,128)(2,1)S(1)} %collective-permute-done.6.refs_5_.refs_1_), channel_id=1, source_target_pairs={{0,4},{4,0},{1,5},{5,1},{2,6},{6,2},{3,7},{7,3},{8,12},{12,8},{9,1... | collective-permute-start | bytes 1081352 | tf_op jit(solution)/shard_map/ppermute | solution.py:34
  33.3 13.9 %collective-permute-start.3 = (bf16[144,384]{1,0:T(8,128)(2,1)S(1)}, bf16[144,384]{1,0:T(8,128)(2,1)S(1)}, u32[]{:S(2)}, u32[]{:S(2)}) collective-permute-start(bf16[144,384]{1,0:T(8,128)(2,1)S(1)} %slice.54), channel_id=1, source_target_pairs={{0,8},{8,16},{16,24},{24,0},{1,9},{9,17},{17,25},{25,1},{2,10},{10... | collective-permute-start | bytes 331784 | tf_op jit(solution)/shard_map/ppermute | solution.py:30
  47.2 4.8 %collective-permute-start.12 = (bf16[352,512]{1,0:T(8,128)(2,1)S(1)}, bf16[352,512]{1,0:T(8,128)(2,1)S(1)}, u32[]{:S(2)}, u32[]{:S(2)}) collective-permute-start(bf16[352,512]{1,0:T(8,128)(2,1)S(1)} %collective-permute-done.8.refs_7_.refs_3_), channel_id=1, source_target_pairs={{0,4},{4,0},{1,5},{5,1},{2,6},{6,2},{3,7},{7,3},{8,12},{12,8},{9,1... | collective-permute-start | bytes 1081352 | tf_op jit(solution)/shard_map/ppermute | solution.py:34
  47.7 20.7 %collective-permute-start.25 = (bf16[512,384]{1,0:T(8,128)(2,1)S(1)}, bf16[512,384]{1,0:T(8,128)(2,1)S(1)}, u32[]{:S(2)}, u32[]{:S(2)}) collective-permute-start(bf16[512,384]{1,0:T(8,128)(2,1)S(1)} %collective-permute-done.23.refs_2_), channel_id=1, source_target_pairs={{0,224},{32,0},{64,32},{96,64},{128,96},{160,128},{192,160},{224,1... | collective-permute-start | bytes 1179656 | tf_op jit(solution)/shard_map/ppermute | solution.py:30
  47.9 23.1 %collective-permute-start.24 = (bf16[512,384]{1,0:T(8,128)(2,1)S(1)}, bf16[512,384]{1,0:T(8,128)(2,1)S(1)}, u32[]{:S(2)}, u32[]{:S(2)}) collective-permute-start(bf16[512,384]{1,0:T(8,128)(2,1)S(1)} %collective-permute-done.22.refs_1_), channel_id=1, source_target_pairs={{0,32},{32,64},{64,96},{96,128},{128,160},{160,192},{192,224},{224... | collective-permute-start | bytes 1179656 | tf_op jit(solution)/shard_map/ppermute | solution.py:30
  56.7 6.2 %collective-permute-start.14 = (bf16[144,256]{1,0:T(8,128)(2,1)S(1)}, bf16[144,256]{1,0:T(8,128)(2,1)S(1)}, u32[]{:S(2)}, u32[]{:S(2)}) collective-permute-start(bf16[144,256]{1,0:T(8,128)(2,1)S(1)} %get-tuple-element.26), channel_id=1, source_target_pairs={{0,24},{8,0},{16,8},{24,16},{1,25},{9,1},{17,9},{25,17},{2,26},{10... | collective-permute-start | bytes 221192 | tf_op jit(solution)/shard_map/ppermute | solution.py:30
  59.9 4.8 %collective-permute-start.15 = (bf16[144,256]{1,0:T(8,128)(2,1)S(1)}, bf16[144,256]{1,0:T(8,128)(2,1)S(1)}, u32[]{:S(2)}, u32[]{:S(2)}) collective-permute-start(bf16[144,256]{1,0:T(8,128)(2,1)S(1)} %get-tuple-element.27), channel_id=1, source_target_pairs={{0,16},{8,24},{16,0},{24,8},{1,17},{9,25},{17,1},{25,9},{2,18},{10... | collective-permute-start | bytes 221192 | tf_op jit(solution)/shard_map/ppermute | solution.py:30
  59.9 6.7 %collective-permute-start.16 = (bf16[144,256]{1,0:T(8,128)(2,1)S(1)}, bf16[144,256]{1,0:T(8,128)(2,1)S(1)}, u32[]{:S(2)}, u32[]{:S(2)}) collective-permute-start(bf16[144,256]{1,0:T(8,128)(2,1)S(1)} %get-tuple-element.28), channel_id=1, source_target_pairs={{0,8},{8,16},{16,24},{24,0},{1,9},{9,17},{17,25},{25,1},{2,10},{10... | collective-permute-start | bytes 221192 | tf_op jit(solution)/shard_map/ppermute | solution.py:30
  67.0 7.3 %collective-permute-start.19 = (bf16[144,256]{1,0:T(8,128)(2,1)S(1)}, bf16[144,256]{1,0:T(8,128)(2,1)S(1)}, u32[]{:S(2)}, u32[]{:S(2)}) collective-permute-start(bf16[144,256]{1,0:T(8,128)(2,1)S(1)} %join.1.refs_0_), channel_id=1, source_target_pairs={{0,1},{1,2},{2,3},{3,0},{4,5},{5,6},{6,7},{7,4},{8,9},{9,10},{10,1... | collective-permute-start | bytes 221192 | tf_op jit(solution)/shard_map/ppermute | solution.py:30
  68.3 19.8 %collective-permute-start.27 = (bf16[512,384]{1,0:T(8,128)(2,1)S(1)}, bf16[512,384]{1,0:T(8,128)(2,1)S(1)}, u32[]{:S(2)}, u32[]{:S(2)}) collective-permute-start(bf16[512,384]{1,0:T(8,128)(2,1)S(1)} %collective-permute-done.25.refs_4_), channel_id=1, source_target_pairs={{0,224},{32,0},{64,32},{96,64},{128,96},{160,128},{192,160},{224,1... | collective-permute-start | bytes 1179656 | tf_op jit(solution)/shard_map/ppermute | solution.py:30
  70.9 20.2 %collective-permute-start.26 = (bf16[512,384]{1,0:T(8,128)(2,1)S(1)}, bf16[512,384]{1,0:T(8,128)(2,1)S(1)}, u32[]{:S(2)}, u32[]{:S(2)}) collective-permute-start(bf16[512,384]{1,0:T(8,128)(2,1)S(1)} %collective-permute-done.24.refs_3_), channel_id=1, source_target_pairs={{0,32},{32,64},{64,96},{96,128},{128,160},{160,192},{192,224},{224... | collective-permute-start | bytes 1179656 | tf_op jit(solution)/shard_map/ppermute | solution.py:30
  71.6 19.7 %collective-permute-start.31 = (bf16[512,384]{1,0:T(8,128)(2,1)S(1)}, bf16[512,384]{1,0:T(8,128)(2,1)S(1)}, u32[]{:S(2)}, u32[]{:S(2)}) collective-permute-start(bf16[512,384]{1,0:T(8,128)(2,1)S(1)} %lay_down.1.refs_8_), channel_id=1, source_target_pairs={{0,8},{8,16},{16,24},{24,0},{1,9},{9,17},{17,25},{25,1},{2,10},{10... | collective-permute-start | bytes 1179656 | tf_op jit(solution)/shard_map/ppermute | solution.py:30
  71.7 19.8 %collective-permute-start.30 = (bf16[512,384]{1,0:T(8,128)(2,1)S(1)}, bf16[512,384]{1,0:T(8,128)(2,1)S(1)}, u32[]{:S(2)}, u32[]{:S(2)}) collective-permute-start(bf16[512,384]{1,0:T(8,128)(2,1)S(1)} %lay_down.1.refs_8_), channel_id=1, source_target_pairs={{0,24},{8,0},{16,8},{24,16},{1,25},{9,1},{17,9},{25,17},{2,26},{10... | collective-permute-start | bytes 1179656 | tf_op jit(solution)/shard_map/ppermute | solution.py:30
  74.3 4.7 %collective-permute-start.18 = (bf16[144,256]{1,0:T(8,128)(2,1)S(1)}, bf16[144,256]{1,0:T(8,128)(2,1)S(1)}, u32[]{:S(2)}, u32[]{:S(2)}) collective-permute-start(bf16[144,256]{1,0:T(8,128)(2,1)S(1)} %join.1.refs_0_), channel_id=1, source_target_pairs={{0,2},{1,3},{2,0},{3,1},{4,6},{5,7},{6,4},{7,5},{8,10},{9,11},{10,... | collective-permute-start | bytes 221192 | tf_op jit(solution)/shard_map/ppermute | solution.py:30
  84.2 14.6 %collective-permute-start.20 = (bf16[144,2048]{1,0:T(8,128)(2,1)S(1)}, bf16[144,2048]{1,0:T(8,128)(2,1)S(1)}, u32[]{:S(2)}, u32[]{:S(2)}) collective-permute-start(bf16[144,2048]{1,0:T(8,128)(2,1)S(1)} %get-tuple-element.30.own), channel_id=1, source_target_pairs={{0,4},{4,0},{1,5},{5,1},{2,6},{6,2},{3,7},{7,3},{8,12},{12,8},{9,1... | collective-permute-start | bytes 1769480 | tf_op jit(solution)/shard_map/ppermute | solution.py:34
  88.2 7.3 %collective-permute-start.29 = (bf16[256,384]{1,0:T(8,128)(2,1)S(1)}, bf16[256,384]{1,0:T(8,128)(2,1)S(1)}, u32[]{:S(2)}, u32[]{:S(2)}) collective-permute-start(bf16[256,384]{1,0:T(8,128)(2,1)S(1)} %slice.61), channel_id=1, source_target_pairs={{0,224},{32,0},{64,32},{96,64},{128,96},{160,128},{192,160},{224,1... | collective-permute-start | bytes 589832 | tf_op jit(solution)/shard_map/ppermute | solution.py:30
  91.2 7.4 %collective-permute-start.28 = (bf16[256,384]{1,0:T(8,128)(2,1)S(1)}, bf16[256,384]{1,0:T(8,128)(2,1)S(1)}, u32[]{:S(2)}, u32[]{:S(2)}) collective-permute-start(bf16[256,384]{1,0:T(8,128)(2,1)S(1)} %slice.60), channel_id=1, source_target_pairs={{0,32},{32,64},{64,96},{96,128},{128,160},{160,192},{192,224},{224... | collective-permute-start | bytes 589832 | tf_op jit(solution)/shard_map/ppermute | solution.py:30
  91.3 7.4 %collective-permute-start.32 = (bf16[256,384]{1,0:T(8,128)(2,1)S(1)}, bf16[256,384]{1,0:T(8,128)(2,1)S(1)}, u32[]{:S(2)}, u32[]{:S(2)}) collective-permute-start(bf16[256,384]{1,0:T(8,128)(2,1)S(1)} %slice.62), channel_id=1, source_target_pairs={{0,8},{8,16},{16,24},{24,0},{1,9},{9,17},{17,25},{25,1},{2,10},{10... | collective-permute-start | bytes 589832 | tf_op jit(solution)/shard_map/ppermute | solution.py:30
  91.5 7.3 %collective-permute-start.33 = (bf16[256,384]{1,0:T(8,128)(2,1)S(1)}, bf16[256,384]{1,0:T(8,128)(2,1)S(1)}, u32[]{:S(2)}, u32[]{:S(2)}) collective-permute-start(bf16[256,384]{1,0:T(8,128)(2,1)S(1)} %slice.63), channel_id=1, source_target_pairs={{0,24},{8,0},{16,8},{24,16},{1,25},{9,1},{17,9},{25,17},{2,26},{10... | collective-permute-start | bytes 589832 | tf_op jit(solution)/shard_map/ppermute | solution.py:30
  104.8 6.0 %collective-permute-start.35 = (bf16[32,2048]{1,0:T(8,128)(2,1)S(1)}, bf16[32,2048]{1,0:T(8,128)(2,1)S(1)}, u32[]{:S(2)}, u32[]{:S(2)}) collective-permute-start(bf16[32,2048]{1,0:T(8,128)(2,1)S(1)} %get-tuple-element.35), channel_id=1, source_target_pairs={{0,1},{1,2},{2,3},{3,0},{4,5},{5,6},{6,7},{7,4},{8,9},{9,10},{10,1... | collective-permute-start | bytes 393224 | tf_op jit(solution)/shard_map/ppermute | solution.py:30
  106.1 4.7 %collective-permute-start.37 = (bf16[32,2048]{1,0:T(8,128)(2,1)S(1)}, bf16[32,2048]{1,0:T(8,128)(2,1)S(1)}, u32[]{:S(2)}, u32[]{:S(2)}) collective-permute-start(bf16[32,2048]{1,0:T(8,128)(2,1)S(1)} %get-tuple-element.36), channel_id=1, source_target_pairs={{0,3},{1,0},{2,1},{3,2},{4,7},{5,4},{6,5},{7,6},{8,11},{9,8},{10,9... | collective-permute-start | bytes 393224 | tf_op jit(solution)/shard_map/ppermute | solution.py:30
  107.6 7.1 %collective-permute-start.36 = (bf16[32,2048]{1,0:T(8,128)(2,1)S(1)}, bf16[32,2048]{1,0:T(8,128)(2,1)S(1)}, u32[]{:S(2)}, u32[]{:S(2)}) collective-permute-start(bf16[32,2048]{1,0:T(8,128)(2,1)S(1)} %get-tuple-element.37), channel_id=1, source_target_pairs={{0,2},{1,3},{2,0},{3,1},{4,6},{5,7},{6,4},{7,5},{8,10},{9,11},{10,... | collective-permute-start | bytes 393224 | tf_op jit(solution)/shard_map/ppermute | solution.py:30
  (10 other events, 149.9 us)
